TPU v7x, 256 devices: a whole 4x4x8 slice. The times are simulated.
256 devices in a mesh: ep: 32 (over z, x), tp: 8 (over y, core).
Axes of the slice: x: 4, y: 4, z: 8, core: 2. Of those that a mesh axis runs over, the one named last changes fastest.
Arguments:
- tokens: bfloat16 [512, 2048], P('ep'), may hold values from -6 to 6
- norm_attn: float32 [2048], replicated, may hold values from 0.1 to 1.9
- w_query: bfloat16 [2048, 1024], P(None, 'tp'), may hold values from -0.125 to 0.125
- w_key: bfloat16 [2048, 1024], P(None, 'tp'), may hold values from -0.125 to 0.125
- w_value: bfloat16 [2048, 1024], P(None, 'tp'), may hold values from -0.125 to 0.125
- w_forget: bfloat16 [2048, 16], P(None, 'tp'), may hold values from -0.125 to 0.125
- forget_bias: float32 [16], P('tp'), may hold values from -1.5 to 1.5
- w_output: bfloat16 [1024, 2048], P('tp'), may hold values from -0.1875 to 0.1875
- key_cache: bfloat16 [512, 1024, 1024], P('ep', None, 'tp'), may hold values from -488 to 488
- value_cache: bfloat16 [512, 1024, 1024], P('ep', None, 'tp'), may hold values from -6 to 6
- gate_cache: float32 [512, 16, 1024], P('ep', 'tp'), may hold values from -132 to 0, as said below
- lengths: int32 [512], P('ep'), may hold values from 256 to 1024
- norm_ffn: float32 [2048], replicated, may hold values from 0.1 to 1.9
- route_group: int32 [512], P('ep'), may hold values from 0 to 3
- route_slot: int32 [512, 2], P('ep'), may hold values from 0 to 7, as said below
- route_weight: float32 [512, 2], P('ep'), may hold values from 0.2 to 1
- expert_gate: bfloat16 [32, 2048, 1024], P('ep', None, 'tp'), may hold values from -0.125 to 0.125
- expert_up: bfloat16 [32, 2048, 1024], P('ep', None, 'tp'), may hold values from -0.125 to 0.125
- expert_down: bfloat16 [32, 1024, 2048], P('ep', 'tp'), may hold values from -0.1875 to 0.1875
- dense_gate: bfloat16 [2048, 4096], P('tp', 'ep'), may hold values from -0.125 to 0.125
- dense_up: bfloat16 [2048, 4096], P('tp', 'ep'), may hold values from -0.125 to 0.125
- dense_down: bfloat16 [4096, 2048], P('ep', 'tp'), may hold values from -0.09375 to 0.09375
- mix_vector: float32 [2048], replicated, may hold values from -0.125 to 0.125
Outputs:
- mixed_out: bfloat16 [512, 2048], P('ep', 'tp')
Inputs may be any that keep to these rules, and one draw needn't show every extreme that they name: `route_slot`: the two picks of a token are different experts of its group. Among the sequences of one index of ep at most 2 picks name one expert, and in every draw some expert gets exactly 2 picks from every index of ep. `gate_cache`: along the positions of each sequence and head the values never rise.
All inputs are finite; a program needn't handle non-finite values.
Results may differ from a plain program's by a relative error of at most 0.014.
Values may be sent and summed in bfloat16 or wider, within the bound.
No kernel may reach another device: no remote copies, remote signals or barrier semaphores. Data moves between devices by JAX's collectives and lax.ppermute only.
A program may use at most 64 MiB of HBM per device.

v0:
```python
import jax
import jax.numpy as jnp
from jax import lax
from jax.sharding import Mesh
from jax.sharding import PartitionSpec as P

EXPERTS_PER_GROUP = 8
EP = ("ep_0", "ep_1")


EPS = 1e-06


def sent_to_all(array, axis):
    devices = lax.axis_size(axis)
    return lax.all_to_all(
        jnp.broadcast_to(array[None], (devices, *array.shape)), axis, 0, 0, tiled=True
    )


def of_everyone(array, axis):
    return sent_to_all(array, axis).astype(jnp.float32).sum(axis=0)


def split_up(array, dim, devices):
    before, after = (array.shape[:dim], array.shape[dim + 1 :])
    return jnp.moveaxis(array.reshape(*before, devices, -1, *after), dim, 0)


def sum_at_owner(array, axis, dim):
    devices = lax.axis_size(axis)
    tiles = lax.all_to_all(split_up(array, dim, devices), axis, 0, 0, tiled=True)
    return jnp.sum(tiles.astype(jnp.float32), axis=0)


def in_one_piece(arrays, axis, dim, along):
    ends, at = ([], 0)
    for a in arrays[:-1]:
        at += a.shape[along]
        ends.append(at)
    both = jnp.concatenate(arrays, axis=along)
    return tuple(jnp.split(lax.all_gather(both, axis, axis=dim, tiled=True), ends, axis=along))


def whole_of(array, axes, dim):
    for axis in reversed(axes):
        array = lax.all_gather(array, axis, axis=dim, tiled=True)
    return array


def rms_scale(row_block, gain_vector):
    row_block = row_block.astype(jnp.float32)
    return (
        row_block
        * lax.rsqrt(jnp.mean(row_block * row_block, axis=-1, keepdims=True) + EPS)
        * gain_vector
    )


def bf16_round(array):
    return lax.optimization_barrier(array.astype(jnp.bfloat16)).astype(jnp.float32)


def attend(queries, key_new, value_new, forget_log, key_cache, value_cache, gate_cache, lengths):
    seq_count, cache_len, head_width = key_cache.shape
    head_local = gate_cache.shape[1]
    head_size = head_width // head_local
    score_scale = head_size ** (-0.5)
    query_h = queries.reshape(seq_count, head_local, head_size)
    key_rows = key_cache.reshape(seq_count, cache_len, head_local, head_size)
    value_rows = value_cache.reshape(seq_count, cache_len, head_local, head_size)
    entry_indices = jnp.arange(cache_len, dtype=jnp.int32)
    at_last = entry_indices[None, None, :] == (lengths - 1)[:, None, None]
    last_gate = jnp.sum(jnp.where(at_last, gate_cache, jnp.zeros_like(gate_cache)), axis=2)
    current = last_gate + forget_log
    scores = (
        jnp.einsum("shd,sjhd->shj", query_h, key_rows, preferred_element_type=jnp.float32)
        * score_scale
    )
    scores = scores + (current[:, :, None] - gate_cache)
    scores = jnp.where(entry_indices[None, None, :] < lengths[:, None, None], scores, -jnp.inf)
    own_score = (
        jnp.sum(
            query_h.astype(jnp.float32)
            * key_new.reshape(seq_count, head_local, head_size).astype(jnp.float32),
            axis=2,
        )
        * score_scale
    )
    row_peak = jnp.maximum(jnp.max(scores, axis=2), own_score)
    weights = jnp.exp(scores - row_peak[:, :, None])
    own_weight = jnp.exp(own_score - row_peak)
    denominator = jnp.sum(weights, axis=2) + own_weight
    weighted = jnp.einsum(
        "shj,sjhd->shd",
        weights.astype(jnp.bfloat16),
        value_rows,
        preferred_element_type=jnp.float32,
    )
    weighted = weighted + bf16_round(own_weight)[:, :, None] * value_new.reshape(
        seq_count, head_local, head_size
    ).astype(jnp.float32)
    return (weighted / denominator[:, :, None]).astype(jnp.bfloat16).reshape(seq_count, head_width)


def body(
    tokens,
    norm_attn,
    w_query,
    w_key,
    w_value,
    w_forget,
    forget_bias,
    w_output,
    key_cache,
    value_cache,
    gate_cache,
    lengths,
    norm_ffn,
    route_group,
    route_slot,
    route_weight,
    expert_gate,
    expert_up,
    expert_down,
    dense_gate,
    dense_up,
    dense_down,
    mix_vector,
):
    seq_local = tokens.shape[0]
    model_width = tokens.shape[1]
    ep_count = lax.axis_size(EP)
    tp_count = lax.axis_size("tp")
    tp_position = lax.axis_index("tp")
    width_local = model_width // tp_count
    normed = rms_scale(tokens, norm_attn).astype(jnp.bfloat16)
    queries = jnp.dot(normed, w_query, preferred_element_type=jnp.float32).astype(jnp.bfloat16)
    key_new = jnp.dot(normed, w_key, preferred_element_type=jnp.float32).astype(jnp.bfloat16)
    value_new = jnp.dot(normed, w_value, preferred_element_type=jnp.float32).astype(jnp.bfloat16)
    forget_log = jax.nn.log_sigmoid(
        jnp.dot(normed, w_forget, preferred_element_type=jnp.float32) + forget_bias
    )
    attended = attend(
        queries, key_new, value_new, forget_log, key_cache, value_cache, gate_cache, lengths
    )
    head_part = bf16_round(jnp.dot(attended, w_output, preferred_element_type=jnp.float32))
    attn_sum = of_everyone(head_part.astype(jnp.bfloat16), "tp").astype(jnp.float32)
    residual = tokens.astype(jnp.float32) + attn_sum
    normed_ffn = rms_scale(residual, norm_ffn).astype(jnp.bfloat16)
    residual_mine = lax.dynamic_slice_in_dim(residual, tp_position * width_local, width_local, 1)
    normed_mine = lax.dynamic_slice_in_dim(normed_ffn, tp_position * width_local, width_local, 1)
    mix_gate = jax.nn.sigmoid(
        jnp.dot(normed_ffn.astype(jnp.float32), mix_vector, precision=lax.Precision.HIGHEST)
    )
    picks = route_slot.shape[1]
    expert_local = expert_gate.shape[0]
    expert_count = expert_local * ep_count
    capacity = seq_local // EXPERTS_PER_GROUP
    flat_ids = (route_group[:, None] * EXPERTS_PER_GROUP + route_slot).reshape(-1)
    matches = (flat_ids[:, None] == jnp.arange(expert_count, dtype=jnp.int32)[None, :]).astype(
        jnp.int32
    )
    earlier = jnp.sum((jnp.cumsum(matches, axis=0) - matches) * matches, axis=1)
    slot_ids = flat_ids * capacity + earlier
    slot_table = slot_ids[:, None] == jnp.arange(expert_count * capacity, dtype=jnp.int32)[None, :]
    replicas = jnp.repeat(normed_ffn, picks, axis=0)
    outgoing = jnp.einsum(
        "rc,rd->cd", slot_table.astype(jnp.bfloat16), replicas, preferred_element_type=jnp.float32
    ).astype(jnp.bfloat16)
    outgoing = outgoing.reshape(ep_count, expert_local, capacity, model_width)
    arrived = lax.all_to_all(outgoing, EP, split_axis=0, concat_axis=0, tiled=True)
    gate_act = jnp.einsum(
        "nesd,edf->nesf", arrived, expert_gate, preferred_element_type=jnp.float32
    )
    up_act = jnp.einsum("nesd,edf->nesf", arrived, expert_up, preferred_element_type=jnp.float32)
    hidden = (jax.nn.silu(gate_act) * up_act).astype(jnp.bfloat16)
    partial_value = bf16_round(
        jnp.einsum("nesf,efd->nesd", hidden, expert_down, preferred_element_type=jnp.float32)
    )
    summed = sum_at_owner(partial_value.astype(jnp.bfloat16), "tp", 3).astype(jnp.bfloat16)
    returned = lax.all_to_all(summed, EP, split_axis=0, concat_axis=0, tiled=True)
    returned = returned.reshape(expert_count * capacity, width_local)
    pick_weights = route_weight.reshape(-1)
    combine_table = jnp.where(slot_table, pick_weights[:, None], jnp.zeros((), jnp.float32))
    combine_table = jnp.sum(
        combine_table.reshape(seq_local, picks, expert_count * capacity), axis=1
    )
    moe = jnp.dot(combine_table, returned.astype(jnp.float32), precision=lax.Precision.HIGHEST)
    hidden_total = dense_gate.shape[1] * ep_count
    blank_carry = jnp.zeros((seq_local, 2 * hidden_total), jnp.float32)
    running = blank_carry
    portion = in_one_piece((dense_gate, dense_up), EP, 1, 0)
    gate_part = jnp.dot(normed_mine, portion[0], preferred_element_type=jnp.float32)
    up_part = jnp.dot(normed_mine, portion[1], preferred_element_type=jnp.float32)
    running = lax.dynamic_update_slice_in_dim(running, gate_part, jnp.int32(0), 1)
    dense_local = lax.dynamic_update_slice_in_dim(running, up_part, hidden_total, 1)
    dense_pre = of_everyone(bf16_round(dense_local).astype(jnp.bfloat16), "tp").astype(jnp.float32)
    dense_hidden = (jax.nn.silu(dense_pre[:, :hidden_total]) * dense_pre[:, hidden_total:]).astype(
        jnp.bfloat16
    )
    dense_out = jnp.dot(
        dense_hidden, whole_of(dense_down, EP, 0), preferred_element_type=jnp.float32
    )
    return (residual_mine + moe + mix_gate[:, None] * dense_out).astype(jnp.bfloat16)


def solution(mesh):
    split = Mesh(mesh.devices.reshape(8, 4, mesh.shape["tp"]), ("ep_0", "ep_1", "tp"))
    return jax.shard_map(
        body,
        mesh=split,
        in_specs=(
            P(EP, None),
            P(),
            P(None, "tp"),
            P(None, "tp"),
            P(None, "tp"),
            P(None, "tp"),
            P("tp"),
            P("tp", None),
            P(EP, None, "tp"),
            P(EP, None, "tp"),
            P(EP, "tp", None),
            P(EP),
            P(),
            P(EP),
            P(EP, None),
            P(EP, None),
            P(EP, None, "tp"),
            P(EP, None, "tp"),
            P(EP, "tp", None),
            P("tp", EP),
            P("tp", EP),
            P(EP, "tp"),
            P(),
        ),
        out_specs=P(EP, "tp"),
        check_vma=False,
    )
```

profile of v0, /device:TPU:1, one launch (start us, length us, event | category | flops | bytes accessed | tf_op | source)
XLA Modules:
  0.0 152.7 jit_solution(9235204135030168959)
XLA Ops:
  6.5 1.6 %pad_maximum_fusion.1 = bf16[512,128]{1,0:T(8,128)(2,1)} fusion(bf16[256,128]{1,0:T(8,128)(2,1)} %param.43, bf16[256,128]{1,0:T(8,128)(2,1)} %param.42), kind=kLoop, calls=%fused_computation.48 | loop fusion | flops 262144 | bytes 262144 | tf_op jit(solution)/shard_map/concatenate | solution.py:41
  8.2 1.0 fusion.26
  9.1 1.3 convolution_convert_fusion.7
  10.7 6.5 %copy.45 = bf16[16,1024,128]{1,2,0:T(8,128)(2,1)} copy(bf16[16,1024,128]{2,1,0:T(8,128)(2,1)} %param.31) | data formatting | bytes 8388608 | tf_op args[8]
  17.6 0.2 fusion.52
  17.9 0.2 fusion.9
  18.5 2.8 %fusion.63 = f32[16,2,1,1024]{3,2,1,0:T(1,128)S(1)} fusion(bf16[16,2,64,1]{2,3,1,0:T(2,128)(2,1)S(1)} %reshape.185, bf16[16,1024,2,64]{1,3,2,0:T(8,128)(2,1)} %bitcast.97), kind=kOutput, calls=%fused_computation.101 | convolution fusion | flops 4194304 | bytes 4329472 | tf_op jit(solution)/shard_map/shd,sjhd->shj/dot_general | solution.py:77
  21.3 0.3 fusion.61
  21.6 0.3 fusion.35
  21.9 6.5 %copy.48 = bf16[16,1024,128]{1,2,0:T(8,128)(2,1)} copy(bf16[16,1024,128]{2,1,0:T(8,128)(2,1)} %param.32) | data formatting | bytes 8388608 | tf_op args[9]
  28.4 0.2 fusion.8
  28.8 3.4 %fusion.32 = f32[16,2,1,64]{3,2,1,0:T(1,128)S(1)} fusion(bf16[16,1024,2,64]{1,3,2,0:T(8,128)(2,1)} %bitcast.98, bf16[16,2,1024,1]{2,1,0,3:T(2,128)(2,1)S(1)} %get-tuple-element.10), kind=kOutput, calls=%fused_computation.52 | convolution fusion | flops 4194304 | bytes 4268032 | tf_op jit(solution)/shard_map/shj,sjhd->shd/dot_general | solution.py:94
  32.6 0.9 broadcast_in_dim.40
  33.4 6.6 %all-to-all-start = ((bf16[8,16,2048]{2,1,0:T(8,128)(2,1)}), bf16[8,16,2048]{2,1,0:T(8,128)(2,1)S(1)}, u32[]{:S(2)}, u32[]{:S(2)}) async-start(bf16[8,16,2048]{2,1,0:T(8,128)(2,1)} %broadcast_in_dim.40), calls=%async_computation | async-start | bytes 1048576 | tf_op jit(solution)/shard_map/all_to_all | solution.py:16
  40.7 8.8 %all-to-all-done = bf16[8,16,2048]{2,1,0:T(8,128)(2,1)S(1)} async-done(((bf16[8,16,2048]{2,1,0:T(8,128)(2,1)}), bf16[8,16,2048]{2,1,0:T(8,128)(2,1)S(1)}, u32[]{:S(2)}, u32[]{:S(2)}) %all-to-all-start) | async-done | bytes 524320 | tf_op jit(solution)/shard_map/all_to_all | solution.py:16
  49.9 0.3 convolution_convert_fusion.3
  50.4 23.5 %all_to_all.25 = bf16[32,1,2,2048]{3,2,1,0:T(2,128)(2,1)S(1)} all-to-all(bf16[32,1,2,2048]{3,2,1,0:T(2,128)(2,1)S(1)} %bitcast.100), channel_id=1, replica_groups=mesh['ep_0'=8,'ep_1'=4,'tp'=8] {'ep_0','ep_1'}, dimensions={0} | all-to-all | bytes 524288 | tf_op jit(solution)/shard_map/all_to_all | solution.py:172
  74.0 0.2 convolution_bitcast_fusion.1
  74.3 0.4 fusion
  74.7 0.7 copy.76
  75.4 6.7 %all-to-all-start.2 = ((bf16[8,32,1,2,256]{4,1,3,2,0:T(8,128)(2,1)}), bf16[8,32,1,2,256]{4,1,3,2,0:T(8,128)(2,1)S(1)}, u32[]{:S(2)}, u32[]{:S(2)}) async-start(bf16[8,32,1,2,256]{4,1,3,2,0:T(8,128)(2,1)} %bitcast.96), calls=%async_computation.2 | async-start | bytes 524288 | tf_op jit(solution)/shard_map/all_to_all | solution.py:32
  82.1 11.4 %all_gather.10 = bf16[512,256]{1,0:T(8,128)(2,1)} all-gather(bf16[128,256]{1,0:T(8,128)(2,1)S(1)} %copy-done.9), channel_id=1, replica_groups=mesh['ep_0'=8,'ep_1'=4,'tp'=8] {'ep_1'}, dimensions={0}, use_global_device_ids=true | all-gather | bytes 327680 | tf_op jit(solution)/shard_map/all_gather | solution.py:47
  93.6 0.6 copy.55
  94.2 3.9 %all-to-all-start.3 = ((bf16[32,1,2,256]{3,2,1,0:T(2,128)(2,1)}), bf16[32,1,2,256]{3,2,1,0:T(2,128)(2,1)S(1)}, u32[]{:S(2)}, u32[]{:S(2)}) async-start(bf16[32,1,2,256]{3,2,1,0:T(2,128)(2,1)} %copy.55), calls=%async_computation.3 | async-start | bytes 65536 | tf_op jit(solution)/shard_map/all_to_all | solution.py:182
  98.2 2.0 %convolution_convert_fusion = bf16[16,4096]{1,0:T(8,128)(2,1)S(1)} fusion(bf16[512,4096]{1,0:T(8,128)(2,1)} %all-gather.3.cloned.1.call-done, bf16[16,2048]{1,0:T(8,128)(2,1)S(1)} %multiply_convert_fusion, s32[]{:T(128)S(6)} %select_n.25), kind=kOutput, calls=%fused_computation | convolution fusion | flops 33619968 | bytes 2236420 | tf_op jit(solution)/shard_map/dot_general | solution.py:195
  100.2 2.0 %convolution_convert_fusion.1 = bf16[16,4096]{1,0:T(8,128)(2,1)S(1)} fusion(bf16[512,4096]{1,0:T(8,128)(2,1)} %all-gather.3.cloned.1.call-done, bf16[16,2048]{1,0:T(8,128)(2,1)S(1)} %multiply_convert_fusion, s32[]{:T(128)S(6)} %select_n.25), kind=kOutput, calls=%fused_computation.1 | convolution fusion | flops 33619968 | bytes 2236420 | tf_op jit(solution)/shard_map/dot_general | solution.py:194
  102.2 4.6 %all-to-all-done.3 = bf16[32,1,2,256]{3,2,1,0:T(2,128)(2,1)S(1)} async-done(((bf16[32,1,2,256]{3,2,1,0:T(2,128)(2,1)}), bf16[32,1,2,256]{3,2,1,0:T(2,128)(2,1)S(1)}, u32[]{:S(2)}, u32[]{:S(2)}) %all-to-all-start.3) | async-done | bytes 32800 | tf_op jit(solution)/shard_map/all_to_all | solution.py:182
  106.9 1.6 %broadcast_in_dim.48 = bf16[8,16,8192]{2,1,0:T(8,128)(2,1)} broadcast(bf16[16,8192]{1,0:T(8,128)(2,1)S(1)} %pad_maximum_fusion), dimensions={1,2} | broadcast | bytes 2359296 | tf_op jit(solution)/shard_map/broadcast_in_dim | solution.py:17
  108.4 8.3 %all-to-all-start.4 = ((bf16[8,16,8192]{2,1,0:T(8,128)(2,1)}), bf16[8,16,8192]{2,1,0:T(8,128)(2,1)S(1)}, u32[]{:S(2)}, u32[]{:S(2)}) async-start(bf16[8,16,8192]{2,1,0:T(8,128)(2,1)} %broadcast_in_dim.48), calls=%async_computation.4 | async-start | bytes 4194304 | tf_op jit(solution)/shard_map/all_to_all | solution.py:16
  117.4 25.5 %all-to-all-done.4 = bf16[8,16,8192]{2,1,0:T(8,128)(2,1)S(1)} async-done(((bf16[8,16,8192]{2,1,0:T(8,128)(2,1)}), bf16[8,16,8192]{2,1,0:T(8,128)(2,1)S(1)}, u32[]{:S(2)}, u32[]{:S(2)}) %all-to-all-start.4) | async-done | bytes 2097184 | tf_op jit(solution)/shard_map/all_to_all | solution.py:16
  143.0 0.3 convert_reduce_fusion
  143.3 2.6 %fusion.7 = bf16[16,256]{1,0:T(8,128)(2,1)} fusion(f32[16,256]{1,0:T(8,128)S(1)} %convolution_add_fusion, bf16[4096,256]{1,0:T(8,128)(2,1)} %all-gather.5.cloned.1.call-done, f32[16,8192]{1,0:T(8,128)S(1)} %convert_reduce_fusion, f32[16]{0:T(128)S(1)} %fusion.14), kind=kOutput, calls=%fused_computation.17 | convolution fusion | flops 33959936 | bytes 2646080 | tf_op jit(solution)/shard_map/dot_general | solution.py:202
  (85 shorter events, 3.4 us)
Async XLA Ops:
  6.5 67.7 %copy-start = (bf16[1,128,2048]{2,1,0:T(8,128)(2,1)S(1)}, bf16[1,128,2048]{2,1,0:T(8,128)(2,1)}, u32[]{:S(2)}) copy-start(bf16[1,128,2048]{2,1,0:T(8,128)(2,1)} %param.41) | copy-start | bytes 1572868
  6.5 91.6 %all-gather.3.cloned.1.call-start = ((), (), s32[]{:S(2)}) async-start(), calls=%async_computation.5 | async-start | bytes 4325376 | tf_op jit(solution)/shard_map/all_gather | solution.py:42
  10.6 6.6 %copy-start.13 = (s32[16]{0:T(128)S(1)}, s32[16]{0:T(128)}, u32[]{:S(2)}) copy-start(s32[16]{0:T(128)} %param.34) | copy-start | bytes 196
  10.7 6.7 %copy-start.7 = (f32[16,2,1024]{2,1,0:T(2,128)S(1)}, f32[16,2,1024]{2,1,0:T(2,128)}, u32[]{:S(2)}) copy-start(f32[16,2,1024]{2,1,0:T(2,128)} %param.33) | copy-start | bytes 393220
  10.7 7.0 %copy-start.1 = (bf16[16,2048]{1,0:T(8,128)(2,1)S(1)}, bf16[16,2048]{1,0:T(8,128)(2,1)}, u32[]{:S(2)}) copy-start(bf16[16,2048]{1,0:T(8,128)(2,1)} %param.23) | copy-start | bytes 196612
  10.7 7.0 %copy-start.8 = (f32[2048]{0:T(1024)S(1)}, f32[2048]{0:T(1024)}, u32[]{:S(2)}) copy-start(f32[2048]{0:T(1024)} %param.24) | copy-start | bytes 24580
  10.7 7.0 %copy-start.14 = (bf16[2048,2]{0,1:T(2,128)(2,1)S(1)}, bf16[2048,2]{0,1:T(2,128)(2,1)}, u32[]{:S(2)}) copy-start(bf16[2048,2]{0,1:T(2,128)(2,1)} %param.28) | copy-start | bytes 24580
  10.7 6.9 %copy-start.16 = (f32[2]{0:T(128)S(1)}, f32[2]{0:T(128)}, u32[]{:S(2)}) copy-start(f32[2]{0:T(128)} %param.29) | copy-start | bytes 28
  10.7 7.2 %copy-start.4 = (bf16[2048,128]{1,0:T(8,128)(2,1)S(1)}, bf16[2048,128]{1,0:T(8,128)(2,1)}, u32[]{:S(2)}) copy-start(bf16[2048,128]{1,0:T(8,128)(2,1)} %param.26) | copy-start | bytes 1572868
  21.9 6.5 %copy-start.5 = (bf16[2048,128]{1,0:T(8,128)(2,1)S(1)}, bf16[2048,128]{1,0:T(8,128)(2,1)}, u32[]{:S(2)}) copy-start(bf16[2048,128]{1,0:T(8,128)(2,1)} %param.27) | copy-start | bytes 1572868
  28.4 4.0 %copy-start.3 = (bf16[128,2048]{1,0:T(8,128)(2,1)S(1)}, bf16[128,2048]{1,0:T(8,128)(2,1)}, u32[]{:S(2)}) copy-start(bf16[128,2048]{1,0:T(8,128)(2,1)} %param.30) | copy-start | bytes 1572868
  28.4 11.7 %copy-start.11 = (s32[16,2]{0,1:T(2,128)S(1)}, s32[16,2]{0,1:T(2,128)}, u32[]{:S(2)}) copy-start(s32[16,2]{0,1:T(2,128)} %param.37) | copy-start | bytes 388
  28.4 11.7 %copy-start.17 = (s32[16]{0:T(128)S(1)}, s32[16]{0:T(128)}, u32[]{:S(2)}) copy-start(s32[16]{0:T(128)} %param.36) | copy-start | bytes 196
  28.4 21.2 %copy-start.10 = (f32[2048]{0:T(1024)S(1)}, f32[2048]{0:T(1024)}, u32[]{:S(2)}) copy-start(f32[2048]{0:T(1024)} %param.35) | copy-start | bytes 24580
  28.8 45.2 %copy-start.6 = (bf16[1,2048,128]{2,1,0:T(8,128)(2,1)S(1)}, bf16[1,2048,128]{2,1,0:T(8,128)(2,1)}, u32[]{:S(2)}) copy-start(bf16[1,2048,128]{2,1,0:T(8,128)(2,1)} %param.39) | copy-start | bytes 1572868
  32.2 42.0 %copy-start.2 = (bf16[1,2048,128]{2,1,0:T(8,128)(2,1)S(1)}, bf16[1,2048,128]{2,1,0:T(8,128)(2,1)}, u32[]{:S(2)}) copy-start(bf16[1,2048,128]{2,1,0:T(8,128)(2,1)} %param.40) | copy-start | bytes 1572868
  32.6 49.5 %copy-start.9 = (bf16[128,256]{1,0:T(8,128)(2,1)S(1)}, bf16[128,256]{1,0:T(8,128)(2,1)}, u32[]{:S(2)}) copy-start(bf16[128,256]{1,0:T(8,128)(2,1)} %param.44) | copy-start | bytes 196612
  33.4 16.0 %all-to-all-start = ((bf16[8,16,2048]{2,1,0:T(8,128)(2,1)}), bf16[8,16,2048]{2,1,0:T(8,128)(2,1)S(1)}, u32[]{:S(2)}, u32[]{:S(2)}) async-start(bf16[8,16,2048]{2,1,0:T(8,128)(2,1)} %broadcast_in_dim.40), calls=%async_computation | async-start | bytes 1048576 | tf_op jit(solution)/shard_map/all_to_all | solution.py:16
  75.4 18.1 %all-to-all-start.2 = ((bf16[8,32,1,2,256]{4,1,3,2,0:T(8,128)(2,1)}), bf16[8,32,1,2,256]{4,1,3,2,0:T(8,128)(2,1)S(1)}, u32[]{:S(2)}, u32[]{:S(2)}) async-start(bf16[8,32,1,2,256]{4,1,3,2,0:T(8,128)(2,1)} %bitcast.96), calls=%async_computation.2 | async-start | bytes 524288 | tf_op jit(solution)/shard_map/all_to_all | solution.py:32
  82.1 61.2 %all-gather.5.cloned.1.call-start = ((), (), s32[]{:S(2)}) async-start(), calls=%async_computation.6 | async-start | bytes 2359296 | tf_op jit(solution)/shard_map/all_gather | solution.py:47
  94.2 12.7 %all-to-all-start.3 = ((bf16[32,1,2,256]{3,2,1,0:T(2,128)(2,1)}), bf16[32,1,2,256]{3,2,1,0:T(2,128)(2,1)S(1)}, u32[]{:S(2)}, u32[]{:S(2)}) async-start(bf16[32,1,2,256]{3,2,1,0:T(2,128)(2,1)} %copy.55), calls=%async_computation.3 | async-start | bytes 65536 | tf_op jit(solution)/shard_map/all_to_all | solution.py:182
  100.2 16.8 %copy-start.12 = (f32[16,2]{0,1:T(2,128)S(1)}, f32[16,2]{0,1:T(2,128)}, u32[]{:S(2)}) copy-start(f32[16,2]{0,1:T(2,128)} %param.38) | copy-start | bytes 388
  100.2 16.9 %copy-start.15 = (f32[2048]{0:T(1024)S(1)}, f32[2048]{0:T(1024)}, u32[]{:S(2)}) copy-start(f32[2048]{0:T(1024)} %param.45) | copy-start | bytes 24580
  108.4 34.5 %all-to-all-start.4 = ((bf16[8,16,8192]{2,1,0:T(8,128)(2,1)}), bf16[8,16,8192]{2,1,0:T(8,128)(2,1)S(1)}, u32[]{:S(2)}, u32[]{:S(2)}) async-start(bf16[8,16,8192]{2,1,0:T(8,128)(2,1)} %broadcast_in_dim.48), calls=%async_computation.4 | async-start | bytes 4194304 | tf_op jit(solution)/shard_map/all_to_all | solution.py:16
Sparse Core Ops, SparseCore 0:
  9.8 88.3 all-gather.2
  100.0 37.9 all-gather.4
where the time goes:
time: 154 us; the launch traced here: 153 us
  waiting for transfers between devices  39 us (25%)
  blocking collectives  34.9 us (23%)
  starting transfers between devices  25.6 us (17%)
  local copies, waits for them, and re-layouts  18.2 us (12%)
  matrix products  16.3 us (11%)
  between operations  13.7 us (9%)
  other arithmetic  4.93 us (3%)
    all_to_all x2, waiting for transfers between devices, sent_to_all(): lax.all_to_all(jnp.broadcast_to(array[None], (devices, *array.shape)), ax...  34.3 us
    all_to_all x1, blocking collectives, body(): lax.all_to_all(outgoing, EP, split_axis=0, concat_axis=0, tiled=True)  23.5 us
    all_to_all x2, starting transfers between devices, sent_to_all(): lax.all_to_all(jnp.broadcast_to(array[None], (devices, *array.shape)), ax...  15 us
    unnamed x39, local copies, waits for them, and re-layouts  13.2 us
    all_gather x1, blocking collectives, whole_of(): array = lax.all_gather(array, axis, axis=dim, tiled=True)  11.4 us
    all_to_all x1, starting transfers between devices, sum_at_owner(): lax.all_to_all(split_up(array, dim, devices), axis, 0, 0, tiled=True)  6.68 us
    all_to_all x1, waiting for transfers between devices, body(): lax.all_to_all(summed, EP, split_axis=0, concat_axis=0, tiled=True)  4.65 us
    all_to_all x1, starting transfers between devices, body(): lax.all_to_all(summed, EP, split_axis=0, concat_axis=0, tiled=True)  3.94 us
  transfers between devices with their start and end apart: 6, of which 3 were waited for; matrix products, arithmetic and copies ran while one was open for 23% of the time, Pallas kernels for 0%

commit v1 on v0

v1 whole, which is shorter than its diff:
```python
import functools

import jax
import jax.numpy as jnp
from jax import lax
from jax.experimental import pallas as pl
from jax.experimental.pallas import tpu as pltpu
from jax.sharding import Mesh
from jax.sharding import PartitionSpec as P

EXPERTS_PER_GROUP = 8
EP = ("ep_0", "ep_1")
EPS = 1e-06
F32 = jnp.float32
BF16 = jnp.bfloat16
NT = (((1,), (1,)), ((), ()))
VMEM = pl.BlockSpec(memory_space=pltpu.VMEM)
ANY = pl.BlockSpec(memory_space=pl.ANY)
MIB = 1 << 20


def rms_scale(rows, gain):
    rows = rows.astype(F32)
    return rows * lax.rsqrt(jnp.mean(rows * rows, axis=-1, keepdims=True) + EPS) * gain


def silu(v):
    return v * jax.nn.sigmoid(v)


def stacked(pair):
    return jnp.concatenate([pair[:, 0:1], pair[:, 1:2]], axis=0)


def attention_kernel(
    tokens_ref,
    gain_ref,
    forget_ref,
    bias_ref,
    gate_ref,
    length_ref,
    wq_hbm,
    wk_hbm,
    wv_hbm,
    wo_hbm,
    key_hbm,
    value_hbm,
    dg_hbm,
    du_hbm,
    dd_hbm,
    parts_ref,
    dense_ref,
    wqkv,
    wo,
    keys,
    values,
    dense,
    scores,
    weighted,
    w_sems,
    key_sems,
    value_sems,
):
    seqs, cache_len, width = keys.shape
    heads = 2
    half = width // heads
    rows = heads * seqs
    scale = half ** (-0.5)
    weight_copies = [
        pltpu.make_async_copy(src, wqkv.at[i], w_sems.at[i])
        for i, src in enumerate((wq_hbm, wk_hbm, wv_hbm))
    ]
    rows_in = dg_hbm.shape[0]
    hidden_in = dd_hbm.shape[0]
    late_copies = [
        pltpu.make_async_copy(wo_hbm, wo, w_sems.at[3]),
        pltpu.make_async_copy(dg_hbm, dense.at[pl.ds(0, rows_in)], w_sems.at[4]),
        pltpu.make_async_copy(du_hbm, dense.at[pl.ds(rows_in, rows_in)], w_sems.at[5]),
        pltpu.make_async_copy(
            dd_hbm.at[:, pl.ds(0, width)],
            dense.at[pl.ds(2 * rows_in, hidden_in)],
            w_sems.at[6],
        ),
        pltpu.make_async_copy(
            dd_hbm.at[:, pl.ds(width, width)],
            dense.at[pl.ds(2 * rows_in + hidden_in, hidden_in)],
            w_sems.at[7],
        ),
    ]
    key_copies = [
        pltpu.make_async_copy(key_hbm.at[s], keys.at[s], key_sems.at[s]) for s in range(seqs)
    ]
    value_copies = [
        pltpu.make_async_copy(value_hbm.at[s], values.at[s], value_sems.at[s]) for s in range(seqs)
    ]
    for copy in weight_copies + key_copies + late_copies + value_copies:
        copy.start()

    normed = rms_scale(tokens_ref[...], gain_ref[...]).astype(BF16)
    forget_logit = jnp.dot(normed, forget_ref[...], preferred_element_type=F32) + bias_ref[...]
    forget_log = stacked(jax.nn.log_sigmoid(forget_logit))
    qkv = []
    for i in range(3):
        weight_copies[i].wait()
        qkv.append(jnp.dot(normed, wqkv[i], preferred_element_type=F32).astype(BF16).astype(F32))
    query, key_new, value_new = qkv
    lane = lax.broadcasted_iota(jnp.int32, (1, width), 1)
    first_head = lane < half
    own = query * key_new
    own_score = scale * jnp.concatenate(
        [
            jnp.sum(jnp.where(first_head, own, 0.0), axis=1, keepdims=True),
            jnp.sum(jnp.where(first_head, 0.0, own), axis=1, keepdims=True),
        ],
        axis=0,
    )
    row8 = lax.broadcasted_iota(jnp.int32, (8, width), 0)
    lane8 = lax.broadcasted_iota(jnp.int32, (8, width), 1)
    head_mask = (row8 < heads) & ((lane8 < half) == (row8 == 0))
    for s in range(seqs):
        masked = jnp.where(head_mask, query[s : s + 1], 0.0).astype(BF16)
        key_copies[s].wait()
        result = lax.dot_general(masked, keys[s], NT, preferred_element_type=F32)
        scores[s : s + 1] = result[0:1]
        scores[seqs + s : seqs + s + 1] = result[1:2]
    gate = jnp.concatenate([gate_ref[:, 0, :], gate_ref[:, 1, :]], axis=0)
    length = jnp.concatenate([length_ref[...], length_ref[...]], axis=0)
    entry = lax.broadcasted_iota(jnp.int32, (rows, cache_len), 1)
    last_gate = jnp.sum(jnp.where(entry == length - 1, gate, 0.0), axis=1, keepdims=True)
    current = last_gate + forget_log
    score = scores[...] * scale + (current - gate)
    score = jnp.where(entry < length, score, -jnp.inf)
    peak = jnp.maximum(jnp.max(score, axis=1, keepdims=True), own_score)
    weights = jnp.exp(score - peak)
    own_weight = jnp.exp(own_score - peak)
    denominator = jnp.sum(weights, axis=1, keepdims=True) + own_weight
    scores[...] = weights
    for copy in late_copies:
        copy.wait()
    dense_block = dense[...]
    for i in range(dense_ref.shape[0]):
        dense_ref[i] = dense_block
    for s in range(seqs):
        pair = jnp.concatenate(
            [
                scores[s : s + 1],
                scores[seqs + s : seqs + s + 1],
                jnp.zeros((6, cache_len), F32),
            ],
            axis=0,
        ).astype(BF16)
        value_copies[s].wait()
        result = jnp.dot(pair, values[s], preferred_element_type=F32)
        weighted[s : s + 1] = jnp.where(first_head, result[0:1], result[1:2])
    own_weight = own_weight.astype(BF16).astype(F32)
    own_weight = jnp.where(first_head, own_weight[:seqs], own_weight[seqs:])
    denominator = jnp.where(first_head, denominator[:seqs], denominator[seqs:])
    attended = ((weighted[...] + own_weight * value_new) / denominator).astype(BF16)
    part = jnp.dot(attended, wo[...], preferred_element_type=F32).astype(BF16)
    for i in range(parts_ref.shape[0]):
        parts_ref[i] = part


def dispatch_kernel(
    parts_ref, tokens_ref, gain_ref, select_ref, mix_ref, out_ref, residual_ref, mix_gate_ref
):
    half = out_ref.shape[1]
    attn = parts_ref[0].astype(F32)
    for i in range(1, parts_ref.shape[0]):
        attn = attn + parts_ref[i].astype(F32)
    residual = tokens_ref[...].astype(F32) + attn
    residual_ref[...] = residual
    normed = rms_scale(residual, gain_ref[...]).astype(BF16)
    mix_gate_ref[...] = jax.nn.sigmoid(
        jnp.sum(normed.astype(F32) * mix_ref[...], axis=1, keepdims=True)
    )
    both = jnp.concatenate([normed[:, :half], normed[:, half:]], axis=0)
    out_ref[...] = jnp.dot(select_ref[...], both, preferred_element_type=F32).astype(BF16)


def expert_kernel(rows_ref, gate_ref, up_ref, down_ref, dense_ref, out_ref):
    rows, half = rows_ref.shape
    blocks, _, width = dense_ref.shape
    per_half = blocks // 2
    kb = half // per_half
    row = lax.broadcasted_iota(jnp.int32, (rows, 1), 0)
    second = lax.rem(row, 8) >= 4
    is_dense = lax.rem(row, 4) >= 2
    sums = [None, None]
    for t in range(blocks):
        h, b = divmod(t, per_half)
        part = jnp.dot(
            rows_ref[:, b * kb : (b + 1) * kb],
            jnp.concatenate(
                [
                    gate_ref[t * kb : (t + 1) * kb],
                    up_ref[t * kb : (t + 1) * kb],
                    dense_ref[t, 0:kb],
                    dense_ref[t, kb : 2 * kb],
                ],
                axis=1,
            ),
            preferred_element_type=F32,
        )
        sums[h] = part if sums[h] is None else sums[h] + part
    both = jnp.where(second, sums[1], sums[0])
    both = both.reshape(rows // 8, 8, 4 * width)
    both = (both + pltpu.roll(both, 4, 1)).reshape(rows, 4 * width)
    picked = silu(both[:, 0:width]) * both[:, width : 2 * width]
    dense = silu(both[:, 2 * width : 3 * width]) * both[:, 3 * width :]
    hidden = jnp.concatenate(
        [jnp.where(is_dense, 0.0, picked), jnp.where(is_dense, dense, 0.0)], axis=1
    ).astype(BF16)

    def block(t):
        dense_down = jnp.concatenate(
            [
                dense_ref[t, 2 * kb : 2 * kb + width],
                dense_ref[t, 2 * kb + width : 2 * kb + 2 * width],
            ],
            axis=1,
        )
        down = jnp.concatenate([down_ref[:, t * kb : (t + 1) * kb], dense_down], axis=0)
        return jnp.dot(hidden, down, preferred_element_type=F32)

    for b in range(per_half):
        out_ref[:, b * kb : (b + 1) * kb] = jnp.where(
            second, block(per_half + b), block(b)
        ).astype(BF16)


def combine_kernel(rows_ref, weight_ref, dense_mask_ref, mix_ref, out_ref):
    blocks, seqs, width = out_ref.shape
    mix = jnp.concatenate([mix_ref[...], mix_ref[...]], axis=0)
    weight = weight_ref[...] + dense_mask_ref[...] * mix
    high = weight.astype(BF16)
    low = (weight - high.astype(F32)).astype(BF16)
    rows = rows_ref[...]
    total = jnp.dot(high, rows, preferred_element_type=F32) + jnp.dot(
        low, rows, preferred_element_type=F32
    )
    per_half = blocks // 2
    for t in range(blocks):
        h, b = divmod(t, per_half)
        out_ref[t] = total[h * seqs : (h + 1) * seqs, b * width : (b + 1) * width].astype(BF16)


def limits(mib):
    return pltpu.CompilerParams(vmem_limit_bytes=mib * MIB)


def exchange(array, axis):
    return lax.all_to_all(array, axis, 0, 0, tiled=True)


def body(
    tokens,
    norm_attn,
    w_query,
    w_key,
    w_value,
    w_forget,
    forget_bias,
    w_output,
    key_cache,
    value_cache,
    gate_cache,
    lengths,
    norm_ffn,
    route_group,
    route_slot,
    route_weight,
    expert_gate,
    expert_up,
    expert_down,
    dense_gate,
    dense_up,
    dense_down,
    mix_vector,
):
    seqs, model_width = tokens.shape
    ep_count = lax.axis_size(EP)
    tp_count = lax.axis_size("tp")
    tp_position = lax.axis_index("tp")
    width_local = model_width // tp_count
    half = model_width // 2
    head_width = key_cache.shape[2]
    cache_len = key_cache.shape[1]
    dense_rows = 2 * dense_gate.shape[0] + 2 * dense_down.shape[0]

    parts, dense_out = pl.pallas_call(
        attention_kernel,
        name="attention",
        out_shape=(
            jax.ShapeDtypeStruct((tp_count, seqs, model_width), BF16),
            jax.ShapeDtypeStruct((tp_count, dense_rows, head_width), BF16),
        ),
        in_specs=[VMEM] * 6 + [ANY] * 9,
        out_specs=(VMEM, VMEM),
        scratch_shapes=[
            pltpu.VMEM((3, model_width, head_width), BF16),
            pltpu.VMEM((head_width, model_width), BF16),
            pltpu.VMEM((seqs, cache_len, head_width), BF16),
            pltpu.VMEM((seqs, cache_len, head_width), BF16),
            pltpu.VMEM((dense_rows, head_width), BF16),
            pltpu.VMEM((2 * seqs, cache_len), F32),
            pltpu.VMEM((seqs, head_width), F32),
            pltpu.SemaphoreType.DMA((8,)),
            pltpu.SemaphoreType.DMA((seqs,)),
            pltpu.SemaphoreType.DMA((seqs,)),
        ],
        compiler_params=limits(24),
        cost_estimate=pl.CostEstimate(flops=10**9, bytes_accessed=12 * MIB, transcendentals=40000),
    )(
        tokens,
        norm_attn.reshape(1, -1),
        w_forget,
        forget_bias.reshape(1, -1),
        gate_cache,
        lengths.reshape(-1, 1),
        w_query,
        w_key,
        w_value,
        w_output,
        key_cache,
        value_cache,
        dense_gate,
        dense_up,
        dense_down,
    )
    parts = exchange(parts, "tp")
    dense_weights = exchange(dense_out, "tp")

    picks = route_slot.shape[1]
    ids = (route_group[:, None] * EXPERTS_PER_GROUP + route_slot).reshape(-1)
    order = jnp.arange(seqs * picks, dtype=jnp.int32)
    earlier = jnp.sum(
        ((ids[:, None] == ids[None, :]) & (order[None, :] < order[:, None])).astype(jnp.int32),
        axis=1,
    )
    place = (ids * 8 + earlier).reshape(seqs, picks)
    row = jnp.arange(ep_count * 8, dtype=jnp.int32)
    row_half = (row // 4) % 2
    row_slot = row % 4
    row_place = (row // 8) * 8 + row_slot
    token = jnp.arange(2 * seqs, dtype=jnp.int32) % seqs
    token_half = jnp.arange(2 * seqs, dtype=jnp.int32) // seqs
    same_half = token_half[:, None] == row_half[None, :]
    hits = [
        same_half
        & (row_slot < 2)[None, :]
        & (jnp.tile(place[:, k], 2)[:, None] == row_place[None, :])
        for k in range(picks)
    ]
    dense_hit = (
        same_half
        & (row_slot >= 2)[None, :]
        & (token[:, None] == (tp_position * 2 + row_slot - 2)[None, :])
    )
    pick_weight = sum(
        jnp.where(hits[k], jnp.tile(route_weight[:, k], 2)[:, None], 0.0) for k in range(picks)
    )
    dense_mask = dense_hit.astype(F32)
    select = (functools.reduce(jnp.logical_or, hits) | dense_hit).astype(BF16).T

    outgoing, residual, mix_gate = pl.pallas_call(
        dispatch_kernel,
        name="dispatch",
        out_shape=(
            jax.ShapeDtypeStruct((ep_count * 8, half), BF16),
            jax.ShapeDtypeStruct((seqs, model_width), F32),
            jax.ShapeDtypeStruct((seqs, 1), F32),
        ),
        in_specs=[VMEM] * 5,
        out_specs=(VMEM, VMEM, VMEM),
        compiler_params=limits(8),
    )(parts, tokens, norm_ffn.reshape(1, -1), select, mix_vector.reshape(1, -1))
    arrived = exchange(outgoing.reshape(ep_count, 8, half), EP).reshape(ep_count * 8, half)
    results = pl.pallas_call(
        expert_kernel,
        name="experts",
        out_shape=jax.ShapeDtypeStruct((ep_count * 8, half), BF16),
        in_specs=[VMEM] * 5,
        out_specs=VMEM,
        compiler_params=limits(16),
    )(arrived, expert_gate[0], expert_up[0], expert_down[0], dense_weights)
    returned = exchange(results.reshape(ep_count, 8, half), EP).reshape(ep_count * 8, half)
    sums = pl.pallas_call(
        combine_kernel,
        name="combine",
        out_shape=jax.ShapeDtypeStruct((tp_count, seqs, width_local), BF16),
        in_specs=[VMEM] * 4,
        out_specs=VMEM,
        compiler_params=limits(8),
    )(returned, pick_weight, dense_mask, mix_gate)
    sums = exchange(sums, "tp")
    residual_mine = lax.dynamic_slice_in_dim(residual, tp_position * width_local, width_local, 1)
    return (residual_mine + jnp.sum(sums.astype(F32), axis=0)).astype(BF16)


def solution(mesh):
    split = Mesh(mesh.devices.reshape(8, 4, mesh.shape["tp"]), ("ep_0", "ep_1", "tp"))
    return jax.shard_map(
        body,
        mesh=split,
        in_specs=(
            P(EP, None),
            P(),
            P(None, "tp"),
            P(None, "tp"),
            P(None, "tp"),
            P(None, "tp"),
            P("tp"),
            P("tp", None),
            P(EP, None, "tp"),
            P(EP, None, "tp"),
            P(EP, "tp", None),
            P(EP),
            P(),
            P(EP),
            P(EP, None),
            P(EP, None),
            P(EP, None, "tp"),
            P(EP, None, "tp"),
            P(EP, "tp", None),
            P("tp", EP),
            P("tp", EP),
            P(EP, "tp"),
            P(),
        ),
        out_specs=P(EP, "tp"),
        check_vma=False,
    )
```

time: 154 us -> 132 us (0.86)
  matrix products: 16.3 us -> 0 us
  between operations: 13.7 us -> 0.2 us
  Pallas kernels: 0 us -> 11.8 us
  starting transfers between devices: 25.6 us -> 17.5 us
  blocking collectives: 34.9 us -> 41.4 us
  other arithmetic: 4.93 us -> 1.39 us
  local copies, waits for them, and re-layouts: 18.2 us -> 19.9 us
    all_to_all x1 -> x2, blocking collectives: 23.5 us -> 41.4 us  [exchange(): return lax.all_to_all(array, axis, 0, 0, tiled=True)]
    dot_general x15 -> x0, matrix products: 16.3 us -> none  [the longest x1 3.43 us: attend(): jnp.einsum('shj,sjhd->shd', weights.astype(jnp.bfloat16), value_rows, pre...]
    pallas_call x0 -> x4, Pallas kernels: none -> 11.8 us  [the longest x1 8.46 us: body(): pl.pallas_call(attention_kernel, name='attention', out_shape=(jax.ShapeDt...]
    all_gather x1 -> x0, blocking collectives: 11.4 us -> none  [whole_of(): array = lax.all_gather(array, axis, axis=dim, tiled=True)]
    all_to_all x4 -> x3, starting transfers between devices: 25.6 us -> 17.5 us  [exchange(): return lax.all_to_all(array, axis, 0, 0, tiled=True)]
    unnamed x39 -> x48, local copies, waits for them, and re-layouts: 13.2 us -> 18.5 us
    broadcast_in_dim x3 -> x2, local copies, waits for them, and re-layouts: 2.47 us -> 0.17 us  [body(): jnp.where(hits[k], jnp.tile(route_weight[:, k], 2)[:, None], 0.0)]
    reduce_sum x10 -> x2, other arithmetic: 2.31 us -> 0.19 us  [the longest x1 0.18 us: body(): jnp.sum(((ids[:, None] == ids[None, :]) & (order[None, :] < order[:, None...]
  transfers between devices with their start and end apart: 6 -> 3, of which waited for: 3 -> 3; matrix products, arithmetic and copies ran while one was open for 23% -> 1% of each run, Pallas kernels for 0% -> 0%
where the time goes in v1:
time: 132 us; the launch traced here: 131 us
  blocking collectives  41.4 us (31%)
  waiting for transfers between devices  38.6 us (29%)
  local copies, waits for them, and re-layouts  19.9 us (15%)
  starting transfers between devices  17.5 us (13%)
  Pallas kernels  11.8 us (9%)
  other arithmetic  1.39 us (1%)
    all_to_all x2, blocking collectives, exchange(): return lax.all_to_all(array, axis, 0, 0, tiled=True)  41.4 us
    all_to_all x3, waiting for transfers between devices, exchange(): return lax.all_to_all(array, axis, 0, 0, tiled=True)  38.6 us
    unnamed x48, local copies, waits for them, and re-layouts  18.5 us
    all_to_all x3, starting transfers between devices, exchange(): return lax.all_to_all(array, axis, 0, 0, tiled=True)  17.5 us
    pallas_call x1, Pallas kernels, body(): pl.pallas_call(attention_kernel, name='attention', out_shape=(jax.ShapeDt...  8.46 us
  transfers between devices with their start and end apart: 3, of which 3 were waited for; matrix products, arithmetic and copies ran while one was open for 1% of the time, Pallas kernels for 0%

profile of v1, /device:TPU:1, one launch (start us, length us, event | category | flops | bytes accessed | tf_op | source)
XLA Modules:
  0.0 130.8 jit_solution(13478545030352400555)
XLA Ops:
  0.0 0.7 copy.34.length_ref
  0.7 1.0 copy.33.forget_ref
  1.8 2.2 %copy-done = bf16[16,1024,128]{2,1,0:T(8,128)(2,1)S(1)} copy-done((bf16[16,1024,128]{2,1,0:T(8,128)(2,1)S(1)}, bf16[16,1024,128]{2,1,0:T(8,128)(2,1)}, u32[]{:S(2)}) %copy-start) | copy-done | bytes 4194328
  3.9 2.2 %copy-done.1 = bf16[16,1024,128]{2,1,0:T(8,128)(2,1)S(1)} copy-done((bf16[16,1024,128]{2,1,0:T(8,128)(2,1)S(1)}, bf16[16,1024,128]{2,1,0:T(8,128)(2,1)}, u32[]{:S(2)}) %copy-start.1) | copy-done | bytes 4194328
  6.1 1.0 copy-done.3
  7.2 1.0 copy-done.4
  8.2 1.0 copy-done.5
  9.3 1.0 copy-done.6
  10.3 0.8 copy-done.10
  11.1 0.9 copy-done.12
  12.0 0.8 copy-done.13
  12.9 0.8 copy-done.14
  13.7 0.8 copy-done.15
  14.6 0.7 copy-done.18
  15.3 0.7 copy-done.19
  15.9 8.5 %attention.1 = (bf16[8,16,2048]{2,1,0:T(8,128)(2,1)S(1)}, bf16[8,768,128]{2,1,0:T(8,128)(2,1)S(1)}) custom-call(bf16[16,2048]{1,0:T(8,128)(2,1)S(1)} %copy-done.10, f32[1,2048]{1,0:T(1,128)S(1)} %bitcast.24, bf16[2048,2]{1,0:T(8,128)(2,1)S(1)} %copy.33.forget_ref, f32[1,2]{1,0:T(1,128)S(1)} %bitcast.25, f32[16,2,1024]{2,1,0:T(2,128)S(1)} %copy-done.12, ...), custom_call_target="tpu_custom_call" | custom-call | flops 1000000000 | bytes 12582912 | tf_op jit(solution)/shard_map/attention/pallas_call | solution.py:291
  24.4 1.1 copy-done.2
  25.6 15.2 %all_to_all.25.parts_ref = bf16[8,16,2048]{2,1,0:T(8,128)(2,1)S(1)} all-to-all(bf16[8,16,2048]{2,1,0:T(8,128)(2,1)S(1)} %get-tuple-element.10), channel_id=1, replica_groups=mesh['ep_0'=8,'ep_1'=4,'tp'=8] {'tp'}, dimensions={0} | all-to-all | bytes 1048576 | tf_op jit(solution)/shard_map/all_to_all | solution.py:253
  40.8 4.5 %all-to-all-start.2 = ((bf16[8,768,128]{2,1,0:T(8,128)(2,1)}), bf16[8,768,128]{2,1,0:T(8,128)(2,1)S(1)}, u32[]{:S(2)}, u32[]{:S(2)}) async-start(bf16[8,768,128]{2,1,0:T(8,128)(2,1)} %copy-done.2), calls=%async_computation.2 | async-start | bytes 3145728 | tf_op jit(solution)/shard_map/all_to_all | solution.py:253
  46.3 0.2 fusion.4.select_ref
  46.6 0.4 dispatch.1
  47.1 18.9 %all-to-all-done.2.dense_ref = bf16[8,768,128]{2,1,0:T(8,128)(2,1)S(1)} async-done(((bf16[8,768,128]{2,1,0:T(8,128)(2,1)}), bf16[8,768,128]{2,1,0:T(8,128)(2,1)S(1)}, u32[]{:S(2)}, u32[]{:S(2)}) %all-to-all-start.2) | async-done | bytes 1572896 | tf_op jit(solution)/shard_map/all_to_all | solution.py:253
  65.9 26.2 %all_to_all.26 = bf16[32,8,1024]{2,1,0:T(8,128)(2,1)S(1)} all-to-all(bf16[32,8,1024]{2,1,0:T(8,128)(2,1)S(1)} %bitcast.18), channel_id=1, replica_groups=mesh['ep_0'=8,'ep_1'=4,'tp'=8] {'ep_0','ep_1'}, dimensions={0} | all-to-all | bytes 1048576 | tf_op jit(solution)/shard_map/all_to_all | solution.py:253
  92.1 1.0 copy-done.8
  93.2 1.0 copy-done.9
  94.2 1.9 %experts.1 = bf16[256,1024]{1,0:T(8,128)(2,1)} custom-call(bf16[256,1024]{1,0:T(8,128)(2,1)S(1)} %bitcast.17, bf16[2048,128]{1,0:T(8,128)(2,1)S(1)} %bitcast.19, bf16[2048,128]{1,0:T(8,128)(2,1)S(1)} %bitcast.20, bf16[128,2048]{1,0:T(8,128)(2,1)S(1)} %bitcast.21, bf16[8,768,128]{2,1,0:T(8,128)(2,1)S(1)} %all-to-all-done.2.dense_ref), custom_call_target="tpu_custom_call" | custom-call | tf_op jit(solution)/shard_map/experts/pallas_call | solution.py:379
  96.1 6.2 %all-to-all-start.3 = ((bf16[32,8,1024]{2,1,0:T(8,128)(2,1)}), bf16[32,8,1024]{2,1,0:T(8,128)(2,1)S(1)}, u32[]{:S(2)}, u32[]{:S(2)}) async-start(bf16[32,8,1024]{2,1,0:T(8,128)(2,1)} %bitcast.10), calls=%async_computation.3 | async-start | bytes 1048576 | tf_op jit(solution)/shard_map/all_to_all | solution.py:253
  102.7 14.8 %all-to-all-done.3 = bf16[32,8,1024]{2,1,0:T(8,128)(2,1)S(1)} async-done(((bf16[32,8,1024]{2,1,0:T(8,128)(2,1)}), bf16[32,8,1024]{2,1,0:T(8,128)(2,1)S(1)}, u32[]{:S(2)}, u32[]{:S(2)}) %all-to-all-start.3) | async-done | bytes 524320 | tf_op jit(solution)/shard_map/all_to_all | solution.py:253
  117.5 1.0 combine.1
  118.5 6.8 %all-to-all-start.4 = ((bf16[8,16,256]{2,1,0:T(8,128)(2,1)}), bf16[8,16,256]{2,1,0:T(8,128)(2,1)S(1)}, u32[]{:S(2)}, u32[]{:S(2)}) async-start(bf16[8,16,256]{2,1,0:T(8,128)(2,1)} %combine.1), calls=%async_computation.4 | async-start | bytes 131072 | tf_op jit(solution)/shard_map/all_to_all | solution.py:253
  125.3 4.9 %all-to-all-done.4 = bf16[8,16,256]{2,1,0:T(8,128)(2,1)S(1)} async-done(((bf16[8,16,256]{2,1,0:T(8,128)(2,1)}), bf16[8,16,256]{2,1,0:T(8,128)(2,1)S(1)}, u32[]{:S(2)}, u32[]{:S(2)}) %all-to-all-start.4) | async-done | bytes 65568 | tf_op jit(solution)/shard_map/all_to_all | solution.py:253
  130.2 0.6 add_convert_fusion
  (54 shorter events, 1.4 us)
Async XLA Ops:
  1.7 2.2 %copy-start = (bf16[16,1024,128]{2,1,0:T(8,128)(2,1)S(1)}, bf16[16,1024,128]{2,1,0:T(8,128)(2,1)}, u32[]{:S(2)}) copy-start(bf16[16,1024,128]{2,1,0:T(8,128)(2,1)} %key_hbm.1) | copy-start | bytes 12582916
  3.9 2.2 %copy-start.1 = (bf16[16,1024,128]{2,1,0:T(8,128)(2,1)S(1)}, bf16[16,1024,128]{2,1,0:T(8,128)(2,1)}, u32[]{:S(2)}) copy-start(bf16[16,1024,128]{2,1,0:T(8,128)(2,1)} %value_hbm.1) | copy-start | bytes 12582916
  6.1 1.0 copy-start.3
  7.2 1.0 copy-start.4
  8.2 1.0 copy-start.5
  9.3 1.0 copy-start.6
  10.3 0.8 copy-start.10
  11.1 0.9 copy-start.12
  12.0 0.8 copy-start.13
  12.9 0.8 copy-start.14
  13.7 0.8 copy-start.15
  14.6 0.7 copy-start.18
  15.3 0.7 copy-start.19
  24.4 1.2 copy-start.2
  25.5 19.8 %copy-start.22 = (s32[16]{0:T(128)S(1)}, s32[16]{0:T(128)}, u32[]{:S(2)}) copy-start(s32[16]{0:T(128)} %param.36) | copy-start | bytes 196
  25.5 19.8 %copy-start.20 = (s32[16,2]{0,1:T(2,128)S(1)}, s32[16,2]{0,1:T(2,128)}, u32[]{:S(2)}) copy-start(s32[16,2]{0,1:T(2,128)} %param.37) | copy-start | bytes 388
  25.5 21.0 %copy-start.11 = (bf16[16,2048]{1,0:T(8,128)(2,1)S(1)}, bf16[16,2048]{1,0:T(8,128)(2,1)}, u32[]{:S(2)}) copy-start(bf16[16,2048]{1,0:T(8,128)(2,1)} %tokens_ref.3) | copy-start | bytes 196612
  25.5 21.0 %copy-start.16 = (f32[2048]{0:T(1024)S(1)}, f32[2048]{0:T(1024)}, u32[]{:S(2)}) copy-start(f32[2048]{0:T(1024)} %param.35) | copy-start | bytes 24580
  25.6 21.0 %copy-start.17 = (f32[2048]{0:T(1024)S(1)}, f32[2048]{0:T(1024)}, u32[]{:S(2)}) copy-start(f32[2048]{0:T(1024)} %param.45) | copy-start | bytes 24580
  25.6 66.6 %copy-start.7 = (bf16[1,2048,128]{2,1,0:T(8,128)(2,1)S(1)}, bf16[1,2048,128]{2,1,0:T(8,128)(2,1)}, u32[]{:S(2)}) copy-start(bf16[1,2048,128]{2,1,0:T(8,128)(2,1)} %param.39) | copy-start | bytes 1572868
  40.8 25.1 %all-to-all-start.2 = ((bf16[8,768,128]{2,1,0:T(8,128)(2,1)}), bf16[8,768,128]{2,1,0:T(8,128)(2,1)S(1)}, u32[]{:S(2)}, u32[]{:S(2)}) async-start(bf16[8,768,128]{2,1,0:T(8,128)(2,1)} %copy-done.2), calls=%async_computation.2 | async-start | bytes 3145728 | tf_op jit(solution)/shard_map/all_to_all | solution.py:253
  45.3 57.0 %copy-start.21 = (f32[16,2]{0,1:T(2,128)S(1)}, f32[16,2]{0,1:T(2,128)}, u32[]{:S(2)}) copy-start(f32[16,2]{0,1:T(2,128)} %param.38) | copy-start | bytes 388
  92.1 1.0 copy-start.8
  93.2 1.0 copy-start.9
  96.1 21.4 %all-to-all-start.3 = ((bf16[32,8,1024]{2,1,0:T(8,128)(2,1)}), bf16[32,8,1024]{2,1,0:T(8,128)(2,1)S(1)}, u32[]{:S(2)}, u32[]{:S(2)}) async-start(bf16[32,8,1024]{2,1,0:T(8,128)(2,1)} %bitcast.10), calls=%async_computation.3 | async-start | bytes 1048576 | tf_op jit(solution)/shard_map/all_to_all | solution.py:253
  118.5 11.7 %all-to-all-start.4 = ((bf16[8,16,256]{2,1,0:T(8,128)(2,1)}), bf16[8,16,256]{2,1,0:T(8,128)(2,1)S(1)}, u32[]{:S(2)}, u32[]{:S(2)}) async-start(bf16[8,16,256]{2,1,0:T(8,128)(2,1)} %combine.1), calls=%async_computation.4 | async-start | bytes 131072 | tf_op jit(solution)/shard_map/all_to_all | solution.py:253

commit v2 on v1

v2 whole, which is shorter than its diff:
```python
import functools

import jax
import jax.numpy as jnp
from jax import lax
from jax.experimental import pallas as pl
from jax.experimental.pallas import tpu as pltpu
from jax.sharding import Mesh
from jax.sharding import PartitionSpec as P

EXPERTS_PER_GROUP = 8
EP = ("ep_0", "ep_1")
EPS = 1e-06
F32 = jnp.float32
BF16 = jnp.bfloat16
NT = (((1,), (1,)), ((), ()))
VMEM = pl.BlockSpec(memory_space=pltpu.VMEM)
SMEM = pl.BlockSpec(memory_space=pltpu.SMEM)
ANY = pl.BlockSpec(memory_space=pl.ANY)
MIB = 1 << 20


def rms_scale(rows, gain):
    rows = rows.astype(F32)
    return rows * lax.rsqrt(jnp.mean(rows * rows, axis=-1, keepdims=True) + EPS) * gain


def silu(v):
    return v * jax.nn.sigmoid(v)


def stacked(pair):
    return jnp.concatenate([pair[:, 0:1], pair[:, 1:2]], axis=0)


def attention_kernel(
    tokens_hbm,
    gain_hbm,
    forget_hbm,
    bias_hbm,
    gate_hbm,
    length_hbm,
    wq_hbm,
    wk_hbm,
    wv_hbm,
    wo_hbm,
    key_hbm,
    value_hbm,
    parts_ref,
    tokens_ref,
    gain_ref,
    forget_ref,
    bias_ref,
    gate_ref,
    length_ref,
    wqkv,
    wo,
    keys,
    values,
    scores,
    weighted,
    small_sems,
    w_sems,
    key_sems,
    value_sems,
):
    seqs, cache_len, width = keys.shape
    heads = 2
    half = width // heads
    rows = heads * seqs
    scale = half ** (-0.5)
    group = 4
    groups = seqs // group
    small = [
        pltpu.make_async_copy(src, dst, small_sems.at[i])
        for i, (src, dst) in enumerate(
            (
                (tokens_hbm, tokens_ref),
                (gain_hbm, gain_ref),
                (forget_hbm, forget_ref),
                (bias_hbm, bias_ref),
                (length_hbm, length_ref),
                (gate_hbm, gate_ref),
            )
        )
    ]
    weight_copies = [
        pltpu.make_async_copy(src, wqkv.at[i], w_sems.at[i])
        for i, src in enumerate((wq_hbm, wk_hbm, wv_hbm))
    ]
    output_copy = pltpu.make_async_copy(wo_hbm, wo, w_sems.at[3])
    part = lambda g: pl.ds(g * group, group)
    key_copies = [
        pltpu.make_async_copy(key_hbm.at[part(g)], keys.at[part(g)], key_sems.at[g])
        for g in range(groups)
    ]
    value_copies = [
        pltpu.make_async_copy(value_hbm.at[part(g)], values.at[part(g)], value_sems.at[g])
        for g in range(groups)
    ]
    for copy in small + weight_copies + key_copies + value_copies + [output_copy]:
        copy.start()
    for copy in small:
        copy.wait()
    normed = rms_scale(tokens_ref[...], gain_ref[...]).astype(BF16)
    forget_logit = (
        lax.dot_general(normed, forget_ref[...], NT, preferred_element_type=F32) + bias_ref[...]
    )
    forget_log = stacked(jax.nn.log_sigmoid(forget_logit))
    same = lax.broadcasted_iota(jnp.int32, (seqs, seqs), 0) == lax.broadcasted_iota(
        jnp.int32, (seqs, seqs), 1
    )
    length = jnp.sum(
        jnp.where(same, length_ref[...].astype(F32), 0.0), axis=1, keepdims=True
    ).astype(jnp.int32)
    length = jnp.concatenate([length, length], axis=0)
    gate = jnp.concatenate([gate_ref[:, 0, :], gate_ref[:, 1, :]], axis=0)
    entry = lax.broadcasted_iota(jnp.int32, (rows, cache_len), 1)
    last_gate = jnp.sum(jnp.where(entry == length - 1, gate, 0.0), axis=1, keepdims=True)
    current = last_gate + forget_log
    for copy in weight_copies:
        copy.wait()
    query, key_new, value_new = [
        jnp.dot(normed, wqkv[i], preferred_element_type=F32).astype(BF16).astype(F32)
        for i in range(3)
    ]
    lane = lax.broadcasted_iota(jnp.int32, (1, width), 1)
    first_head = lane < half
    own = query * key_new
    own_score = scale * jnp.concatenate(
        [
            jnp.sum(jnp.where(first_head, own, 0.0), axis=1, keepdims=True),
            jnp.sum(jnp.where(first_head, 0.0, own), axis=1, keepdims=True),
        ],
        axis=0,
    )
    row8 = lax.broadcasted_iota(jnp.int32, (8, width), 0)
    lane8 = lax.broadcasted_iota(jnp.int32, (8, width), 1)
    head_mask = (row8 < heads) & ((lane8 < half) == (row8 == 0))
    for g in range(groups):
        key_copies[g].wait()
        for s in range(g * group, (g + 1) * group):
            masked = jnp.where(head_mask, query[s : s + 1], 0.0).astype(BF16)
            result = lax.dot_general(masked, keys[s], NT, preferred_element_type=F32)
            scores[s : s + 1] = result[0:1]
            scores[seqs + s : seqs + s + 1] = result[1:2]
    score = scores[...] * scale + (current - gate)
    score = jnp.where(entry < length, score, -jnp.inf)
    peak = jnp.maximum(jnp.max(score, axis=1, keepdims=True), own_score)
    weights = jnp.exp(score - peak)
    own_weight = jnp.exp(own_score - peak)
    denominator = jnp.sum(weights, axis=1, keepdims=True) + own_weight
    scores[...] = weights
    for g in range(groups):
        value_copies[g].wait()
        for s in range(g * group, (g + 1) * group):
            pair = jnp.concatenate(
                [
                    scores[s : s + 1],
                    scores[seqs + s : seqs + s + 1],
                    jnp.zeros((6, cache_len), F32),
                ],
                axis=0,
            ).astype(BF16)
            result = jnp.dot(pair, values[s], preferred_element_type=F32)
            weighted[s : s + 1] = jnp.where(first_head, result[0:1], result[1:2])
    output_copy.wait()
    own_weight = own_weight.astype(BF16).astype(F32)
    own_weight = jnp.where(first_head, own_weight[:seqs], own_weight[seqs:])
    denominator = jnp.where(first_head, denominator[:seqs], denominator[seqs:])
    attended = ((weighted[...] + own_weight * value_new) / denominator).astype(BF16)
    head_part = jnp.dot(attended, wo[...], preferred_element_type=F32).astype(BF16)
    for i in range(parts_ref.shape[0]):
        parts_ref[i] = head_part


def dispatch_kernel(
    position_ref,
    parts_ref,
    tokens_ref,
    gain_ref,
    select_ref,
    mix_ref,
    pick_ref,
    dense_mask_ref,
    out_ref,
    residual_ref,
    high_ref,
    low_ref,
    scratch,
):
    half = out_ref.shape[1]
    width = residual_ref.shape[1]
    attn = parts_ref[0].astype(F32)
    for i in range(1, parts_ref.shape[0]):
        attn = attn + parts_ref[i].astype(F32)
    residual = tokens_ref[...].astype(F32) + attn
    scratch[...] = residual
    normed = rms_scale(residual, gain_ref[...]).astype(BF16)
    both = jnp.concatenate([normed[:, :half], normed[:, half:]], axis=0)
    out_ref[...] = jnp.dot(select_ref[...], both, preferred_element_type=F32).astype(BF16)
    mix = jax.nn.sigmoid(jnp.sum(normed.astype(F32) * mix_ref[...], axis=1, keepdims=True))
    weight = pick_ref[...] + dense_mask_ref[...] * jnp.concatenate([mix, mix], axis=0)
    high = weight.astype(BF16)
    high_ref[...] = high
    low_ref[...] = (weight - high.astype(F32)).astype(BF16)
    mine = pl.ds(pl.multiple_of(position_ref[0] * width, width), width)
    residual_ref[...] = scratch[:, mine]


def row_kinds(rows):
    row = lax.broadcasted_iota(jnp.int32, (rows, 1), 0)
    return lax.rem(row, 8) >= 4, lax.rem(row, 4) >= 2


def whole_rows(both):
    rows, width = both.shape
    both = both.reshape(rows // 8, 8, width)
    return (both + pltpu.roll(both, 4, 1)).reshape(rows, width)


def picked_kernel(rows_ref, gate_ref, up_ref, down_ref, out_ref):
    rows, half = rows_ref.shape
    width = gate_ref.shape[1]
    second, _ = row_kinds(rows)
    sums = []
    for h in range(2):
        weights = jnp.concatenate(
            [gate_ref[h * half : (h + 1) * half], up_ref[h * half : (h + 1) * half]], axis=1
        )
        sums.append(jnp.dot(rows_ref[...], weights, preferred_element_type=F32))
    both = whole_rows(jnp.where(second, sums[1], sums[0]))
    hidden = (silu(both[:, :width]) * both[:, width:]).astype(BF16)
    results = [
        jnp.dot(hidden, down_ref[:, h * half : (h + 1) * half], preferred_element_type=F32)
        for h in range(2)
    ]
    out_ref[...] = jnp.where(second, results[1], results[0]).astype(BF16)


def dense_kernel(position_ref, rows_ref, picked_ref, *refs):
    out_ref = refs[-1]
    dense_refs = refs[:-1]
    rows, half = rows_ref.shape
    blocks = len(dense_refs)
    width = dense_refs[0].shape[1]
    per_half = blocks // 2
    kb = half // per_half
    position = position_ref[0]
    second, is_dense = row_kinds(rows)
    places = []
    for k in range(blocks):
        t = lax.rem(position - k + blocks, blocks)
        b = lax.rem(t, per_half)
        places.append((pl.ds(pl.multiple_of(b * kb, kb), kb), second == (t >= per_half)))
    both = None
    for (inner, mine), dense_ref in zip(places, dense_refs):
        weights = jnp.concatenate([dense_ref[0:kb], dense_ref[kb : 2 * kb]], axis=1)
        part = jnp.dot(rows_ref[:, inner], weights, preferred_element_type=F32)
        part = jnp.where(mine, part, 0.0)
        both = part if both is None else both + part
    both = whole_rows(both)
    hidden = (silu(both[:, :width]) * both[:, width:]).astype(BF16)
    out_ref[...] = picked_ref[...]
    for (inner, mine), dense_ref in zip(places, dense_refs):
        down = jnp.concatenate(
            [
                dense_ref[2 * kb : 2 * kb + width],
                dense_ref[2 * kb + width : 2 * kb + 2 * width],
            ],
            axis=1,
        )
        result = jnp.dot(hidden, down, preferred_element_type=F32).astype(BF16)
        out_ref[:, inner] = jnp.where(mine & is_dense, result, out_ref[:, inner])


def combine_kernel(rows_ref, high_ref, low_ref, out_ref):
    blocks, seqs, width = out_ref.shape
    rows = rows_ref[...]
    total = jnp.dot(high_ref[...], rows, preferred_element_type=F32) + jnp.dot(
        low_ref[...], rows, preferred_element_type=F32
    )
    per_half = blocks // 2
    for t in range(blocks):
        h, b = divmod(t, per_half)
        out_ref[t] = total[h * seqs : (h + 1) * seqs, b * width : (b + 1) * width].astype(BF16)


def limits(mib):
    return pltpu.CompilerParams(vmem_limit_bytes=mib * MIB)


def exchange(array, axis):
    return lax.all_to_all(array, axis, 0, 0, tiled=True)


def body(
    tokens,
    norm_attn,
    w_query,
    w_key,
    w_value,
    w_forget,
    forget_bias,
    w_output,
    key_cache,
    value_cache,
    gate_cache,
    lengths,
    norm_ffn,
    route_group,
    route_slot,
    route_weight,
    expert_gate,
    expert_up,
    expert_down,
    dense_gate,
    dense_up,
    dense_down,
    mix_vector,
):
    seqs, model_width = tokens.shape
    ep_count = lax.axis_size(EP)
    tp_count = lax.axis_size("tp")
    tp_position = lax.axis_index("tp")
    width_local = model_width // tp_count
    half = model_width // 2
    head_width = key_cache.shape[2]
    cache_len = key_cache.shape[1]

    own_dense = jnp.concatenate(
        [dense_gate, dense_up, dense_down[:, :head_width], dense_down[:, head_width:]], axis=0
    )
    dense_weights = [own_dense]
    for k in range(1, tp_count):
        dense_weights.append(
            lax.ppermute(own_dense, "tp", [(i, (i + k) % tp_count) for i in range(tp_count)])
        )
    parts = pl.pallas_call(
        attention_kernel,
        name="attention",
        out_shape=jax.ShapeDtypeStruct((tp_count, seqs, model_width), BF16),
        in_specs=[ANY] * 12,
        out_specs=VMEM,
        scratch_shapes=[
            pltpu.VMEM((seqs, model_width), BF16),
            pltpu.VMEM((1, model_width), F32),
            pltpu.VMEM((2, model_width), BF16),
            pltpu.VMEM((1, 2), F32),
            pltpu.VMEM((seqs, 2, cache_len), F32),
            pltpu.VMEM((1, seqs), jnp.int32),
            pltpu.VMEM((3, model_width, head_width), BF16),
            pltpu.VMEM((head_width, model_width), BF16),
            pltpu.VMEM((seqs, cache_len, head_width), BF16),
            pltpu.VMEM((seqs, cache_len, head_width), BF16),
            pltpu.VMEM((2 * seqs, cache_len), F32),
            pltpu.VMEM((seqs, head_width), F32),
            pltpu.SemaphoreType.DMA((6,)),
            pltpu.SemaphoreType.DMA((4,)),
            pltpu.SemaphoreType.DMA((4,)),
            pltpu.SemaphoreType.DMA((4,)),
        ],
        compiler_params=limits(60),
        cost_estimate=pl.CostEstimate(flops=10**9, bytes_accessed=12 * MIB, transcendentals=40000),
    )(
        tokens,
        norm_attn.reshape(1, -1),
        w_forget.T,
        forget_bias.reshape(1, -1),
        gate_cache,
        lengths.reshape(1, -1),
        w_query,
        w_key,
        w_value,
        w_output,
        key_cache,
        value_cache,
    )
    parts = exchange(parts, "tp")

    picks = route_slot.shape[1]
    ids = (route_group[:, None] * EXPERTS_PER_GROUP + route_slot).reshape(-1)
    order = jnp.arange(seqs * picks, dtype=jnp.int32)
    earlier = jnp.sum(
        ((ids[:, None] == ids[None, :]) & (order[None, :] < order[:, None])).astype(jnp.int32),
        axis=1,
    )
    place = (ids * 8 + earlier).reshape(seqs, picks)
    row = jnp.arange(ep_count * 8, dtype=jnp.int32)
    row_half = (row // 4) % 2
    row_slot = row % 4
    row_place = (row // 8) * 8 + row_slot
    token = jnp.arange(2 * seqs, dtype=jnp.int32) % seqs
    token_half = jnp.arange(2 * seqs, dtype=jnp.int32) // seqs
    same_half = token_half[:, None] == row_half[None, :]
    hits = [
        same_half
        & (row_slot < 2)[None, :]
        & (jnp.tile(place[:, k], 2)[:, None] == row_place[None, :])
        for k in range(picks)
    ]
    dense_hit = (
        same_half
        & (row_slot >= 2)[None, :]
        & (token[:, None] == (tp_position * 2 + row_slot - 2)[None, :])
    )
    pick_weight = sum(
        jnp.where(hits[k], jnp.tile(route_weight[:, k], 2)[:, None], 0.0) for k in range(picks)
    )
    dense_mask = dense_hit.astype(F32)
    select = (functools.reduce(jnp.logical_or, hits) | dense_hit).astype(BF16).T

    position = tp_position.reshape(1)
    dispatch = pl.pallas_call(
        dispatch_kernel,
        name="dispatch",
        out_shape=(
            jax.ShapeDtypeStruct((ep_count * 8, half), BF16),
            jax.ShapeDtypeStruct((seqs, width_local), F32),
            jax.ShapeDtypeStruct((2 * seqs, ep_count * 8), BF16),
            jax.ShapeDtypeStruct((2 * seqs, ep_count * 8), BF16),
        ),
        in_specs=[SMEM] + [VMEM] * 7,
        out_specs=(VMEM, VMEM, VMEM, VMEM),
        scratch_shapes=[pltpu.VMEM((seqs, model_width), F32)],
        compiler_params=limits(8),
    )
    outgoing, residual, high, low = dispatch(
        position,
        parts,
        tokens,
        norm_ffn.reshape(1, -1),
        select,
        mix_vector.reshape(1, -1),
        pick_weight,
        dense_mask,
    )
    arrived = exchange(outgoing.reshape(ep_count, 8, half), EP).reshape(ep_count * 8, half)
    results = pl.pallas_call(
        picked_kernel,
        name="picked",
        out_shape=jax.ShapeDtypeStruct((ep_count * 8, half), BF16),
        in_specs=[VMEM] * 4,
        out_specs=VMEM,
        compiler_params=limits(8),
    )(arrived, expert_gate[0], expert_up[0], expert_down[0])
    results = pl.pallas_call(
        dense_kernel,
        name="dense",
        out_shape=jax.ShapeDtypeStruct((ep_count * 8, half), BF16),
        in_specs=[SMEM] + [VMEM] * (2 + tp_count),
        out_specs=VMEM,
        compiler_params=limits(8),
    )(position, arrived, results, *dense_weights)
    returned = exchange(results.reshape(ep_count, 8, half), EP).reshape(ep_count * 8, half)
    sums = pl.pallas_call(
        combine_kernel,
        name="combine",
        out_shape=jax.ShapeDtypeStruct((tp_count, seqs, width_local), BF16),
        in_specs=[VMEM] * 3,
        out_specs=VMEM,
        compiler_params=limits(8),
    )(returned, high, low)
    sums = exchange(sums, "tp")
    return (residual + jnp.sum(sums.astype(F32), axis=0)).astype(BF16)


def solution(mesh):
    split = Mesh(mesh.devices.reshape(8, 4, mesh.shape["tp"]), ("ep_0", "ep_1", "tp"))
    return jax.shard_map(
        body,
        mesh=split,
        in_specs=(
            P(EP, None),
            P(),
            P(None, "tp"),
            P(None, "tp"),
            P(None, "tp"),
            P(None, "tp"),
            P("tp"),
            P("tp", None),
            P(EP, None, "tp"),
            P(EP, None, "tp"),
            P(EP, "tp", None),
            P(EP),
            P(),
            P(EP),
            P(EP, None),
            P(EP, None),
            P(EP, None, "tp"),
            P(EP, None, "tp"),
            P(EP, "tp", None),
            P("tp", EP),
            P("tp", EP),
            P(EP, "tp"),
            P(),
        ),
        out_specs=P(EP, "tp"),
        check_vma=False,
    )
```

time: 132 us -> 96.8 us (0.73)
  waiting for transfers between devices: 38.6 us -> 17.7 us
  local copies, waits for them, and re-layouts: 19.9 us -> 0.84 us
  starting transfers between devices: 17.5 us -> 27.5 us
  blocking collectives: 41.4 us -> 36.1 us
    all_to_all x3 -> x2, waiting for transfers between devices: 38.6 us -> 11.4 us  [exchange(): return lax.all_to_all(array, axis, 0, 0, tiled=True)]
    unnamed x48 -> x25, local copies, waits for them, and re-layouts: 18.5 us -> 0.13 us
    ppermute x0 -> x7, starting transfers between devices: none -> 10.5 us  [body(): lax.ppermute(own_dense, 'tp', [(i, (i + k) % tp_count) for i in range(tp_...]
    ppermute x0 -> x7, waiting for transfers between devices: none -> 6.26 us  [body(): lax.ppermute(own_dense, 'tp', [(i, (i + k) % tp_count) for i in range(tp_...]
    all_to_all x2, blocking collectives: 41.4 us -> 36.1 us  [exchange(): return lax.all_to_all(array, axis, 0, 0, tiled=True)]
    pallas_call x3 -> x4, Pallas kernels: 10.8 us -> 12.3 us  [the longest x1 8.21 us: body(): pl.pallas_call(attention_kernel, name='attention', out_shape=jax.ShapeDty...]
    all_to_all x3 -> x2, starting transfers between devices: 17.5 us -> 17 us  [exchange(): return lax.all_to_all(array, axis, 0, 0, tiled=True)]
  transfers between devices with their start and end apart: 3 -> 9, of which waited for: 3 -> 6; matrix products, arithmetic and copies ran while one was open for 1% -> 2% of each run, Pallas kernels for 0% -> 1%
where the time goes in v2:
time: 96.8 us; the launch traced here: 96.4 us
  blocking collectives  36.1 us (37%)
  starting transfers between devices  27.5 us (28%)
  waiting for transfers between devices  17.7 us (18%)
  Pallas kernels  12.6 us (13%)
  other arithmetic  1.42 us (1%)
    all_to_all x2, blocking collectives, exchange(): return lax.all_to_all(array, axis, 0, 0, tiled=True)  36.1 us
    all_to_all x2, starting transfers between devices, exchange(): return lax.all_to_all(array, axis, 0, 0, tiled=True)  17 us
    all_to_all x2, waiting for transfers between devices, exchange(): return lax.all_to_all(array, axis, 0, 0, tiled=True)  11.4 us
    ppermute x7, starting transfers between devices, body(): lax.ppermute(own_dense, 'tp', [(i, (i + k) % tp_count) for i in range(tp_...  10.5 us
    pallas_call x1, Pallas kernels, body(): pl.pallas_call(attention_kernel, name='attention', out_shape=jax.ShapeDty...  8.21 us
    ppermute x7, waiting for transfers between devices, body(): lax.ppermute(own_dense, 'tp', [(i, (i + k) % tp_count) for i in range(tp_...  6.26 us
    pallas_call x1, Pallas kernels, body(): pl.pallas_call(dense_kernel, name='dense', out_shape=jax.ShapeDtypeStruct...  2.07 us
  transfers between devices with their start and end apart: 9, of which 6 were waited for; matrix products, arithmetic and copies ran while one was open for 2% of the time, Pallas kernels for 1%

profile of v2, /device:TPU:1, one launch (start us, length us, event | category | flops | bytes accessed | tf_op | source)
XLA Modules:
  0.0 96.4 jit_solution(12832844804366167415)
XLA Ops:
  0.1 8.2 %attention.1 = bf16[8,16,2048]{2,1,0:T(8,128)(2,1)} custom-call(bf16[16,2048]{1,0:T(8,128)(2,1)} %tokens_ref.1, f32[1,2048]{1,0:T(1,128)} %bitcast.27, bf16[2,2048]{1,0:T(2,128)(2,1)} %bitcast.28, f32[1,2]{1,0:T(1,128)} %bitcast.29, f32[16,2,1024]{2,1,0:T(2,128)} %gate_hbm.1, s32[1,16]{1,0:T(1,128)} %bitcast.30, bf16[2048,128]{1,0:T(8,128)(2,1)} %wq_hbm.1, ...), custom_call_target="tpu_custom_call" | custom-call | flops 1000000000 | bytes 12582912 | tf_op jit(solution)/shard_map/attention/pallas_call | solution.py:339
  8.3 6.6 %all-to-all-start = ((bf16[8,16,2048]{2,1,0:T(8,128)(2,1)}), bf16[8,16,2048]{2,1,0:T(8,128)(2,1)S(1)}, u32[]{:S(2)}, u32[]{:S(2)}) async-start(bf16[8,16,2048]{2,1,0:T(8,128)(2,1)} %attention.1), calls=%async_computation | async-start | bytes 1048576 | tf_op jit(solution)/shard_map/all_to_all | solution.py:294
  15.2 0.1 eq.131
  15.3 0.2 convert_reduce_fusion.1
  15.5 0.1 multiply_add_fusion
  15.6 0.1 fusion.9.dense_mask_ref
  15.7 0.2 slice_reduce_fusion.1
  16.0 0.1 broadcast_in_dim.37
  16.1 0.1 eq.135
  16.2 0.1 select_add_fusion.pick_ref
  16.3 0.2 fusion.4.select_ref
  16.6 7.7 %all-to-all-done.parts_ref = bf16[8,16,2048]{2,1,0:T(8,128)(2,1)S(1)} async-done(((bf16[8,16,2048]{2,1,0:T(8,128)(2,1)}), bf16[8,16,2048]{2,1,0:T(8,128)(2,1)S(1)}, u32[]{:S(2)}, u32[]{:S(2)}) %all-to-all-start) | async-done | bytes 524320 | tf_op jit(solution)/shard_map/all_to_all | solution.py:294
  24.3 1.3 %dispatch.1 = (bf16[256,1024]{1,0:T(8,128)(2,1)}, f32[16,256]{1,0:T(8,128)S(1)}, bf16[32,256]{1,0:T(8,128)(2,1)S(1)}, bf16[32,256]{1,0:T(8,128)(2,1)S(1)}) custom-call(s32[1]{0:T(128)} %bitcast.position_ref, bf16[8,16,2048]{2,1,0:T(8,128)(2,1)S(1)} %all-to-all-done.parts_ref, bf16[16,2048]{1,0:T(8,128)(2,1)S(1)} %copy-done.3, f32[1,2048]{1,0:T(1,128)S(1)} %bitcast.25, ...), custom_call_target="tpu_custom_call" | custom-call | tf_op jit(solution)/shard_map/dispatch/pallas_call | solution.py:428
  25.6 10.4 %all-to-all-start.1 = ((bf16[32,8,1024]{2,1,0:T(8,128)(2,1)}), bf16[32,8,1024]{2,1,0:T(8,128)(2,1)S(1)}, u32[]{:S(2)}, u32[]{:S(2)}) async-start(bf16[32,8,1024]{2,1,0:T(8,128)(2,1)} %bitcast.9), calls=%async_computation.1 | async-start | bytes 1048576 | tf_op jit(solution)/shard_map/all_to_all | solution.py:294
  36.0 1.3 %collective-permute-start.6 = (bf16[768,128]{1,0:T(8,128)(2,1)S(1)}, bf16[768,128]{1,0:T(8,128)(2,1)S(1)}, u32[]{:S(2)}, u32[]{:S(2)}) collective-permute-start(bf16[768,128]{1,0:T(8,128)(2,1)S(1)} %pad_maximum_fusion.refs_0_), channel_id=1, source_target_pairs={{0,7},{1,0},{2,1},{3,2},{4,3},{5,4},{6,5},{7,6},{8,15},{9,8},{10,9... | collective-permute-start | bytes 589832 | tf_op jit(solution)/shard_map/ppermute | solution.py:337
  37.3 0.9 collective-permute-start.5
  38.2 0.8 collective-permute-start.4
  38.9 1.8 %collective-permute-start.3 = (bf16[768,128]{1,0:T(8,128)(2,1)S(1)}, bf16[768,128]{1,0:T(8,128)(2,1)S(1)}, u32[]{:S(2)}, u32[]{:S(2)}) collective-permute-start(bf16[768,128]{1,0:T(8,128)(2,1)S(1)} %pad_maximum_fusion.refs_0_), channel_id=1, source_target_pairs={{0,4},{1,5},{2,6},{3,7},{4,0},{5,1},{6,2},{7,3},{8,12},{9,13},{10,... | collective-permute-start | bytes 589832 | tf_op jit(solution)/shard_map/ppermute | solution.py:337
  40.8 2.1 %collective-permute-start.2 = (bf16[768,128]{1,0:T(8,128)(2,1)S(1)}, bf16[768,128]{1,0:T(8,128)(2,1)S(1)}, u32[]{:S(2)}, u32[]{:S(2)}) collective-permute-start(bf16[768,128]{1,0:T(8,128)(2,1)S(1)} %pad_maximum_fusion.refs_0_), channel_id=1, source_target_pairs={{0,3},{1,4},{2,5},{3,6},{4,7},{5,0},{6,1},{7,2},{8,11},{9,12},{10,... | collective-permute-start | bytes 589832 | tf_op jit(solution)/shard_map/ppermute | solution.py:337
  42.9 0.2 collective-permute-start.1
  43.1 1.1 %collective-permute-done.5.refs_6_ = bf16[768,128]{1,0:T(8,128)(2,1)S(1)} collective-permute-done((bf16[768,128]{1,0:T(8,128)(2,1)S(1)}, bf16[768,128]{1,0:T(8,128)(2,1)S(1)}, u32[]{:S(2)}, u32[]{:S(2)}) %collective-permute-start.5) | collective-permute-done | bytes 196640 | tf_op jit(solution)/shard_map/ppermute | solution.py:337
  44.2 3.4 %collective-permute-start = (bf16[768,128]{1,0:T(8,128)(2,1)S(1)}, bf16[768,128]{1,0:T(8,128)(2,1)}, u32[]{:S(2)}, u32[]{:S(2)}) collective-permute-start(bf16[768,128]{1,0:T(8,128)(2,1)S(1)} %pad_maximum_fusion.refs_0_), channel_id=1, source_target_pairs={{0,1},{1,2},{2,3},{3,4},{4,5},{5,6},{6,7},{7,0},{8,9},{9,10},{10,1... | collective-permute-start | bytes 589832 | tf_op jit(solution)/shard_map/ppermute | solution.py:337
  47.6 3.7 %all-to-all-done.1 = bf16[32,8,1024]{2,1,0:T(8,128)(2,1)S(1)} async-done(((bf16[32,8,1024]{2,1,0:T(8,128)(2,1)}), bf16[32,8,1024]{2,1,0:T(8,128)(2,1)S(1)}, u32[]{:S(2)}, u32[]{:S(2)}) %all-to-all-start.1) | async-done | bytes 524320 | tf_op jit(solution)/shard_map/all_to_all | solution.py:294
  51.3 0.8 picked.1.picked_ref
  52.2 3.0 %collective-permute-done.2.refs_3_ = bf16[768,128]{1,0:T(8,128)(2,1)S(1)} collective-permute-done((bf16[768,128]{1,0:T(8,128)(2,1)S(1)}, bf16[768,128]{1,0:T(8,128)(2,1)S(1)}, u32[]{:S(2)}, u32[]{:S(2)}) %collective-permute-start.2) | collective-permute-done | bytes 196640 | tf_op jit(solution)/shard_map/ppermute | solution.py:337
  55.2 0.5 collective-permute-done.1.refs_2_
  55.7 1.6 %collective-permute-done.refs_1_ = bf16[768,128]{1,0:T(8,128)(2,1)} collective-permute-done((bf16[768,128]{1,0:T(8,128)(2,1)S(1)}, bf16[768,128]{1,0:T(8,128)(2,1)}, u32[]{:S(2)}, u32[]{:S(2)}) %collective-permute-start) | collective-permute-done | bytes 196640 | tf_op jit(solution)/shard_map/ppermute | solution.py:337
  57.3 2.1 %dense.1 = bf16[256,1024]{1,0:T(8,128)(2,1)S(1)} custom-call(s32[1]{0:T(128)} %bitcast.position_ref, bf16[256,1024]{1,0:T(8,128)(2,1)S(1)} %bitcast.19, bf16[256,1024]{1,0:T(8,128)(2,1)S(1)} %picked.1.picked_ref, bf16[768,128]{1,0:T(8,128)(2,1)S(1)} %pad_maximum_fusion.refs_0_, bf16[768,128]{1,0:T(8,128)(2,1)} %collective-permute-done.refs_1_, ...), custom_call_target="tpu_custom_call" | custom-call | tf_op jit(solution)/shard_map/dense/pallas_call | solution.py:447
  59.4 22.8 %all_to_all.20 = bf16[32,8,1024]{2,1,0:T(8,128)(2,1)S(1)} all-to-all(bf16[32,8,1024]{2,1,0:T(8,128)(2,1)S(1)} %bitcast.21), channel_id=1, replica_groups=mesh['ep_0'=8,'ep_1'=4,'tp'=8] {'ep_0','ep_1'}, dimensions={0} | all-to-all | bytes 1048576 | tf_op jit(solution)/shard_map/all_to_all | solution.py:294
  82.2 0.3 combine.1
  82.5 13.3 %all_to_all.21 = bf16[8,16,256]{2,1,0:T(8,128)(2,1)S(1)} all-to-all(bf16[8,16,256]{2,1,0:T(8,128)(2,1)S(1)} %combine.1), channel_id=1, replica_groups=mesh['ep_0'=8,'ep_1'=4,'tp'=8] {'tp'}, dimensions={0} | all-to-all | bytes 131072 | tf_op jit(solution)/shard_map/all_to_all | solution.py:294
  95.8 0.6 add_convert_fusion
  (45 shorter events, 0.5 us)
Async XLA Ops:
  0.0 14.9 %copy-start.11 = (s32[16]{0:T(128)S(1)}, s32[16]{0:T(128)}, u32[]{:S(2)}) copy-start(s32[16]{0:T(128)} %param.36) | copy-start | bytes 196
  0.0 15.0 %copy-start.10 = (f32[16,2]{0,1:T(2,128)S(1)}, f32[16,2]{0,1:T(2,128)}, u32[]{:S(2)}) copy-start(f32[16,2]{0,1:T(2,128)} %param.38) | copy-start | bytes 388
  0.0 15.0 %copy-start.9 = (s32[16,2]{0,1:T(2,128)S(1)}, s32[16,2]{0,1:T(2,128)}, u32[]{:S(2)}) copy-start(s32[16,2]{0,1:T(2,128)} %param.37) | copy-start | bytes 388
  0.0 24.3 %copy-start.3 = (bf16[16,2048]{1,0:T(8,128)(2,1)S(1)}, bf16[16,2048]{1,0:T(8,128)(2,1)}, u32[]{:S(2)}) copy-start(bf16[16,2048]{1,0:T(8,128)(2,1)} %tokens_ref.1) | copy-start | bytes 196612
  0.0 24.3 %copy-start.4 = (f32[2048]{0:T(1024)S(1)}, f32[2048]{0:T(1024)}, u32[]{:S(2)}) copy-start(f32[2048]{0:T(1024)} %param.35) | copy-start | bytes 24580
  0.0 24.3 %copy-start.5 = (f32[2048]{0:T(1024)S(1)}, f32[2048]{0:T(1024)}, u32[]{:S(2)}) copy-start(f32[2048]{0:T(1024)} %param.45) | copy-start | bytes 24580
  0.0 35.9 %copy-start.6 = (bf16[128,256]{1,0:T(8,128)(2,1)S(1)}, bf16[128,256]{1,0:T(8,128)(2,1)}, u32[]{:S(2)}) copy-start(bf16[128,256]{1,0:T(8,128)(2,1)} %param.44) | copy-start | bytes 196612
  0.0 35.9 %copy-start.7 = (bf16[256,128]{1,0:T(8,128)(2,1)S(1)}, bf16[256,128]{1,0:T(8,128)(2,1)}, u32[]{:S(2)}) copy-start(bf16[256,128]{1,0:T(8,128)(2,1)} %param.43) | copy-start | bytes 196612
  0.1 35.9 %copy-start.8 = (bf16[256,128]{1,0:T(8,128)(2,1)S(1)}, bf16[256,128]{1,0:T(8,128)(2,1)}, u32[]{:S(2)}) copy-start(bf16[256,128]{1,0:T(8,128)(2,1)} %param.42) | copy-start | bytes 196612
  0.1 51.3 %copy-start = (bf16[1,2048,128]{2,1,0:T(8,128)(2,1)S(1)}, bf16[1,2048,128]{2,1,0:T(8,128)(2,1)}, u32[]{:S(2)}) copy-start(bf16[1,2048,128]{2,1,0:T(8,128)(2,1)} %param.39) | copy-start | bytes 1572868
  0.1 51.2 %copy-start.1 = (bf16[1,2048,128]{2,1,0:T(8,128)(2,1)S(1)}, bf16[1,2048,128]{2,1,0:T(8,128)(2,1)}, u32[]{:S(2)}) copy-start(bf16[1,2048,128]{2,1,0:T(8,128)(2,1)} %param.40) | copy-start | bytes 1572868
  0.1 51.2 %copy-start.2 = (bf16[1,128,2048]{2,1,0:T(8,128)(2,1)S(1)}, bf16[1,128,2048]{2,1,0:T(8,128)(2,1)}, u32[]{:S(2)}) copy-start(bf16[1,128,2048]{2,1,0:T(8,128)(2,1)} %param.41) | copy-start | bytes 1572868
  8.3 16.0 %all-to-all-start = ((bf16[8,16,2048]{2,1,0:T(8,128)(2,1)}), bf16[8,16,2048]{2,1,0:T(8,128)(2,1)S(1)}, u32[]{:S(2)}, u32[]{:S(2)}) async-start(bf16[8,16,2048]{2,1,0:T(8,128)(2,1)} %attention.1), calls=%async_computation | async-start | bytes 1048576 | tf_op jit(solution)/shard_map/all_to_all | solution.py:294
  25.6 25.8 %all-to-all-start.1 = ((bf16[32,8,1024]{2,1,0:T(8,128)(2,1)}), bf16[32,8,1024]{2,1,0:T(8,128)(2,1)S(1)}, u32[]{:S(2)}, u32[]{:S(2)}) async-start(bf16[32,8,1024]{2,1,0:T(8,128)(2,1)} %bitcast.9), calls=%async_computation.1 | async-start | bytes 1048576 | tf_op jit(solution)/shard_map/all_to_all | solution.py:294
  36.0 6.9 %collective-permute-start.6 = (bf16[768,128]{1,0:T(8,128)(2,1)S(1)}, bf16[768,128]{1,0:T(8,128)(2,1)S(1)}, u32[]{:S(2)}, u32[]{:S(2)}) collective-permute-start(bf16[768,128]{1,0:T(8,128)(2,1)S(1)} %pad_maximum_fusion.refs_0_), channel_id=1, source_target_pairs={{0,7},{1,0},{2,1},{3,2},{4,3},{5,4},{6,5},{7,6},{8,15},{9,8},{10,9... | collective-permute-start | bytes 589832 | tf_op jit(solution)/shard_map/ppermute | solution.py:337
  37.3 6.9 %collective-permute-start.5 = (bf16[768,128]{1,0:T(8,128)(2,1)S(1)}, bf16[768,128]{1,0:T(8,128)(2,1)S(1)}, u32[]{:S(2)}, u32[]{:S(2)}) collective-permute-start(bf16[768,128]{1,0:T(8,128)(2,1)S(1)} %pad_maximum_fusion.refs_0_), channel_id=1, source_target_pairs={{0,6},{1,7},{2,0},{3,1},{4,2},{5,3},{6,4},{7,5},{8,14},{9,15},{10,... | collective-permute-start | bytes 589832 | tf_op jit(solution)/shard_map/ppermute | solution.py:337
  38.2 14.0 %collective-permute-start.4 = (bf16[768,128]{1,0:T(8,128)(2,1)S(1)}, bf16[768,128]{1,0:T(8,128)(2,1)S(1)}, u32[]{:S(2)}, u32[]{:S(2)}) collective-permute-start(bf16[768,128]{1,0:T(8,128)(2,1)S(1)} %pad_maximum_fusion.refs_0_), channel_id=1, source_target_pairs={{0,5},{1,6},{2,7},{3,0},{4,1},{5,2},{6,3},{7,4},{8,13},{9,14},{10,... | collective-permute-start | bytes 589832 | tf_op jit(solution)/shard_map/ppermute | solution.py:337
  38.9 13.2 %collective-permute-start.3 = (bf16[768,128]{1,0:T(8,128)(2,1)S(1)}, bf16[768,128]{1,0:T(8,128)(2,1)S(1)}, u32[]{:S(2)}, u32[]{:S(2)}) collective-permute-start(bf16[768,128]{1,0:T(8,128)(2,1)S(1)} %pad_maximum_fusion.refs_0_), channel_id=1, source_target_pairs={{0,4},{1,5},{2,6},{3,7},{4,0},{5,1},{6,2},{7,3},{8,12},{9,13},{10,... | collective-permute-start | bytes 589832 | tf_op jit(solution)/shard_map/ppermute | solution.py:337
  40.8 14.4 %collective-permute-start.2 = (bf16[768,128]{1,0:T(8,128)(2,1)S(1)}, bf16[768,128]{1,0:T(8,128)(2,1)S(1)}, u32[]{:S(2)}, u32[]{:S(2)}) collective-permute-start(bf16[768,128]{1,0:T(8,128)(2,1)S(1)} %pad_maximum_fusion.refs_0_), channel_id=1, source_target_pairs={{0,3},{1,4},{2,5},{3,6},{4,7},{5,0},{6,1},{7,2},{8,11},{9,12},{10,... | collective-permute-start | bytes 589832 | tf_op jit(solution)/shard_map/ppermute | solution.py:337
  42.9 12.8 %collective-permute-start.1 = (bf16[768,128]{1,0:T(8,128)(2,1)S(1)}, bf16[768,128]{1,0:T(8,128)(2,1)S(1)}, u32[]{:S(2)}, u32[]{:S(2)}) collective-permute-start(bf16[768,128]{1,0:T(8,128)(2,1)S(1)} %pad_maximum_fusion.refs_0_), channel_id=1, source_target_pairs={{0,2},{1,3},{2,4},{3,5},{4,6},{5,7},{6,0},{7,1},{8,10},{9,11},{10,... | collective-permute-start | bytes 589832 | tf_op jit(solution)/shard_map/ppermute | solution.py:337
  44.2 13.1 %collective-permute-start = (bf16[768,128]{1,0:T(8,128)(2,1)S(1)}, bf16[768,128]{1,0:T(8,128)(2,1)}, u32[]{:S(2)}, u32[]{:S(2)}) collective-permute-start(bf16[768,128]{1,0:T(8,128)(2,1)S(1)} %pad_maximum_fusion.refs_0_), channel_id=1, source_target_pairs={{0,1},{1,2},{2,3},{3,4},{4,5},{5,6},{6,7},{7,0},{8,9},{9,10},{10,1... | collective-permute-start | bytes 589832 | tf_op jit(solution)/shard_map/ppermute | solution.py:337

commit v3 on v2

v3 whole, which is shorter than its diff:
```python
import jax
import jax.numpy as jnp
from jax import lax
from jax.experimental import pallas as pl
from jax.experimental.pallas import tpu as pltpu
from jax.sharding import Mesh
from jax.sharding import PartitionSpec as P

EXPERTS_PER_GROUP = 8
EXPERTS = 32
EP = ("ep_0", "ep_1")
EPS = 1e-06
F32 = jnp.float32
BF16 = jnp.bfloat16
NT = (((1,), (1,)), ((), ()))
VMEM = pl.BlockSpec(memory_space=pltpu.VMEM)
SMEM = pl.BlockSpec(memory_space=pltpu.SMEM)
ANY = pl.BlockSpec(memory_space=pl.ANY)
MIB = 1 << 20


def rms_scale(rows, gain):
    rows = rows.astype(F32)
    return rows * lax.rsqrt(jnp.mean(rows * rows, axis=-1, keepdims=True) + EPS) * gain


def silu(v):
    return v * jax.nn.sigmoid(v)


def stacked(pair):
    return jnp.concatenate([pair[:, 0:1], pair[:, 1:2]], axis=0)


def attention_kernel(
    tokens_hbm,
    gain_hbm,
    forget_hbm,
    bias_hbm,
    gate_hbm,
    length_hbm,
    group_hbm,
    slot_hbm,
    route_weight_hbm,
    wq_hbm,
    wk_hbm,
    wv_hbm,
    wo_hbm,
    key_hbm,
    value_hbm,
    parts_ref,
    table_ref,
    tokens_ref,
    gain_ref,
    forget_ref,
    bias_ref,
    gate_ref,
    length_ref,
    group_ref,
    slot_ref,
    route_weight_ref,
    wqkv,
    wo,
    keys,
    values,
    scores,
    weighted,
    small_sems,
    w_sems,
    key_sems,
    value_sems,
):
    seqs, cache_len, width = keys.shape
    heads = 2
    half = width // heads
    rows = heads * seqs
    scale = half ** (-0.5)
    key_group, value_group = 16, 16
    small = [
        pltpu.make_async_copy(src, dst, small_sems.at[i])
        for i, (src, dst) in enumerate(
            (
                (tokens_hbm, tokens_ref),
                (gain_hbm, gain_ref),
                (forget_hbm, forget_ref),
                (bias_hbm, bias_ref),
                (length_hbm, length_ref),
                (gate_hbm, gate_ref),
                (group_hbm, group_ref),
                (slot_hbm, slot_ref),
                (route_weight_hbm, route_weight_ref),
            )
        )
    ]
    weight_copies = [
        pltpu.make_async_copy(src, wqkv.at[i], w_sems.at[i])
        for i, src in enumerate((wq_hbm, wk_hbm, wv_hbm))
    ]
    output_copy = pltpu.make_async_copy(wo_hbm, wo, w_sems.at[3])
    part = lambda g, n: pl.ds(g * n, n)
    key_copies = [
        pltpu.make_async_copy(key_hbm.at[part(g, key_group)], keys.at[part(g, key_group)], key_sems.at[g])
        for g in range(seqs // key_group)
    ]
    value_copies = [
        pltpu.make_async_copy(value_hbm.at[part(g, value_group)], values.at[part(g, value_group)], value_sems.at[g])
        for g in range(seqs // value_group)
    ]
    for copy in small + weight_copies + key_copies + value_copies + [output_copy]:
        copy.start()
    for copy in small:
        copy.wait()
    normed = rms_scale(tokens_ref[...], gain_ref[...]).astype(BF16)
    forget_logit = (
        lax.dot_general(normed, forget_ref[...], NT, preferred_element_type=F32) + bias_ref[...]
    )
    forget_log = stacked(jax.nn.log_sigmoid(forget_logit))
    length = column_of(length_ref[...]).astype(jnp.int32)
    length = jnp.concatenate([length, length], axis=0)
    gate = jnp.concatenate([gate_ref[:, 0, :], gate_ref[:, 1, :]], axis=0)
    entry = lax.broadcasted_iota(jnp.int32, (rows, cache_len), 1)
    last_gate = jnp.sum(jnp.where(entry == length - 1, gate, 0.0), axis=1, keepdims=True)
    current = last_gate + forget_log
    for copy in weight_copies:
        copy.wait()
    query, key_new, value_new = [
        jnp.dot(normed, wqkv[i], preferred_element_type=F32).astype(BF16).astype(F32)
        for i in range(3)
    ]
    lane = lax.broadcasted_iota(jnp.int32, (1, width), 1)
    first_head = lane < half
    own = query * key_new
    own_score = scale * jnp.concatenate(
        [
            jnp.sum(jnp.where(first_head, own, 0.0), axis=1, keepdims=True),
            jnp.sum(jnp.where(first_head, 0.0, own), axis=1, keepdims=True),
        ],
        axis=0,
    )
    row8 = lax.broadcasted_iota(jnp.int32, (8, width), 0)
    lane8 = lax.broadcasted_iota(jnp.int32, (8, width), 1)
    masks = [
        (row8 // heads == i) & ((lane8 < half) == (lax.rem(row8, heads) == 0)) for i in range(2)
    ]
    place_columns = routing_places(group_ref[...] * EXPERTS_PER_GROUP + slot_ref[...])
    combine_table(place_columns, route_weight_ref[...], table_ref)
    tail = jnp.zeros((seqs, width), F32)
    for k, place in enumerate(place_columns):
        tail = tail + jnp.where(lane == k, place.astype(F32), 0.0)
    tail = tail.astype(BF16)
    for g in range(seqs // key_group):
        key_copies[g].wait()
        for s in range(g * key_group, (g + 1) * key_group, 2):
            masked = jnp.concatenate(
                [jnp.where(masks[i], query[s + i : s + i + 1], 0.0) for i in range(2)], axis=1
            ).astype(BF16)
            pair = jnp.concatenate([keys[s], keys[s + 1]], axis=1)
            result = lax.dot_general(masked, pair, NT, preferred_element_type=F32)
            for i in range(2):
                for h in range(heads):
                    scores[h * seqs + s + i : h * seqs + s + i + 1] = result[
                        heads * i + h : heads * i + h + 1
                    ]
    score = scores[...] * scale + (current - gate)
    score = jnp.where(entry < length, score, -jnp.inf)
    peak = jnp.maximum(jnp.max(score, axis=1, keepdims=True), own_score)
    weights = jnp.exp(score - peak)
    own_weight = jnp.exp(own_score - peak)
    denominator = jnp.sum(weights, axis=1, keepdims=True) + own_weight
    scores[...] = weights
    for g in range(seqs // value_group):
        value_copies[g].wait()
        for s in range(g * value_group, (g + 1) * value_group, 2):
            four = jnp.concatenate(
                [
                    scores[h * seqs + s + i : h * seqs + s + i + 1]
                    for i in range(2)
                    for h in range(heads)
                ]
                + [jnp.zeros((4, cache_len), F32)],
                axis=0,
            ).astype(BF16)
            pair = jnp.concatenate([values[s], values[s + 1]], axis=1)
            result = jnp.dot(four, pair, preferred_element_type=F32)
            for i in range(2):
                mine = result[heads * i : heads * i + heads, i * width : (i + 1) * width]
                weighted[s + i : s + i + 1] = jnp.where(first_head, mine[0:1], mine[1:2])
    output_copy.wait()
    own_weight = own_weight.astype(BF16).astype(F32)
    own_weight = jnp.where(first_head, own_weight[:seqs], own_weight[seqs:])
    denominator = jnp.where(first_head, denominator[:seqs], denominator[seqs:])
    attended = ((weighted[...] + own_weight * value_new) / denominator).astype(BF16)
    head_part = jnp.dot(attended, wo[...], preferred_element_type=F32).astype(BF16)
    model_width = head_part.shape[1]
    for i in range(parts_ref.shape[0]):
        parts_ref[i, :, 0:model_width] = head_part
        parts_ref[i, :, model_width:] = tail


def column_of(row):
    n = row.shape[1]
    same = lax.broadcasted_iota(jnp.int32, (n, n), 0) == lax.broadcasted_iota(
        jnp.int32, (n, n), 1
    )
    return jnp.sum(jnp.where(same, row.astype(F32), 0.0), axis=1, keepdims=True)


def routing_places(ids):
    picks, seqs = ids.shape
    columns = [column_of(ids[k : k + 1]) for k in range(picks)]
    down = lax.broadcasted_iota(jnp.int32, (seqs, seqs), 0)
    across = lax.broadcasted_iota(jnp.int32, (seqs, seqs), 1)
    rows = [ids[k : k + 1].astype(F32) for k in range(picks)]
    places = []
    for column in columns:
        before = jnp.zeros((seqs, 1), F32)
        for row in rows:
            hit = (column == row) & (across < down)
            before = before + jnp.sum(jnp.where(hit, 1.0, 0.0), axis=1, keepdims=True)
        places.append((column * 8 + before).astype(jnp.int32))
    return places


def select_table(place_rows, position, rows):
    seqs = place_rows[0].shape[1]
    row = lax.broadcasted_iota(jnp.int32, (rows, 2 * seqs), 0)
    column = lax.broadcasted_iota(jnp.int32, (rows, 2 * seqs), 1)
    slot = row & 3
    row_place = (row & ~7) + slot
    token = column & (seqs - 1)
    hit = (slot >= 2) & (token == position * 2 + slot - 2)
    for place in place_rows:
        places = jnp.concatenate([place, place], axis=1)
        hit = hit | ((slot < 2) & (places == row_place))
    same_half = ((row >> 2) & 1) == (column >= seqs).astype(jnp.int32)
    return jnp.where(hit & same_half, 1.0, 0.0).astype(BF16)


def combine_table(place_columns, weight_rows, table_ref):
    seqs = place_columns[0].shape[0]
    wide = table_ref.shape[1]
    row = lax.broadcasted_iota(jnp.int32, (2 * seqs, wide), 0)
    column = lax.broadcasted_iota(jnp.int32, (2 * seqs, wide), 1)
    slot = column & 3
    source = (column >> 3) & 7
    expert_place = ((column >> 6) << 3) + slot
    same_half = ((column >> 2) & 1) == (row >= seqs).astype(jnp.int32)
    weight = jnp.zeros((2 * seqs, wide), F32)
    for k, place in enumerate(place_columns):
        places = jnp.concatenate([place, place], axis=0)
        value = column_of(weight_rows[k : k + 1])
        value = jnp.concatenate([value, value], axis=0)
        weight = weight + jnp.where(
            same_half & (slot < 2) & (places == expert_place), value, 0.0
        )
    high = weight.astype(BF16)
    table_ref[0 : 2 * seqs] = high
    table_ref[2 * seqs : 4 * seqs] = (weight - high.astype(F32)).astype(BF16)
    dense = same_half & (slot >= 2) & ((row & (seqs - 1)) == source * 2 + slot - 2)
    table_ref[4 * seqs : 6 * seqs] = jnp.where(dense, 1.0, 0.0).astype(BF16)


def dispatch_kernel(
    position_ref,
    parts_ref,
    tokens_ref,
    gain_ref,
    mix_ref,
    out_ref,
    residual_ref,
    mix_gate_ref,
    scratch,
):
    half = out_ref.shape[1]
    width = residual_ref.shape[1]
    model_width = tokens_ref.shape[1]
    seqs = tokens_ref.shape[0]
    columns = parts_ref[0, :, model_width:].astype(F32)
    same = lax.broadcasted_iota(jnp.int32, (seqs, seqs), 0) == lax.broadcasted_iota(
        jnp.int32, (seqs, seqs), 1
    )
    place_rows = [
        jnp.sum(jnp.where(same, columns[:, k : k + 1], 0.0), axis=0, keepdims=True).astype(
            jnp.int32
        )
        for k in range(2)
    ]
    select = select_table(place_rows, position_ref[0], out_ref.shape[0])
    attn = parts_ref[0, :, 0:model_width].astype(F32)
    for i in range(1, parts_ref.shape[0]):
        attn = attn + parts_ref[i, :, 0:model_width].astype(F32)
    residual = tokens_ref[...].astype(F32) + attn
    scratch[...] = residual
    normed = rms_scale(residual, gain_ref[...]).astype(BF16)
    both = jnp.concatenate([normed[:, :half], normed[:, half:]], axis=0)
    mix_gate_ref[...] = jax.nn.sigmoid(
        jnp.sum(normed.astype(F32) * mix_ref[...], axis=1, keepdims=True)
    )
    mine = pl.ds(pl.multiple_of(position_ref[0] * width, width), width)
    residual_ref[...] = scratch[:, mine]
    out_ref[...] = jnp.dot(select, both, preferred_element_type=F32).astype(BF16)


def row_kinds(rows):
    row = lax.broadcasted_iota(jnp.int32, (rows, 1), 0)
    return lax.rem(row, 8) >= 4, lax.rem(row, 4) >= 2


def whole_rows(both):
    rows, width = both.shape
    both = both.reshape(rows // 8, 8, width)
    return (both + pltpu.roll(both, 4, 1)).reshape(rows, width)


def picked_kernel(rows_ref, gate_ref, up_ref, hidden_ref):
    rows, half = rows_ref.shape
    width = gate_ref.shape[1]
    second, is_dense = row_kinds(rows)
    sums = []
    for h in range(2):
        weights = jnp.concatenate(
            [gate_ref[h * half : (h + 1) * half], up_ref[h * half : (h + 1) * half]], axis=1
        )
        sums.append(jnp.dot(rows_ref[...], weights, preferred_element_type=F32))
    both = whole_rows(jnp.where(second, sums[1], sums[0]))
    hidden = silu(both[:, :width]) * both[:, width:]
    hidden_ref[...] = jnp.where(is_dense, 0.0, hidden).astype(BF16)


LATE = (1, 2, 3, 4)


def dense_kernel(position_ref, rows_ref, picked_ref, down_ref, *refs):
    out_ref, late, sems = refs[-3:]
    operands = refs[:-3]
    blocks = len(operands)
    copies = [
        pltpu.make_async_copy(operands[k], late.at[i], sems.at[i]) for i, k in enumerate(LATE)
    ]
    for copy in copies:
        copy.start()
    pieces = {k: operands[k] for k in range(blocks) if k not in LATE}
    pieces.update({k: late.at[i] for i, k in enumerate(LATE)})
    rows, half = rows_ref.shape
    width = late.shape[2]
    per_half = blocks // 2
    kb = half // per_half
    position = position_ref[0]
    second, is_dense = row_kinds(rows)
    both = None
    for k, piece in pieces.items():
        if k == LATE[0]:
            for copy in copies:
                copy.wait()
        t = lax.rem(position - k + blocks, blocks)
        inner = pl.ds(pl.multiple_of(lax.rem(t, per_half) * kb, kb), kb)
        weights = jnp.concatenate([piece[0:kb], piece[kb : 2 * kb]], axis=1)
        part = jnp.dot(rows_ref[:, inner], weights, preferred_element_type=F32)
        part = jnp.where(second == (t >= per_half), part, 0.0)
        both = part if both is None else both + part
    both = whole_rows(both)
    hidden = silu(both[:, :width]) * both[:, width:]
    hidden = jnp.concatenate(
        [picked_ref[...], jnp.where(is_dense, hidden, 0.0).astype(BF16)], axis=1
    )
    for k, piece in pieces.items():
        t = lax.rem(position - k + blocks, blocks)
        dense_down = jnp.concatenate(
            [piece[2 * kb : 2 * kb + width], piece[2 * kb + width : 2 * kb + 2 * width]], axis=1
        )
        whole = pl.ds(pl.multiple_of(t * kb, kb), kb)
        down = jnp.concatenate([down_ref[:, whole], dense_down], axis=0)
        result = jnp.dot(hidden, down, preferred_element_type=F32)
        result = jnp.where(second, result[:, width:], result[:, :width]).astype(BF16)
        out_ref[:, t] = result.reshape(rows // 8, 8, width)


def combine_kernel(rows_ref, table_ref, mix_ref, residual_ref, out_ref):
    seqs = mix_ref.shape[0]
    width = rows_ref.shape[1]
    sums = jnp.dot(table_ref[...], rows_ref[...], preferred_element_type=F32)
    mix = mix_ref[...]
    for p in range(2):
        picked = sums[p * seqs : (p + 1) * seqs] + sums[(2 + p) * seqs : (3 + p) * seqs]
        dense = sums[(4 + p) * seqs : (5 + p) * seqs]
        columns = slice(p * width, (p + 1) * width)
        out_ref[:, columns] = (residual_ref[:, columns] + picked + mix * dense).astype(BF16)


def limits(mib):
    return pltpu.CompilerParams(vmem_limit_bytes=mib * MIB)


def exchange(array, axis):
    return lax.all_to_all(array, axis, 0, 0, tiled=True)


def attention_call(*operands):
    tokens, key_cache = operands[0], operands[13]
    seqs, model_width = tokens.shape
    _, cache_len, head_width = key_cache.shape
    tp_count = 8
    return pl.pallas_call(
        attention_kernel,
        name="attention",
        out_shape=(
            jax.ShapeDtypeStruct((tp_count, seqs, model_width + head_width), BF16),
            jax.ShapeDtypeStruct((6 * seqs, EXPERTS * 8 * tp_count), BF16),
        ),
        in_specs=[ANY] * 15,
        out_specs=(VMEM, VMEM),
        scratch_shapes=[
            pltpu.VMEM((seqs, model_width), BF16),
            pltpu.VMEM((1, model_width), F32),
            pltpu.VMEM((2, model_width), BF16),
            pltpu.VMEM((1, 2), F32),
            pltpu.VMEM((seqs, 2, cache_len), F32),
            pltpu.VMEM((1, seqs), jnp.int32),
            pltpu.VMEM((1, seqs), jnp.int32),
            pltpu.VMEM((2, seqs), jnp.int32),
            pltpu.VMEM((2, seqs), F32),
            pltpu.VMEM((3, model_width, head_width), BF16),
            pltpu.VMEM((head_width, model_width), BF16),
            pltpu.VMEM((seqs, cache_len, head_width), BF16),
            pltpu.VMEM((seqs, cache_len, head_width), BF16),
            pltpu.VMEM((2 * seqs, cache_len), F32),
            pltpu.VMEM((seqs, head_width), F32),
            pltpu.SemaphoreType.DMA((9,)),
            pltpu.SemaphoreType.DMA((4,)),
            pltpu.SemaphoreType.DMA((16,)),
            pltpu.SemaphoreType.DMA((16,)),
        ],
        compiler_params=limits(60),
        cost_estimate=pl.CostEstimate(flops=10**9, bytes_accessed=12 * MIB, transcendentals=40000),
    )(*operands)


def body(
    tokens,
    norm_attn,
    w_query,
    w_key,
    w_value,
    w_forget,
    forget_bias,
    w_output,
    key_cache,
    value_cache,
    gate_cache,
    lengths,
    norm_ffn,
    route_group,
    route_slot,
    route_weight,
    expert_gate,
    expert_up,
    expert_down,
    dense_gate,
    dense_up,
    dense_down,
    mix_vector,
):
    seqs, model_width = tokens.shape
    ep_count = lax.axis_size(EP)
    tp_count = lax.axis_size("tp")
    tp_position = lax.axis_index("tp")
    width_local = model_width // tp_count
    half = model_width // 2
    head_width = key_cache.shape[2]

    own_dense = jnp.concatenate(
        [dense_gate, dense_up, dense_down[:, :head_width], dense_down[:, head_width:]], axis=0
    )
    dense_weights = [own_dense]
    for k in range(1, tp_count):
        dense_weights.append(
            lax.ppermute(own_dense, "tp", [(i, (i + k) % tp_count) for i in range(tp_count)])
        )
    parts, table = attention_call(
        tokens,
        norm_attn.reshape(1, -1),
        w_forget.T,
        forget_bias.reshape(1, -1),
        gate_cache,
        lengths.reshape(1, -1),
        route_group.reshape(1, -1),
        route_slot.T,
        route_weight.T,
        w_query,
        w_key,
        w_value,
        w_output,
        key_cache,
        value_cache,
    )
    parts = exchange(parts, "tp")

    position = tp_position.reshape(1)
    row_count = ep_count * 8
    wide = row_count * tp_count
    dispatch = pl.pallas_call(
        dispatch_kernel,
        name="dispatch",
        out_shape=(
            jax.ShapeDtypeStruct((row_count, half), BF16),
            jax.ShapeDtypeStruct((seqs, width_local), F32),
            jax.ShapeDtypeStruct((seqs, 1), F32),
        ),
        in_specs=[SMEM] + [VMEM] * 4,
        out_specs=(VMEM, VMEM, VMEM),
        scratch_shapes=[pltpu.VMEM((seqs, model_width), F32)],
        compiler_params=limits(8),
    )
    outgoing, residual, mix_gate = dispatch(
        position,
        parts,
        tokens,
        norm_ffn.reshape(1, -1),
        mix_vector.reshape(1, -1),
    )
    arrived = exchange(outgoing.reshape(ep_count, 8, half), EP).reshape(row_count, half)
    hidden = pl.pallas_call(
        picked_kernel,
        name="picked",
        out_shape=jax.ShapeDtypeStruct((row_count, head_width), BF16),
        in_specs=[VMEM] * 3,
        out_specs=VMEM,
        compiler_params=limits(8),
    )(arrived, expert_gate[0], expert_up[0])
    results = pl.pallas_call(
        dense_kernel,
        name="dense",
        out_shape=jax.ShapeDtypeStruct((ep_count, tp_count, 8, width_local // 2), BF16),
        in_specs=[SMEM] + [VMEM] * 3 + [ANY if k in LATE else VMEM for k in range(tp_count)],
        out_specs=VMEM,
        scratch_shapes=[
            pltpu.VMEM((len(LATE), *own_dense.shape), BF16),
            pltpu.SemaphoreType.DMA((len(LATE),)),
        ],
        compiler_params=limits(8),
    )(position, arrived, hidden, expert_down[0], *dense_weights)
    returned = exchange(
        results.reshape(ep_count * tp_count, 8, width_local // 2), (*EP, "tp")
    ).reshape(wide, width_local // 2)
    return pl.pallas_call(
        combine_kernel,
        name="combine",
        out_shape=jax.ShapeDtypeStruct((seqs, width_local), BF16),
        in_specs=[VMEM] * 4,
        out_specs=VMEM,
        compiler_params=limits(8),
    )(returned, table, mix_gate, residual)


def solution(mesh):
    split = Mesh(mesh.devices.reshape(8, 4, mesh.shape["tp"]), ("ep_0", "ep_1", "tp"))
    return jax.shard_map(
        body,
        mesh=split,
        in_specs=(
            P(EP, None),
            P(),
            P(None, "tp"),
            P(None, "tp"),
            P(None, "tp"),
            P(None, "tp"),
            P("tp"),
            P("tp", None),
            P(EP, None, "tp"),
            P(EP, None, "tp"),
            P(EP, "tp", None),
            P(EP),
            P(),
            P(EP),
            P(EP, None),
            P(EP, None),
            P(EP, None, "tp"),
            P(EP, None, "tp"),
            P(EP, "tp", None),
            P("tp", EP),
            P("tp", EP),
            P(EP, "tp"),
            P(),
        ),
        out_specs=P(EP, "tp"),
        check_vma=False,
    )
```

time: 96.8 us -> 92.8 us (0.959)
  blocking collectives: 36.1 us -> 33.6 us
  waiting for transfers between devices: 17.7 us -> 20 us
  Pallas kernels: 12.6 us -> 11 us
  other arithmetic: 1.42 us -> 0.02 us
    all_to_all x2 -> x1, blocking collectives: 36.1 us -> 33.6 us  [exchange(): return lax.all_to_all(array, axis, 0, 0, tiled=True)]
    all_to_all x2, waiting for transfers between devices: 11.4 us -> 13.4 us  [exchange(): return lax.all_to_all(array, axis, 0, 0, tiled=True)]
    pallas_call x2, Pallas kernels: 9.47 us -> 7.81 us  [the longest x1 6.53 us: attention_call(): pl.pallas_call(attention_kernel, name='attention', out_shape=(jax.ShapeDt...]
  transfers between devices with their start and end apart: 9 -> 9, of which waited for: 6 -> 6; matrix products, arithmetic and copies ran while one was open for 2% -> 0% of each run, Pallas kernels for 1% -> 0%
where the time goes in v3:
time: 92.8 us; the launch traced here: 92.5 us
  blocking collectives  33.6 us (36%)
  starting transfers between devices  27.6 us (30%)
  waiting for transfers between devices  20 us (22%)
  Pallas kernels  11 us (12%)
    all_to_all x1, blocking collectives, exchange(): return lax.all_to_all(array, axis, 0, 0, tiled=True)  33.6 us
    all_to_all x2, starting transfers between devices, exchange(): return lax.all_to_all(array, axis, 0, 0, tiled=True)  17.1 us
    all_to_all x2, waiting for transfers between devices, exchange(): return lax.all_to_all(array, axis, 0, 0, tiled=True)  13.4 us
    ppermute x7, starting transfers between devices, body(): lax.ppermute(own_dense, 'tp', [(i, (i + k) % tp_count) for i in range(tp_...  10.5 us
    ppermute x7, waiting for transfers between devices, body(): lax.ppermute(own_dense, 'tp', [(i, (i + k) % tp_count) for i in range(tp_...  6.61 us
    pallas_call x1, Pallas kernels, attention_call(): pl.pallas_call(attention_kernel, name='attention', out_shape=(jax.ShapeDt...  6.53 us
    pallas_call x1, Pallas kernels, body(): pl.pallas_call(dense_kernel, name='dense', out_shape=jax.ShapeDtypeStruct...  1.92 us
  transfers between devices with their start and end apart: 9, of which 6 were waited for; matrix products, arithmetic and copies ran while one was open for 0% of the time, Pallas kernels for 0%

profile of v3, /device:TPU:1, one launch (start us, length us, event | category | flops | bytes accessed | tf_op | source)
XLA Modules:
  0.0 92.5 jit_solution(6717353940418483061)
XLA Ops:
  0.0 0.0 copy-start.7
  0.0 0.0 copy-start.8
  0.0 0.0 copy-start.9
  0.0 0.0 copy-start
  0.1 6.5 %attention.1 = (bf16[8,16,2176]{2,1,0:T(8,128)(2,1)}, bf16[96,2048]{1,0:T(8,128)(2,1)}) custom-call(bf16[16,2048]{1,0:T(8,128)(2,1)} %tokens_ref.1, f32[1,2048]{1,0:T(1,128)} %bitcast.26, bf16[2,2048]{1,0:T(2,128)(2,1)} %bitcast.27, f32[1,2]{1,0:T(1,128)} %bitcast.30, f32[16,2,1024]{2,1,0:T(2,128)} %gate_hbm.1, s32[1,16]{1,0:T(1,128)} %bitcast.31, ...), custom_call_target="tpu_custom_call" | custom-call | flops 1000000000 | bytes 12582912 | tf_op jit(solution)/shard_map/attention/pallas_call | solution.py:403
  6.6 0.0 copy-start.2
  6.6 6.7 %all-to-all-start = ((bf16[8,16,2176]{2,1,0:T(8,128)(2,1)}), bf16[8,16,2176]{2,1,0:T(8,128)(2,1)S(1)}, u32[]{:S(2)}, u32[]{:S(2)}) async-start(bf16[8,16,2176]{2,1,0:T(8,128)(2,1)} %get-tuple-element.10), calls=%async_computation | async-start | bytes 1114112 | tf_op jit(solution)/shard_map/all_to_all | solution.py:395
  13.3 9.7 %all-to-all-done.parts_ref = bf16[8,16,2176]{2,1,0:T(8,128)(2,1)S(1)} async-done(((bf16[8,16,2176]{2,1,0:T(8,128)(2,1)}), bf16[8,16,2176]{2,1,0:T(8,128)(2,1)S(1)}, u32[]{:S(2)}, u32[]{:S(2)}) %all-to-all-start) | async-done | bytes 557088 | tf_op jit(solution)/shard_map/all_to_all | solution.py:395
  23.1 0.0 copy-done.4
  23.1 1.3 %dispatch.1 = (bf16[256,1024]{1,0:T(8,128)(2,1)}, f32[16,256]{1,0:T(8,128)S(1)}, f32[16,1]{1,0:T(8,128)S(1)}) custom-call(s32[1]{0:T(128)} %bitcast.position_ref, bf16[8,16,2176]{2,1,0:T(8,128)(2,1)S(1)} %all-to-all-done.parts_ref, bf16[16,2048]{1,0:T(8,128)(2,1)S(1)} %copy-done.4, f32[1,2048]{1,0:T(1,128)S(1)} %bitcast.24, f32[1,2048]{1,0:T(1,128)S(1)} %bitcast.25), custom_call_target="tpu_custom_call" | custom-call | tf_op jit(solution)/shard_map/dispatch/pallas_call | solution.py:514
  24.4 10.4 %all-to-all-start.1 = ((bf16[32,8,1024]{2,1,0:T(8,128)(2,1)}), bf16[32,8,1024]{2,1,0:T(8,128)(2,1)S(1)}, u32[]{:S(2)}, u32[]{:S(2)}) async-start(bf16[32,8,1024]{2,1,0:T(8,128)(2,1)} %bitcast.10), calls=%async_computation.1 | async-start | bytes 1048576 | tf_op jit(solution)/shard_map/all_to_all | solution.py:395
  34.8 1.3 %collective-permute-start.6 = (bf16[768,128]{1,0:T(8,128)(2,1)S(1)}, bf16[768,128]{1,0:T(8,128)(2,1)S(1)}, u32[]{:S(2)}, u32[]{:S(2)}) collective-permute-start(bf16[768,128]{1,0:T(8,128)(2,1)S(1)} %pad_maximum_fusion.refs_0_), channel_id=1, source_target_pairs={{0,7},{1,0},{2,1},{3,2},{4,3},{5,4},{6,5},{7,6},{8,15},{9,8},{10,9... | collective-permute-start | bytes 589832 | tf_op jit(solution)/shard_map/ppermute | solution.py:477
  36.1 0.9 collective-permute-start.5
  37.0 0.8 collective-permute-start.4
  37.7 1.8 %collective-permute-start.3 = (bf16[768,128]{1,0:T(8,128)(2,1)S(1)}, bf16[768,128]{1,0:T(8,128)(2,1)S(1)}, u32[]{:S(2)}, u32[]{:S(2)}) collective-permute-start(bf16[768,128]{1,0:T(8,128)(2,1)S(1)} %pad_maximum_fusion.refs_0_), channel_id=1, source_target_pairs={{0,4},{1,5},{2,6},{3,7},{4,0},{5,1},{6,2},{7,3},{8,12},{9,13},{10,... | collective-permute-start | bytes 589832 | tf_op jit(solution)/shard_map/ppermute | solution.py:477
  39.6 2.1 %collective-permute-start.2 = (bf16[768,128]{1,0:T(8,128)(2,1)S(1)}, bf16[768,128]{1,0:T(8,128)(2,1)}, u32[]{:S(2)}, u32[]{:S(2)}) collective-permute-start(bf16[768,128]{1,0:T(8,128)(2,1)S(1)} %pad_maximum_fusion.refs_0_), channel_id=1, source_target_pairs={{0,3},{1,4},{2,5},{3,6},{4,7},{5,0},{6,1},{7,2},{8,11},{9,12},{10,... | collective-permute-start | bytes 589832 | tf_op jit(solution)/shard_map/ppermute | solution.py:477
  41.7 0.0 collective-permute-done.6.refs_7_
  41.7 0.2 collective-permute-start.1
  41.9 1.1 %collective-permute-done.5.refs_6_ = bf16[768,128]{1,0:T(8,128)(2,1)S(1)} collective-permute-done((bf16[768,128]{1,0:T(8,128)(2,1)S(1)}, bf16[768,128]{1,0:T(8,128)(2,1)S(1)}, u32[]{:S(2)}, u32[]{:S(2)}) %collective-permute-start.5) | collective-permute-done | bytes 196640 | tf_op jit(solution)/shard_map/ppermute | solution.py:477
  43.0 3.4 %collective-permute-start = (bf16[768,128]{1,0:T(8,128)(2,1)S(1)}, bf16[768,128]{1,0:T(8,128)(2,1)}, u32[]{:S(2)}, u32[]{:S(2)}) collective-permute-start(bf16[768,128]{1,0:T(8,128)(2,1)S(1)} %pad_maximum_fusion.refs_0_), channel_id=1, source_target_pairs={{0,1},{1,2},{2,3},{3,4},{4,5},{5,6},{6,7},{7,0},{8,9},{9,10},{10,1... | collective-permute-start | bytes 589832 | tf_op jit(solution)/shard_map/ppermute | solution.py:477
  46.4 3.7 %all-to-all-done.1 = bf16[32,8,1024]{2,1,0:T(8,128)(2,1)S(1)} async-done(((bf16[32,8,1024]{2,1,0:T(8,128)(2,1)}), bf16[32,8,1024]{2,1,0:T(8,128)(2,1)S(1)}, u32[]{:S(2)}, u32[]{:S(2)}) %all-to-all-start.1) | async-done | bytes 524320 | tf_op jit(solution)/shard_map/all_to_all | solution.py:395
  50.1 0.0 copy-done.1
  50.1 0.4 picked.1.picked_ref
  50.6 0.0 collective-permute-done.4.refs_5_
  50.6 0.0 collective-permute-done.3.refs_4_
  50.6 3.5 %collective-permute-done.2.refs_3_ = bf16[768,128]{1,0:T(8,128)(2,1)} collective-permute-done((bf16[768,128]{1,0:T(8,128)(2,1)S(1)}, bf16[768,128]{1,0:T(8,128)(2,1)}, u32[]{:S(2)}, u32[]{:S(2)}) %collective-permute-start.2) | collective-permute-done | bytes 196640 | tf_op jit(solution)/shard_map/ppermute | solution.py:477
  54.1 0.5 collective-permute-done.1.refs_2_
  54.6 1.5 %collective-permute-done.refs_1_ = bf16[768,128]{1,0:T(8,128)(2,1)} collective-permute-done((bf16[768,128]{1,0:T(8,128)(2,1)S(1)}, bf16[768,128]{1,0:T(8,128)(2,1)}, u32[]{:S(2)}, u32[]{:S(2)}) %collective-permute-start) | collective-permute-done | bytes 196640 | tf_op jit(solution)/shard_map/ppermute | solution.py:477
  56.1 1.9 %dense.1 = bf16[32,8,8,128]{3,2,1,0:T(8,128)(2,1)S(1)} custom-call(s32[1]{0:T(128)} %bitcast.position_ref, bf16[256,1024]{1,0:T(8,128)(2,1)S(1)} %bitcast.18, bf16[256,128]{1,0:T(8,128)(2,1)S(1)} %picked.1.picked_ref, bf16[128,2048]{1,0:T(8,128)(2,1)S(1)} %bitcast.23, bf16[768,128]{1,0:T(8,128)(2,1)S(1)} %pad_maximum_fusion.refs_0_, ...), custom_call_target="tpu_custom_call" | custom-call | tf_op jit(solution)/shard_map/dense/pallas_call | solution.py:530
  58.1 33.6 %all_to_all.15 = bf16[256,8,128]{2,1,0:T(8,128)(2,1)S(1)} all-to-all(bf16[256,8,128]{2,1,0:T(8,128)(2,1)S(1)} %bitcast.20), channel_id=1, replica_groups=mesh['ep_0'=8,'ep_1'=4,'tp'=8] {'ep_0','ep_1','tp'}, dimensions={0} | all-to-all | bytes 1048576 | tf_op jit(solution)/shard_map/all_to_all | solution.py:395
  91.7 0.0 copy-done.3
  91.7 0.9 combine.1
  (14 shorter events, 0.0 us)
Async XLA Ops:
  0.0 23.1 %copy-start.4 = (bf16[16,2048]{1,0:T(8,128)(2,1)S(1)}, bf16[16,2048]{1,0:T(8,128)(2,1)}, u32[]{:S(2)}) copy-start(bf16[16,2048]{1,0:T(8,128)(2,1)} %tokens_ref.1) | copy-start | bytes 196612
  0.0 23.1 %copy-start.5 = (f32[2048]{0:T(1024)S(1)}, f32[2048]{0:T(1024)}, u32[]{:S(2)}) copy-start(f32[2048]{0:T(1024)} %param.35) | copy-start | bytes 24580
  0.0 23.1 %copy-start.6 = (f32[2048]{0:T(1024)S(1)}, f32[2048]{0:T(1024)}, u32[]{:S(2)}) copy-start(f32[2048]{0:T(1024)} %param.45) | copy-start | bytes 24580
  0.0 34.7 %copy-start.7 = (bf16[128,256]{1,0:T(8,128)(2,1)S(1)}, bf16[128,256]{1,0:T(8,128)(2,1)}, u32[]{:S(2)}) copy-start(bf16[128,256]{1,0:T(8,128)(2,1)} %param.44) | copy-start | bytes 196612
  0.0 34.8 %copy-start.8 = (bf16[256,128]{1,0:T(8,128)(2,1)S(1)}, bf16[256,128]{1,0:T(8,128)(2,1)}, u32[]{:S(2)}) copy-start(bf16[256,128]{1,0:T(8,128)(2,1)} %param.43) | copy-start | bytes 196612
  0.0 34.8 %copy-start.9 = (bf16[256,128]{1,0:T(8,128)(2,1)S(1)}, bf16[256,128]{1,0:T(8,128)(2,1)}, u32[]{:S(2)}) copy-start(bf16[256,128]{1,0:T(8,128)(2,1)} %param.42) | copy-start | bytes 196612
  0.0 50.1 %copy-start = (bf16[1,2048,128]{2,1,0:T(8,128)(2,1)S(1)}, bf16[1,2048,128]{2,1,0:T(8,128)(2,1)}, u32[]{:S(2)}) copy-start(bf16[1,2048,128]{2,1,0:T(8,128)(2,1)} %param.39) | copy-start | bytes 1572868
  0.0 50.1 %copy-start.1 = (bf16[1,2048,128]{2,1,0:T(8,128)(2,1)S(1)}, bf16[1,2048,128]{2,1,0:T(8,128)(2,1)}, u32[]{:S(2)}) copy-start(bf16[1,2048,128]{2,1,0:T(8,128)(2,1)} %param.40) | copy-start | bytes 1572868
  6.6 49.5 %copy-start.2 = (bf16[1,128,2048]{2,1,0:T(8,128)(2,1)S(1)}, bf16[1,128,2048]{2,1,0:T(8,128)(2,1)}, u32[]{:S(2)}) copy-start(bf16[1,128,2048]{2,1,0:T(8,128)(2,1)} %param.41) | copy-start | bytes 1572868
  6.6 16.5 %all-to-all-start = ((bf16[8,16,2176]{2,1,0:T(8,128)(2,1)}), bf16[8,16,2176]{2,1,0:T(8,128)(2,1)S(1)}, u32[]{:S(2)}, u32[]{:S(2)}) async-start(bf16[8,16,2176]{2,1,0:T(8,128)(2,1)} %get-tuple-element.10), calls=%async_computation | async-start | bytes 1114112 | tf_op jit(solution)/shard_map/all_to_all | solution.py:395
  13.3 78.3 %copy-start.3 = (bf16[96,2048]{1,0:T(8,128)(2,1)S(1)}, bf16[96,2048]{1,0:T(8,128)(2,1)}, u32[]{:S(2)}) copy-start(bf16[96,2048]{1,0:T(8,128)(2,1)} %get-tuple-element.12.table_ref) | copy-start | bytes 1179652
  24.4 25.7 %all-to-all-start.1 = ((bf16[32,8,1024]{2,1,0:T(8,128)(2,1)}), bf16[32,8,1024]{2,1,0:T(8,128)(2,1)S(1)}, u32[]{:S(2)}, u32[]{:S(2)}) async-start(bf16[32,8,1024]{2,1,0:T(8,128)(2,1)} %bitcast.10), calls=%async_computation.1 | async-start | bytes 1048576 | tf_op jit(solution)/shard_map/all_to_all | solution.py:395
  34.8 6.9 %collective-permute-start.6 = (bf16[768,128]{1,0:T(8,128)(2,1)S(1)}, bf16[768,128]{1,0:T(8,128)(2,1)S(1)}, u32[]{:S(2)}, u32[]{:S(2)}) collective-permute-start(bf16[768,128]{1,0:T(8,128)(2,1)S(1)} %pad_maximum_fusion.refs_0_), channel_id=1, source_target_pairs={{0,7},{1,0},{2,1},{3,2},{4,3},{5,4},{6,5},{7,6},{8,15},{9,8},{10,9... | collective-permute-start | bytes 589832 | tf_op jit(solution)/shard_map/ppermute | solution.py:477
  36.1 6.9 %collective-permute-start.5 = (bf16[768,128]{1,0:T(8,128)(2,1)S(1)}, bf16[768,128]{1,0:T(8,128)(2,1)S(1)}, u32[]{:S(2)}, u32[]{:S(2)}) collective-permute-start(bf16[768,128]{1,0:T(8,128)(2,1)S(1)} %pad_maximum_fusion.refs_0_), channel_id=1, source_target_pairs={{0,6},{1,7},{2,0},{3,1},{4,2},{5,3},{6,4},{7,5},{8,14},{9,15},{10,... | collective-permute-start | bytes 589832 | tf_op jit(solution)/shard_map/ppermute | solution.py:477
  37.0 13.6 %collective-permute-start.4 = (bf16[768,128]{1,0:T(8,128)(2,1)S(1)}, bf16[768,128]{1,0:T(8,128)(2,1)S(1)}, u32[]{:S(2)}, u32[]{:S(2)}) collective-permute-start(bf16[768,128]{1,0:T(8,128)(2,1)S(1)} %pad_maximum_fusion.refs_0_), channel_id=1, source_target_pairs={{0,5},{1,6},{2,7},{3,0},{4,1},{5,2},{6,3},{7,4},{8,13},{9,14},{10,... | collective-permute-start | bytes 589832 | tf_op jit(solution)/shard_map/ppermute | solution.py:477
  37.7 12.8 %collective-permute-start.3 = (bf16[768,128]{1,0:T(8,128)(2,1)S(1)}, bf16[768,128]{1,0:T(8,128)(2,1)S(1)}, u32[]{:S(2)}, u32[]{:S(2)}) collective-permute-start(bf16[768,128]{1,0:T(8,128)(2,1)S(1)} %pad_maximum_fusion.refs_0_), channel_id=1, source_target_pairs={{0,4},{1,5},{2,6},{3,7},{4,0},{5,1},{6,2},{7,3},{8,12},{9,13},{10,... | collective-permute-start | bytes 589832 | tf_op jit(solution)/shard_map/ppermute | solution.py:477
  39.6 14.5 %collective-permute-start.2 = (bf16[768,128]{1,0:T(8,128)(2,1)S(1)}, bf16[768,128]{1,0:T(8,128)(2,1)}, u32[]{:S(2)}, u32[]{:S(2)}) collective-permute-start(bf16[768,128]{1,0:T(8,128)(2,1)S(1)} %pad_maximum_fusion.refs_0_), channel_id=1, source_target_pairs={{0,3},{1,4},{2,5},{3,6},{4,7},{5,0},{6,1},{7,2},{8,11},{9,12},{10,... | collective-permute-start | bytes 589832 | tf_op jit(solution)/shard_map/ppermute | solution.py:477
  41.7 12.9 %collective-permute-start.1 = (bf16[768,128]{1,0:T(8,128)(2,1)S(1)}, bf16[768,128]{1,0:T(8,128)(2,1)}, u32[]{:S(2)}, u32[]{:S(2)}) collective-permute-start(bf16[768,128]{1,0:T(8,128)(2,1)S(1)} %pad_maximum_fusion.refs_0_), channel_id=1, source_target_pairs={{0,2},{1,3},{2,4},{3,5},{4,6},{5,7},{6,0},{7,1},{8,10},{9,11},{10,... | collective-permute-start | bytes 589832 | tf_op jit(solution)/shard_map/ppermute | solution.py:477
  43.0 13.1 %collective-permute-start = (bf16[768,128]{1,0:T(8,128)(2,1)S(1)}, bf16[768,128]{1,0:T(8,128)(2,1)}, u32[]{:S(2)}, u32[]{:S(2)}) collective-permute-start(bf16[768,128]{1,0:T(8,128)(2,1)S(1)} %pad_maximum_fusion.refs_0_), channel_id=1, source_target_pairs={{0,1},{1,2},{2,3},{3,4},{4,5},{5,6},{6,7},{7,0},{8,9},{9,10},{10,1... | collective-permute-start | bytes 589832 | tf_op jit(solution)/shard_map/ppermute | solution.py:477

commit v4 on v3

--- a/solution.py
+++ b/solution.py
@@ -9,6 +9,7 @@
 EXPERTS_PER_GROUP = 8
 EXPERTS = 32
 EP = ("ep_0", "ep_1")
+TP = ("y", "core")
 EPS = 1e-06
 F32 = jnp.float32
 BF16 = jnp.bfloat16
@@ -49,7 +50,7 @@
     key_hbm,
     value_hbm,
     parts_ref,
-    table_ref,
+    table_hbm,
     tokens_ref,
     gain_ref,
     forget_ref,
@@ -59,6 +60,7 @@
     group_ref,
     slot_ref,
     route_weight_ref,
+    table_ref,
     wqkv,
     wo,
     keys,
@@ -144,6 +146,8 @@
     ]
     place_columns = routing_places(group_ref[...] * EXPERTS_PER_GROUP + slot_ref[...])
     combine_table(place_columns, route_weight_ref[...], table_ref)
+    table_copy = pltpu.make_async_copy(table_ref, table_hbm, w_sems.at[4])
+    table_copy.start()
     tail = jnp.zeros((seqs, width), F32)
     for k, place in enumerate(place_columns):
         tail = tail + jnp.where(lane == k, place.astype(F32), 0.0)
@@ -186,6 +190,7 @@
                 mine = result[heads * i : heads * i + heads, i * width : (i + 1) * width]
                 weighted[s + i : s + i + 1] = jnp.where(first_head, mine[0:1], mine[1:2])
     output_copy.wait()
+    table_copy.wait()
     own_weight = own_weight.astype(BF16).astype(F32)
     own_weight = jnp.where(first_head, own_weight[:seqs], own_weight[seqs:])
     denominator = jnp.where(first_head, denominator[:seqs], denominator[seqs:])
@@ -223,17 +228,17 @@
 
 def select_table(place_rows, position, rows):
     seqs = place_rows[0].shape[1]
-    row = lax.broadcasted_iota(jnp.int32, (rows, 2 * seqs), 0)
-    column = lax.broadcasted_iota(jnp.int32, (rows, 2 * seqs), 1)
-    slot = row & 3
-    row_place = (row & ~7) + slot
+    row = lax.broadcasted_iota(jnp.int32, (rows, 4 * seqs), 0)
+    column = lax.broadcasted_iota(jnp.int32, (rows, 4 * seqs), 1)
+    expert = row >> 3
+    is_dense = (row & 1) == 1
     token = column & (seqs - 1)
-    hit = (slot >= 2) & (token == position * 2 + slot - 2)
+    hit = is_dense & (token == position * 2 + (expert & 1))
     for place in place_rows:
-        places = jnp.concatenate([place, place], axis=1)
-        hit = hit | ((slot < 2) & (places == row_place))
-    same_half = ((row >> 2) & 1) == (column >= seqs).astype(jnp.int32)
-    return jnp.where(hit & same_half, 1.0, 0.0).astype(BF16)
+        places = jnp.concatenate([place] * 4, axis=1)
+        hit = hit | (jnp.logical_not(is_dense) & (places == expert * 8 + (position & 1)))
+    same_quarter = ((row >> 1) & 3) == column // seqs
+    return jnp.where(hit & same_quarter, 1.0, 0.0).astype(BF16)
 
 
 def combine_table(place_columns, weight_rows, table_ref):
@@ -241,22 +246,22 @@
     wide = table_ref.shape[1]
     row = lax.broadcasted_iota(jnp.int32, (2 * seqs, wide), 0)
     column = lax.broadcasted_iota(jnp.int32, (2 * seqs, wide), 1)
-    slot = column & 3
-    source = (column >> 3) & 7
-    expert_place = ((column >> 6) << 3) + slot
+    is_dense = (column & 1) == 1
+    core = (column >> 1) & 1
+    chip = (column >> 3) & 3
+    expert = column >> 5
     same_half = ((column >> 2) & 1) == (row >= seqs).astype(jnp.int32)
     weight = jnp.zeros((2 * seqs, wide), F32)
     for k, place in enumerate(place_columns):
         places = jnp.concatenate([place, place], axis=0)
         value = column_of(weight_rows[k : k + 1])
         value = jnp.concatenate([value, value], axis=0)
-        weight = weight + jnp.where(
-            same_half & (slot < 2) & (places == expert_place), value, 0.0
-        )
+        hit = same_half & jnp.logical_not(is_dense) & (places == expert * 8 + core)
+        weight = weight + jnp.where(hit, value, 0.0)
     high = weight.astype(BF16)
     table_ref[0 : 2 * seqs] = high
     table_ref[2 * seqs : 4 * seqs] = (weight - high.astype(F32)).astype(BF16)
-    dense = same_half & (slot >= 2) & ((row & (seqs - 1)) == source * 2 + slot - 2)
+    dense = same_half & is_dense & ((row & (seqs - 1)) == chip * 4 + core * 2 + (expert & 1))
     table_ref[4 * seqs : 6 * seqs] = jnp.where(dense, 1.0, 0.0).astype(BF16)
 
 
@@ -271,7 +276,7 @@
     mix_gate_ref,
     scratch,
 ):
-    half = out_ref.shape[1]
+    quarter = out_ref.shape[1]
     width = residual_ref.shape[1]
     model_width = tokens_ref.shape[1]
     seqs = tokens_ref.shape[0]
@@ -292,90 +297,102 @@
     residual = tokens_ref[...].astype(F32) + attn
     scratch[...] = residual
     normed = rms_scale(residual, gain_ref[...]).astype(BF16)
-    both = jnp.concatenate([normed[:, :half], normed[:, half:]], axis=0)
+    quarters = jnp.concatenate(
+        [normed[:, q * quarter : (q + 1) * quarter] for q in range(4)], axis=0
+    )
     mix_gate_ref[...] = jax.nn.sigmoid(
         jnp.sum(normed.astype(F32) * mix_ref[...], axis=1, keepdims=True)
     )
     mine = pl.ds(pl.multiple_of(position_ref[0] * width, width), width)
     residual_ref[...] = scratch[:, mine]
-    out_ref[...] = jnp.dot(select, both, preferred_element_type=F32).astype(BF16)
-
-
-def row_kinds(rows):
-    row = lax.broadcasted_iota(jnp.int32, (rows, 1), 0)
-    return lax.rem(row, 8) >= 4, lax.rem(row, 4) >= 2
-
-
-def whole_rows(both):
-    rows, width = both.shape
-    both = both.reshape(rows // 8, 8, width)
-    return (both + pltpu.roll(both, 4, 1)).reshape(rows, width)
-
-
-def picked_kernel(rows_ref, gate_ref, up_ref, hidden_ref):
-    rows, half = rows_ref.shape
-    width = gate_ref.shape[1]
-    second, is_dense = row_kinds(rows)
-    sums = []
-    for h in range(2):
-        weights = jnp.concatenate(
-            [gate_ref[h * half : (h + 1) * half], up_ref[h * half : (h + 1) * half]], axis=1
-        )
-        sums.append(jnp.dot(rows_ref[...], weights, preferred_element_type=F32))
-    both = whole_rows(jnp.where(second, sums[1], sums[0]))
-    hidden = silu(both[:, :width]) * both[:, width:]
-    hidden_ref[...] = jnp.where(is_dense, 0.0, hidden).astype(BF16)
-
-
-LATE = (1, 2, 3, 4)
-
-
-def dense_kernel(position_ref, rows_ref, picked_ref, down_ref, *refs):
-    out_ref, late, sems = refs[-3:]
-    operands = refs[:-3]
-    blocks = len(operands)
+    out_ref[...] = jnp.dot(select, quarters, preferred_element_type=F32).astype(BF16)
+
+
+def whole_rows(parts):
+    rows, width = parts.shape
+    parts = parts.reshape(rows // 8, 8, width)
+    parts = parts + pltpu.roll(parts, 4, 1)
+    return (parts + pltpu.roll(parts, 2, 1)).reshape(rows, width)
+
+
+def mark_kernel(rows_hbm, mark_ref):
+    mark_ref[...] = jnp.zeros_like(mark_ref)
+
+
+LATE = (2, 3)
+
+
+def expert_kernel(position_ref, own_ref, other_ref, gate_ref, up_ref, down_ref, *refs):
+    keep_ref, send_ref, late, left, sems = refs[-5:]
+    operands = refs[:-5]
+    blocks = 2 * len(operands)
     copies = [
         pltpu.make_async_copy(operands[k], late.at[i], sems.at[i]) for i, k in enumerate(LATE)
     ]
     for copy in copies:
         copy.start()
-    pieces = {k: operands[k] for k in range(blocks) if k not in LATE}
-    pieces.update({k: late.at[i] for i, k in enumerate(LATE)})
-    rows, half = rows_ref.shape
+    pairs = {k: operands[k] for k in range(len(operands)) if k not in LATE}
+    pairs.update({k: late.at[i] for i, k in enumerate(LATE)})
+    size = late.shape[1] // 2
+    pieces = {
+        2 * k + i: ref.at[pl.ds(i * size, size)] for k, ref in pairs.items() for i in range(2)
+    }
+    rows, quarter = own_ref.shape
     width = late.shape[2]
-    per_half = blocks // 2
-    kb = half // per_half
+    kb = 4 * quarter // blocks
     position = position_ref[0]
-    second, is_dense = row_kinds(rows)
+    core = position & 1
+    row = lax.broadcasted_iota(jnp.int32, (rows, 1), 0)
+    for i, ref in enumerate((own_ref, other_ref)):
+        values = ref[...].astype(F32)
+        for q in range(4):
+            mine = jnp.where(((row >> 1) & 3) == q, values, 0.0)
+            left[i * rows : (i + 1) * rows, q * quarter : (q + 1) * quarter] = mine.astype(BF16)
+    both = jnp.dot(
+        left[...],
+        jnp.concatenate([gate_ref[...], up_ref[...]], axis=1),
+        preferred_element_type=F32,
+    )
+    both = whole_rows(both)
+    row2 = lax.broadcasted_iota(jnp.int32, (2 * rows, 1), 0)
+    is_dense = (row2 & 1) == 1
+    picked = jnp.where(is_dense, 0.0, silu(both[:, :width]) * both[:, width:]).astype(BF16)
     both = None
     for k, piece in pieces.items():
-        if k == LATE[0]:
+        if k == 2 * LATE[0]:
             for copy in copies:
                 copy.wait()
-        t = lax.rem(position - k + blocks, blocks)
-        inner = pl.ds(pl.multiple_of(lax.rem(t, per_half) * kb, kb), kb)
+        inner = pl.ds(pl.multiple_of((position ^ k) * kb, kb), kb)
         weights = jnp.concatenate([piece[0:kb], piece[kb : 2 * kb]], axis=1)
-        part = jnp.dot(rows_ref[:, inner], weights, preferred_element_type=F32)
-        part = jnp.where(second == (t >= per_half), part, 0.0)
+        part = jnp.dot(left[:, inner], weights, preferred_element_type=F32)
         both = part if both is None else both + part
     both = whole_rows(both)
-    hidden = silu(both[:, :width]) * both[:, width:]
-    hidden = jnp.concatenate(
-        [picked_ref[...], jnp.where(is_dense, hidden, 0.0).astype(BF16)], axis=1
-    )
+    hidden = jnp.where(is_dense, silu(both[:, :width]) * both[:, width:], 0.0).astype(BF16)
+    hidden = jnp.concatenate([picked, hidden], axis=1)
+    right = ((row >> 2) & 1) == 1
+    is_own = ((row >> 1) & 1) == core
     for k, piece in pieces.items():
-        t = lax.rem(position - k + blocks, blocks)
+        t = position ^ k
         dense_down = jnp.concatenate(
             [piece[2 * kb : 2 * kb + width], piece[2 * kb + width : 2 * kb + 2 * width]], axis=1
         )
         whole = pl.ds(pl.multiple_of(t * kb, kb), kb)
         down = jnp.concatenate([down_ref[:, whole], dense_down], axis=0)
         result = jnp.dot(hidden, down, preferred_element_type=F32)
-        result = jnp.where(second, result[:, width:], result[:, :width]).astype(BF16)
-        out_ref[:, t] = result.reshape(rows // 8, 8, width)
-
-
-def combine_kernel(rows_ref, table_ref, mix_ref, residual_ref, out_ref):
+        result = jnp.where(is_own, result[:rows], result[rows:])
+        result = jnp.where(right, result[:, width:], result[:, :width])
+        result = result.reshape(rows // 8, 8, width)
+        if k % 2 == 0:
+            keep_ref[:, t >> 1] = result
+        else:
+            send_ref[:, t >> 1] = result.astype(BF16)
+
+
+def add_kernel(keep_ref, got_ref, out_ref):
+    out_ref[...] = (keep_ref[...] + got_ref[...].astype(F32)).astype(BF16)
+
+
+def combine_kernel(rows_ref, table_ref, mix_ref, residual_ref, mark_ref, out_ref):
     seqs = mix_ref.shape[0]
     width = rows_ref.shape[1]
     sums = jnp.dot(table_ref[...], rows_ref[...], preferred_element_type=F32)
@@ -405,10 +422,10 @@
         name="attention",
         out_shape=(
             jax.ShapeDtypeStruct((tp_count, seqs, model_width + head_width), BF16),
-            jax.ShapeDtypeStruct((6 * seqs, EXPERTS * 8 * tp_count), BF16),
+            jax.ShapeDtypeStruct((6 * seqs, EXPERTS * 4 * tp_count), BF16),
         ),
         in_specs=[ANY] * 15,
-        out_specs=(VMEM, VMEM),
+        out_specs=(VMEM, ANY),
         scratch_shapes=[
             pltpu.VMEM((seqs, model_width), BF16),
             pltpu.VMEM((1, model_width), F32),
@@ -419,6 +436,7 @@
             pltpu.VMEM((1, seqs), jnp.int32),
             pltpu.VMEM((2, seqs), jnp.int32),
             pltpu.VMEM((2, seqs), F32),
+            pltpu.VMEM((6 * seqs, EXPERTS * 4 * tp_count), BF16),
             pltpu.VMEM((3, model_width, head_width), BF16),
             pltpu.VMEM((head_width, model_width), BF16),
             pltpu.VMEM((seqs, cache_len, head_width), BF16),
@@ -426,7 +444,7 @@
             pltpu.VMEM((2 * seqs, cache_len), F32),
             pltpu.VMEM((seqs, head_width), F32),
             pltpu.SemaphoreType.DMA((9,)),
-            pltpu.SemaphoreType.DMA((4,)),
+            pltpu.SemaphoreType.DMA((5,)),
             pltpu.SemaphoreType.DMA((16,)),
             pltpu.SemaphoreType.DMA((16,)),
         ],
@@ -462,20 +480,28 @@
 ):
     seqs, model_width = tokens.shape
     ep_count = lax.axis_size(EP)
-    tp_count = lax.axis_size("tp")
-    tp_position = lax.axis_index("tp")
+    tp_count = lax.axis_size(TP)
+    tp_position = lax.axis_index(TP)
     width_local = model_width // tp_count
-    half = model_width // 2
     head_width = key_cache.shape[2]
 
     own_dense = jnp.concatenate(
         [dense_gate, dense_up, dense_down[:, :head_width], dense_down[:, head_width:]], axis=0
     )
-    dense_weights = [own_dense]
-    for k in range(1, tp_count):
-        dense_weights.append(
-            lax.ppermute(own_dense, "tp", [(i, (i + k) % tp_count) for i in range(tp_count)])
-        )
+    ep_1 = lax.axis_size("ep_1")
+    same, cross = [], []
+    for e in range(ep_1):
+        same += [(2 * e, 2 * e), (2 * e + 1, 2 * (e ^ 1) + 1)]
+        cross += [(2 * e + 1, 2 * e), (2 * e, 2 * (e ^ 1) + 1)]
+    first = []
+    for route in (same, cross):
+        first.append(lax.ppermute(own_dense, ("ep_1", "core"), route))
+    pair = jnp.concatenate(first, axis=0)
+    dense_weights = [pair]
+    chips = lax.axis_size("y")
+    for k in range(1, chips):
+        dense_weights.append(lax.ppermute(pair, "y", [(i, i ^ k) for i in range(chips)]))
+    sibling = [(0, 1), (1, 0)]
     parts, table = attention_call(
         tokens,
         norm_attn.reshape(1, -1),
@@ -493,16 +519,16 @@
         key_cache,
         value_cache,
     )
-    parts = exchange(parts, "tp")
+    parts = exchange(parts, TP)
 
     position = tp_position.reshape(1)
     row_count = ep_count * 8
-    wide = row_count * tp_count
+    wide = row_count * tp_count // 2
     dispatch = pl.pallas_call(
         dispatch_kernel,
         name="dispatch",
         out_shape=(
-            jax.ShapeDtypeStruct((row_count, half), BF16),
+            jax.ShapeDtypeStruct((row_count, model_width // 4), BF16),
             jax.ShapeDtypeStruct((seqs, width_local), F32),
             jax.ShapeDtypeStruct((seqs, 1), F32),
         ),
@@ -518,70 +544,82 @@
         norm_ffn.reshape(1, -1),
         mix_vector.reshape(1, -1),
     )
-    arrived = exchange(outgoing.reshape(ep_count, 8, half), EP).reshape(row_count, half)
-    hidden = pl.pallas_call(
-        picked_kernel,
-        name="picked",
-        out_shape=jax.ShapeDtypeStruct((row_count, head_width), BF16),
-        in_specs=[VMEM] * 3,
+    arrived = exchange(outgoing.reshape(ep_count, 8, -1), EP).reshape(row_count, -1)
+    mark = pl.pallas_call(
+        mark_kernel,
+        name="mark",
+        out_shape=jax.ShapeDtypeStruct((8, 128), F32),
+        in_specs=[ANY],
         out_specs=VMEM,
         compiler_params=limits(8),
-    )(arrived, expert_gate[0], expert_up[0])
-    results = pl.pallas_call(
-        dense_kernel,
-        name="dense",
-        out_shape=jax.ShapeDtypeStruct((ep_count, tp_count, 8, width_local // 2), BF16),
-        in_specs=[SMEM] + [VMEM] * 3 + [ANY if k in LATE else VMEM for k in range(tp_count)],
-        out_specs=VMEM,
+    )(arrived)
+    other = lax.ppermute(arrived, "core", sibling)
+    blocks = (ep_count, tp_count // 2, 8, width_local // 2)
+    keep, send = pl.pallas_call(
+        expert_kernel,
+        name="experts",
+        out_shape=(jax.ShapeDtypeStruct(blocks, F32), jax.ShapeDtypeStruct(blocks, BF16)),
+        in_specs=[SMEM] + [VMEM] * 5 + [ANY if k in LATE else VMEM for k in range(chips)],
+        out_specs=(VMEM, VMEM),
         scratch_shapes=[
-            pltpu.VMEM((len(LATE), *own_dense.shape), BF16),
+            pltpu.VMEM((len(LATE), *pair.shape), BF16),
+            pltpu.VMEM((2 * row_count, model_width), BF16),
             pltpu.SemaphoreType.DMA((len(LATE),)),
         ],
+        compiler_params=limits(16),
+    )(position, arrived, other, expert_gate[0], expert_up[0], expert_down[0], *dense_weights)
+    got = lax.ppermute(send, "core", sibling)
+    results = pl.pallas_call(
+        add_kernel,
+        name="add",
+        out_shape=jax.ShapeDtypeStruct(blocks, BF16),
+        in_specs=[VMEM] * 2,
+        out_specs=VMEM,
         compiler_params=limits(8),
-    )(position, arrived, hidden, expert_down[0], *dense_weights)
+    )(keep, got)
     returned = exchange(
-        results.reshape(ep_count * tp_count, 8, width_local // 2), (*EP, "tp")
+        results.reshape(ep_count * tp_count // 2, 8, width_local // 2), (*EP, "y")
     ).reshape(wide, width_local // 2)
     return pl.pallas_call(
         combine_kernel,
         name="combine",
         out_shape=jax.ShapeDtypeStruct((seqs, width_local), BF16),
-        in_specs=[VMEM] * 4,
+        in_specs=[VMEM] * 4 + [ANY],
         out_specs=VMEM,
         compiler_params=limits(8),
-    )(returned, table, mix_gate, residual)
+    )(returned, table, mix_gate, residual, mark)
 
 
 def solution(mesh):
-    split = Mesh(mesh.devices.reshape(8, 4, mesh.shape["tp"]), ("ep_0", "ep_1", "tp"))
+    split = Mesh(mesh.devices.reshape(8, 4, 4, 2), ("ep_0", "ep_1", "y", "core"))
     return jax.shard_map(
         body,
         mesh=split,
         in_specs=(
             P(EP, None),
             P(),
-            P(None, "tp"),
-            P(None, "tp"),
-            P(None, "tp"),
-            P(None, "tp"),
-            P("tp"),
-            P("tp", None),
-            P(EP, None, "tp"),
-            P(EP, None, "tp"),
-            P(EP, "tp", None),
+            P(None, TP),
+            P(None, TP),
+            P(None, TP),
+            P(None, TP),
+            P(TP),
+            P(TP, None),
+            P(EP, None, TP),
+            P(EP, None, TP),
+            P(EP, TP, None),
             P(EP),
             P(),
             P(EP),
             P(EP, None),
             P(EP, None),
-            P(EP, None, "tp"),
-            P(EP, None, "tp"),
-            P(EP, "tp", None),
-            P("tp", EP),
-            P("tp", EP),
-            P(EP, "tp"),
+            P(EP, None, TP),
+            P(EP, None, TP),
+            P(EP, TP, None),
+            P(TP, EP),
+            P(TP, EP),
+            P(EP, TP),
             P(),
         ),
-        out_specs=P(EP, "tp"),
+        out_specs=P(EP, TP),
         check_vma=False,
     )

time: 92.8 us -> 99 us (1.067)
  blocking collectives: 33.6 us -> 0 us
  waiting for transfers between devices: 20 us -> 45.3 us
  starting transfers between devices: 27.6 us -> 39.8 us
  Pallas kernels: 11 us -> 12.3 us
    all_to_all x1 -> x0, blocking collectives: 33.6 us -> none  [exchange(): return lax.all_to_all(array, axis, 0, 0, tiled=True)]
    ppermute x7, waiting for transfers between devices: 6.61 us -> 24.4 us  [the longest x3 16.3 us: body(): lax.ppermute(pair, 'y', [(i, i ^ k) for i in range(chips)])]
    all_to_all x2 -> x3, starting transfers between devices: 17.1 us -> 30.3 us  [exchange(): return lax.all_to_all(array, axis, 0, 0, tiled=True)]
    all_to_all x2 -> x3, waiting for transfers between devices: 13.4 us -> 20.9 us  [exchange(): return lax.all_to_all(array, axis, 0, 0, tiled=True)]
    pallas_call x2 -> x3, Pallas kernels: 2.37 us -> 3.83 us  [the longest x1 3.08 us: body(): pl.pallas_call(expert_kernel, name='experts', out_shape=(jax.ShapeDtypeSt...]
    ppermute x7, starting transfers between devices: 10.5 us -> 9.52 us  [the longest x3 3.95 us: body(): lax.ppermute(pair, 'y', [(i, i ^ k) for i in range(chips)])]
  transfers between devices with their start and end apart: 9 -> 10, of which waited for: 6 -> 7; matrix products, arithmetic and copies ran while one was open for 0% -> 0% of each run, Pallas kernels for 0% -> 1%
where the time goes in v4:
time: 99 us; the launch traced here: 98.6 us
  waiting for transfers between devices  45.3 us (46%)
  starting transfers between devices  39.8 us (40%)
  Pallas kernels  12.3 us (12%)
  local copies, waits for them, and re-layouts  1.01 us (1%)
    all_to_all x3, starting transfers between devices, exchange(): return lax.all_to_all(array, axis, 0, 0, tiled=True)  30.3 us
    all_to_all x3, waiting for transfers between devices, exchange(): return lax.all_to_all(array, axis, 0, 0, tiled=True)  20.9 us
    ppermute x3, waiting for transfers between devices, body(): lax.ppermute(pair, 'y', [(i, i ^ k) for i in range(chips)])  16.3 us
    ppermute x2, waiting for transfers between devices, body(): first.append(lax.ppermute(own_dense, ('ep_1', 'core'), route))  6.61 us
    pallas_call x1, Pallas kernels, attention_call(): pl.pallas_call(attention_kernel, name='attention', out_shape=(jax.ShapeDt...  6.52 us
    ppermute x3, starting transfers between devices, body(): lax.ppermute(pair, 'y', [(i, i ^ k) for i in range(chips)])  3.95 us
    ppermute x2, starting transfers between devices, body(): first.append(lax.ppermute(own_dense, ('ep_1', 'core'), route))  3.78 us
    pallas_call x1, Pallas kernels, body(): pl.pallas_call(expert_kernel, name='experts', out_shape=(jax.ShapeDtypeSt...  3.08 us
  transfers between devices with their start and end apart: 10, of which 7 were waited for; matrix products, arithmetic and copies ran while one was open for 0% of the time, Pallas kernels for 1%

profile of v4, /device:TPU:1, one launch (start us, length us, event | category | flops | bytes accessed | tf_op | source)
XLA Modules:
  0.0 98.6 jit_solution(15185992920993897638)
XLA Ops:
  0.0 0.0 copy-start.3
  0.0 0.0 copy-start.5
  0.0 0.0 copy-start.6
  0.0 0.0 copy-start
  0.1 6.5 %attention.1 = (bf16[8,16,2176]{2,1,0:T(8,128)(2,1)}, bf16[96,1024]{1,0:T(8,128)(2,1)}) custom-call(bf16[16,2048]{1,0:T(8,128)(2,1)} %tokens_ref.1, f32[1,2048]{1,0:T(1,128)} %bitcast.26, bf16[2,2048]{1,0:T(2,128)(2,1)} %bitcast.27, f32[1,2]{1,0:T(1,128)} %bitcast.30, f32[16,2,1024]{2,1,0:T(2,128)} %gate_hbm.1, s32[1,16]{1,0:T(1,128)} %bitcast.31, ...), custom_call_target="tpu_custom_call" | custom-call | flops 1000000000 | bytes 12582912 | tf_op jit(solution)/shard_map/attention/pallas_call | solution.py:420
  6.6 6.6 %all-to-all-start = ((bf16[8,16,2176]{2,1,0:T(8,128)(2,1)}), bf16[8,16,2176]{2,1,0:T(8,128)(2,1)S(1)}, u32[]{:S(2)}, u32[]{:S(2)}) async-start(bf16[8,16,2176]{2,1,0:T(8,128)(2,1)} %get-tuple-element.12), calls=%async_computation | async-start | bytes 1114112 | tf_op jit(solution)/shard_map/all_to_all | solution.py:412
  13.3 2.5 %collective-permute-start.1 = (bf16[768,128]{1,0:T(8,128)(2,1)S(1)}, bf16[768,128]{1,0:T(8,128)(2,1)S(1)}, u32[]{:S(2)}, u32[]{:S(2)}) collective-permute-start(bf16[768,128]{1,0:T(8,128)(2,1)S(1)} %pad_maximum_fusion), channel_id=1, source_target_pairs={{0,0},{1,9},{8,8},{9,1},{16,16},{17,25},{24,24},{25,17},{2,2},{3,1... | collective-permute-start | bytes 589832 | tf_op jit(solution)/shard_map/ppermute | solution.py:498
  15.8 7.2 %all-to-all-done.parts_ref = bf16[8,16,2176]{2,1,0:T(8,128)(2,1)S(1)} async-done(((bf16[8,16,2176]{2,1,0:T(8,128)(2,1)}), bf16[8,16,2176]{2,1,0:T(8,128)(2,1)S(1)}, u32[]{:S(2)}, u32[]{:S(2)}) %all-to-all-start) | async-done | bytes 557088 | tf_op jit(solution)/shard_map/all_to_all | solution.py:412
  23.0 1.1 %dispatch.1 = (bf16[256,512]{1,0:T(8,128)(2,1)}, f32[16,256]{1,0:T(8,128)S(1)}, f32[16,1]{1,0:T(8,128)S(1)}) custom-call(s32[1]{0:T(128)} %bitcast.position_ref, bf16[8,16,2176]{2,1,0:T(8,128)(2,1)S(1)} %all-to-all-done.parts_ref, bf16[16,2048]{1,0:T(8,128)(2,1)S(1)} %copy-done.3, f32[1,2048]{1,0:T(1,128)S(1)} %bitcast.24, f32[1,2048]{1,0:T(1,128)S(1)} %bitcast.25), custom_call_target="tpu_custom_call" | custom-call | tf_op jit(solution)/shard_map/dispatch/pallas_call | solution.py:540
  24.1 10.3 %all-to-all-start.1 = ((bf16[32,8,512]{2,1,0:T(8,128)(2,1)}), bf16[32,8,512]{2,1,0:T(8,128)(2,1)S(1)}, u32[]{:S(2)}, u32[]{:S(2)}) async-start(bf16[32,8,512]{2,1,0:T(8,128)(2,1)} %bitcast.10), calls=%async_computation.1 | async-start | bytes 524288 | tf_op jit(solution)/shard_map/all_to_all | solution.py:412
  34.5 1.3 %collective-permute-start.2 = (bf16[768,128]{1,0:T(8,128)(2,1)S(1)}, bf16[768,128]{1,0:T(8,128)(2,1)S(1)}, u32[]{:S(2)}, u32[]{:S(2)}) collective-permute-start(bf16[768,128]{1,0:T(8,128)(2,1)S(1)} %pad_maximum_fusion), channel_id=1, source_target_pairs={{1,0},{0,9},{9,8},{8,1},{17,16},{16,25},{25,24},{24,17},{3,2},{2,1... | collective-permute-start | bytes 589832 | tf_op jit(solution)/shard_map/ppermute | solution.py:498
  35.8 0.0 collective-permute-done.1
  35.8 6.6 %collective-permute-done.2 = bf16[768,128]{1,0:T(8,128)(2,1)S(1)} collective-permute-done((bf16[768,128]{1,0:T(8,128)(2,1)S(1)}, bf16[768,128]{1,0:T(8,128)(2,1)S(1)}, u32[]{:S(2)}, u32[]{:S(2)}) %collective-permute-start.2) | collective-permute-done | bytes 196640 | tf_op jit(solution)/shard_map/ppermute | solution.py:498
  42.4 0.4 collective-permute-start.3
  42.8 1.8 %collective-permute-start.4 = (bf16[1536,128]{1,0:T(8,128)(2,1)S(1)}, bf16[1536,128]{1,0:T(8,128)(2,1)S(1)}, u32[]{:S(2)}, u32[]{:S(2)}) collective-permute-start(bf16[1536,128]{1,0:T(8,128)(2,1)S(1)} %constant_dynamic-update-slice_fusion.refs_0_), channel_id=1, source_target_pairs={{0,4},{2,6},{4,0},{6,2},{1,5},{3,7},{5,1},{7,3},{8,12},{10,14},{12... | collective-permute-start | bytes 1179656 | tf_op jit(solution)/shard_map/ppermute | solution.py:503
  44.6 1.8 %collective-permute-start.5 = (bf16[1536,128]{1,0:T(8,128)(2,1)S(1)}, bf16[1536,128]{1,0:T(8,128)(2,1)S(1)}, u32[]{:S(2)}, u32[]{:S(2)}) collective-permute-start(bf16[1536,128]{1,0:T(8,128)(2,1)S(1)} %constant_dynamic-update-slice_fusion.refs_0_), channel_id=1, source_target_pairs={{0,6},{2,4},{4,2},{6,0},{1,7},{3,5},{5,3},{7,1},{8,14},{10,12},{12... | collective-permute-start | bytes 1179656 | tf_op jit(solution)/shard_map/ppermute | solution.py:503
  46.4 0.0 all-to-all-done.1
  46.4 1.7 %collective-permute-start = (bf16[256,512]{1,0:T(8,128)(2,1)S(1)}, bf16[256,512]{1,0:T(8,128)(2,1)S(1)}, u32[]{:S(2)}, u32[]{:S(2)}) collective-permute-start(bf16[256,512]{1,0:T(8,128)(2,1)S(1)} %bitcast.17), channel_id=1, source_target_pairs={{0,1},{1,0},{2,3},{3,2},{4,5},{5,4},{6,7},{7,6},{8,9},{9,8},{10,11... | collective-permute-start | bytes 786440 | tf_op jit(solution)/shard_map/ppermute | solution.py:556
  48.1 5.6 %collective-permute-done.3.refs_1_ = bf16[1536,128]{1,0:T(8,128)(2,1)S(1)} collective-permute-done((bf16[1536,128]{1,0:T(8,128)(2,1)S(1)}, bf16[1536,128]{1,0:T(8,128)(2,1)S(1)}, u32[]{:S(2)}, u32[]{:S(2)}) %collective-permute-start.3) | collective-permute-done | bytes 393248 | tf_op jit(solution)/shard_map/ppermute | solution.py:503
  53.7 7.6 %collective-permute-done.4.refs_2_ = bf16[1536,128]{1,0:T(8,128)(2,1)S(1)} collective-permute-done((bf16[1536,128]{1,0:T(8,128)(2,1)S(1)}, bf16[1536,128]{1,0:T(8,128)(2,1)S(1)}, u32[]{:S(2)}, u32[]{:S(2)}) %collective-permute-start.4) | collective-permute-done | bytes 393248 | tf_op jit(solution)/shard_map/ppermute | solution.py:503
  61.2 3.1 %collective-permute-done.5.refs_3_ = bf16[1536,128]{1,0:T(8,128)(2,1)S(1)} collective-permute-done((bf16[1536,128]{1,0:T(8,128)(2,1)S(1)}, bf16[1536,128]{1,0:T(8,128)(2,1)S(1)}, u32[]{:S(2)}, u32[]{:S(2)}) %collective-permute-start.5) | collective-permute-done | bytes 393248 | tf_op jit(solution)/shard_map/ppermute | solution.py:503
  64.4 0.0 collective-permute-done.other_ref
  64.4 0.0 copy-done.1
  64.4 0.0 copy-done.2
  64.4 3.1 %experts.1 = (f32[32,4,8,128]{3,2,1,0:T(8,128)S(1)}, bf16[32,4,8,128]{3,2,1,0:T(8,128)(2,1)S(1)}) custom-call(s32[1]{0:T(128)} %bitcast.position_ref, bf16[256,512]{1,0:T(8,128)(2,1)S(1)} %bitcast.18, bf16[256,512]{1,0:T(8,128)(2,1)S(1)} %collective-permute-done.other_ref, bf16[2048,128]{1,0:T(8,128)(2,1)S(1)} %bitcast.21, bf16[2048,128]{1,0:T(8,128)(2,1)S(1)} %bitcast.22, ...), custom_call_target="tpu_custom_call" | custom-call | tf_op jit(solution)/shard_map/experts/pallas_call | solution.py:558
  67.5 0.1 collective-permute-start.6
  67.6 1.5 %collective-permute-done.6.got_ref = bf16[32,4,8,128]{3,2,1,0:T(8,128)(2,1)S(1)} collective-permute-done((bf16[32,4,8,128]{3,2,1,0:T(8,128)(2,1)S(1)}, bf16[32,4,8,128]{3,2,1,0:T(8,128)(2,1)S(1)}, u32[]{:S(2)}, u32[]{:S(2)}) %collective-permute-start.6) | collective-permute-done | bytes 262176 | tf_op jit(solution)/shard_map/ppermute | solution.py:571
  69.1 0.7 add.5
  69.8 13.3 %all-to-all-start.2 = ((bf16[128,8,128]{2,1,0:T(8,128)(2,1)}), bf16[128,8,128]{2,1,0:T(8,128)(2,1)S(1)}, u32[]{:S(2)}, u32[]{:S(2)}) async-start(bf16[128,8,128]{2,1,0:T(8,128)(2,1)} %bitcast.15), calls=%async_computation.2 | async-start | bytes 524288 | tf_op jit(solution)/shard_map/all_to_all | solution.py:412
  83.2 13.7 %all-to-all-done.2 = bf16[128,8,128]{2,1,0:T(8,128)(2,1)S(1)} async-done(((bf16[128,8,128]{2,1,0:T(8,128)(2,1)}), bf16[128,8,128]{2,1,0:T(8,128)(2,1)S(1)}, u32[]{:S(2)}, u32[]{:S(2)}) %all-to-all-start.2) | async-done | bytes 262176 | tf_op jit(solution)/shard_map/all_to_all | solution.py:412
  96.9 0.9 copy-done.4
  97.8 0.8 combine.1
  (18 shorter events, 0.1 us)
Async XLA Ops:
  0.0 13.2 %copy-start.7 = (bf16[128,256]{1,0:T(8,128)(2,1)S(1)}, bf16[128,256]{1,0:T(8,128)(2,1)}, u32[]{:S(2)}) copy-start(bf16[128,256]{1,0:T(8,128)(2,1)} %param.44) | copy-start | bytes 196612
  0.0 13.2 %copy-start.8 = (bf16[256,128]{1,0:T(8,128)(2,1)S(1)}, bf16[256,128]{1,0:T(8,128)(2,1)}, u32[]{:S(2)}) copy-start(bf16[256,128]{1,0:T(8,128)(2,1)} %param.43) | copy-start | bytes 196612
  0.0 13.3 %copy-start.9 = (bf16[256,128]{1,0:T(8,128)(2,1)S(1)}, bf16[256,128]{1,0:T(8,128)(2,1)}, u32[]{:S(2)}) copy-start(bf16[256,128]{1,0:T(8,128)(2,1)} %param.42) | copy-start | bytes 196612
  0.0 23.0 %copy-start.3 = (bf16[16,2048]{1,0:T(8,128)(2,1)S(1)}, bf16[16,2048]{1,0:T(8,128)(2,1)}, u32[]{:S(2)}) copy-start(bf16[16,2048]{1,0:T(8,128)(2,1)} %tokens_ref.1) | copy-start | bytes 196612
  0.0 23.0 %copy-start.5 = (f32[2048]{0:T(1024)S(1)}, f32[2048]{0:T(1024)}, u32[]{:S(2)}) copy-start(f32[2048]{0:T(1024)} %param.35) | copy-start | bytes 24580
  0.0 22.9 %copy-start.6 = (f32[2048]{0:T(1024)S(1)}, f32[2048]{0:T(1024)}, u32[]{:S(2)}) copy-start(f32[2048]{0:T(1024)} %param.45) | copy-start | bytes 24580
  0.0 64.3 %copy-start = (bf16[1,2048,128]{2,1,0:T(8,128)(2,1)S(1)}, bf16[1,2048,128]{2,1,0:T(8,128)(2,1)}, u32[]{:S(2)}) copy-start(bf16[1,2048,128]{2,1,0:T(8,128)(2,1)} %param.39) | copy-start | bytes 1572868
  0.0 64.3 %copy-start.1 = (bf16[1,2048,128]{2,1,0:T(8,128)(2,1)S(1)}, bf16[1,2048,128]{2,1,0:T(8,128)(2,1)}, u32[]{:S(2)}) copy-start(bf16[1,2048,128]{2,1,0:T(8,128)(2,1)} %param.40) | copy-start | bytes 1572868
  0.1 64.3 %copy-start.2 = (bf16[1,128,2048]{2,1,0:T(8,128)(2,1)S(1)}, bf16[1,128,2048]{2,1,0:T(8,128)(2,1)}, u32[]{:S(2)}) copy-start(bf16[1,128,2048]{2,1,0:T(8,128)(2,1)} %param.41) | copy-start | bytes 1572868
  6.6 16.4 %all-to-all-start = ((bf16[8,16,2176]{2,1,0:T(8,128)(2,1)}), bf16[8,16,2176]{2,1,0:T(8,128)(2,1)S(1)}, u32[]{:S(2)}, u32[]{:S(2)}) async-start(bf16[8,16,2176]{2,1,0:T(8,128)(2,1)} %get-tuple-element.12), calls=%async_computation | async-start | bytes 1114112 | tf_op jit(solution)/shard_map/all_to_all | solution.py:412
  13.3 22.5 %collective-permute-start.1 = (bf16[768,128]{1,0:T(8,128)(2,1)S(1)}, bf16[768,128]{1,0:T(8,128)(2,1)S(1)}, u32[]{:S(2)}, u32[]{:S(2)}) collective-permute-start(bf16[768,128]{1,0:T(8,128)(2,1)S(1)} %pad_maximum_fusion), channel_id=1, source_target_pairs={{0,0},{1,9},{8,8},{9,1},{16,16},{17,25},{24,24},{25,17},{2,2},{3,1... | collective-permute-start | bytes 589832 | tf_op jit(solution)/shard_map/ppermute | solution.py:498
  24.1 22.3 %all-to-all-start.1 = ((bf16[32,8,512]{2,1,0:T(8,128)(2,1)}), bf16[32,8,512]{2,1,0:T(8,128)(2,1)S(1)}, u32[]{:S(2)}, u32[]{:S(2)}) async-start(bf16[32,8,512]{2,1,0:T(8,128)(2,1)} %bitcast.10), calls=%async_computation.1 | async-start | bytes 524288 | tf_op jit(solution)/shard_map/all_to_all | solution.py:412
  34.5 8.0 %collective-permute-start.2 = (bf16[768,128]{1,0:T(8,128)(2,1)S(1)}, bf16[768,128]{1,0:T(8,128)(2,1)S(1)}, u32[]{:S(2)}, u32[]{:S(2)}) collective-permute-start(bf16[768,128]{1,0:T(8,128)(2,1)S(1)} %pad_maximum_fusion), channel_id=1, source_target_pairs={{1,0},{0,9},{9,8},{8,1},{17,16},{16,25},{25,24},{24,17},{3,2},{2,1... | collective-permute-start | bytes 589832 | tf_op jit(solution)/shard_map/ppermute | solution.py:498
  42.4 11.2 %collective-permute-start.3 = (bf16[1536,128]{1,0:T(8,128)(2,1)S(1)}, bf16[1536,128]{1,0:T(8,128)(2,1)S(1)}, u32[]{:S(2)}, u32[]{:S(2)}) collective-permute-start(bf16[1536,128]{1,0:T(8,128)(2,1)S(1)} %constant_dynamic-update-slice_fusion.refs_0_), channel_id=1, source_target_pairs={{0,2},{2,0},{4,6},{6,4},{1,3},{3,1},{5,7},{7,5},{8,10},{10,8},{12,... | collective-permute-start | bytes 1179656 | tf_op jit(solution)/shard_map/ppermute | solution.py:503
  42.8 18.4 %collective-permute-start.4 = (bf16[1536,128]{1,0:T(8,128)(2,1)S(1)}, bf16[1536,128]{1,0:T(8,128)(2,1)S(1)}, u32[]{:S(2)}, u32[]{:S(2)}) collective-permute-start(bf16[1536,128]{1,0:T(8,128)(2,1)S(1)} %constant_dynamic-update-slice_fusion.refs_0_), channel_id=1, source_target_pairs={{0,4},{2,6},{4,0},{6,2},{1,5},{3,7},{5,1},{7,3},{8,12},{10,14},{12... | collective-permute-start | bytes 1179656 | tf_op jit(solution)/shard_map/ppermute | solution.py:503
  44.6 19.8 %collective-permute-start.5 = (bf16[1536,128]{1,0:T(8,128)(2,1)S(1)}, bf16[1536,128]{1,0:T(8,128)(2,1)S(1)}, u32[]{:S(2)}, u32[]{:S(2)}) collective-permute-start(bf16[1536,128]{1,0:T(8,128)(2,1)S(1)} %constant_dynamic-update-slice_fusion.refs_0_), channel_id=1, source_target_pairs={{0,6},{2,4},{4,2},{6,0},{1,7},{3,5},{5,3},{7,1},{8,14},{10,12},{12... | collective-permute-start | bytes 1179656 | tf_op jit(solution)/shard_map/ppermute | solution.py:503
  46.4 18.0 %collective-permute-start = (bf16[256,512]{1,0:T(8,128)(2,1)S(1)}, bf16[256,512]{1,0:T(8,128)(2,1)S(1)}, u32[]{:S(2)}, u32[]{:S(2)}) collective-permute-start(bf16[256,512]{1,0:T(8,128)(2,1)S(1)} %bitcast.17), channel_id=1, source_target_pairs={{0,1},{1,0},{2,3},{3,2},{4,5},{5,4},{6,7},{7,6},{8,9},{9,8},{10,11... | collective-permute-start | bytes 786440 | tf_op jit(solution)/shard_map/ppermute | solution.py:556
  67.5 1.6 %collective-permute-start.6 = (bf16[32,4,8,128]{3,2,1,0:T(8,128)(2,1)S(1)}, bf16[32,4,8,128]{3,2,1,0:T(8,128)(2,1)S(1)}, u32[]{:S(2)}, u32[]{:S(2)}) collective-permute-start(bf16[32,4,8,128]{3,2,1,0:T(8,128)(2,1)S(1)} %get-tuple-element.15), channel_id=1, source_target_pairs={{0,1},{1,0},{2,3},{3,2},{4,5},{5,4},{6,7},{7,6},{8,9},{9,8},{10,11... | collective-permute-start | bytes 786440 | tf_op jit(solution)/shard_map/ppermute | solution.py:571
  69.8 27.0 %all-to-all-start.2 = ((bf16[128,8,128]{2,1,0:T(8,128)(2,1)}), bf16[128,8,128]{2,1,0:T(8,128)(2,1)S(1)}, u32[]{:S(2)}, u32[]{:S(2)}) async-start(bf16[128,8,128]{2,1,0:T(8,128)(2,1)} %bitcast.15), calls=%async_computation.2 | async-start | bytes 524288 | tf_op jit(solution)/shard_map/all_to_all | solution.py:412
  96.9 0.9 copy-start.4

commit v5 on v4

--- a/solution.py
+++ b/solution.py
@@ -315,84 +315,116 @@
     return (parts + pltpu.roll(parts, 2, 1)).reshape(rows, width)
 
 
-def mark_kernel(rows_hbm, mark_ref):
-    mark_ref[...] = jnp.zeros_like(mark_ref)
-
-
-LATE = (2, 3)
-
-
-def expert_kernel(position_ref, own_ref, other_ref, gate_ref, up_ref, down_ref, *refs):
-    keep_ref, send_ref, late, left, sems = refs[-5:]
-    operands = refs[:-5]
-    blocks = 2 * len(operands)
+def spread(values, out_ref, start):
+    rows, quarter = values.shape
+    values = values.astype(F32)
+    row = lax.broadcasted_iota(jnp.int32, (rows, 1), 0)
+    for q in range(4):
+        mine = jnp.where(((row >> 1) & 3) == q, values, 0.0)
+        out_ref[start : start + rows, q * quarter : (q + 1) * quarter] = mine.astype(BF16)
+
+
+def picked_hidden(left, gate_ref, up_ref):
+    width = gate_ref.shape[1]
+    weights = jnp.concatenate([gate_ref[...], up_ref[...]], axis=1)
+    both = whole_rows(jnp.dot(left, weights, preferred_element_type=F32))
+    row = lax.broadcasted_iota(jnp.int32, (both.shape[0], 1), 0)
+    hidden = silu(both[:, :width]) * both[:, width:]
+    return jnp.where((row & 1) == 1, 0.0, hidden).astype(BF16)
+
+
+def own_kernel(own_ref, gate_ref, up_ref, left_ref, picked_ref):
+    spread(own_ref[...], left_ref, 0)
+    picked_ref[...] = picked_hidden(left_ref[...], gate_ref, up_ref)
+
+
+LATE = (1, 2)
+
+
+def split_pairs(operands):
+    size = operands[0].shape[0] // 2
+    return {
+        2 * k + i: operands[k].at[pl.ds(i * size, size)]
+        for k in sorted(range(len(operands)), key=LATE.count)
+        for i in range(2)
+    }
+
+
+def down_block(position, k, hidden, down_ref, piece, rows):
+    width = piece.shape[1]
+    kb = 2 * width
+    row = lax.broadcasted_iota(jnp.int32, (rows, 1), 0)
+    right = ((row >> 2) & 1) == 1
+    is_own = ((row >> 1) & 1) == (position & 1)
+    dense_down = jnp.concatenate(
+        [piece[2 * kb : 2 * kb + width], piece[2 * kb + width : 2 * kb + 2 * width]], axis=1
+    )
+    whole = pl.ds(pl.multiple_of((position ^ k) * kb, kb), kb)
+    down = jnp.concatenate([down_ref[:, whole], dense_down], axis=0)
+    result = jnp.dot(hidden, down, preferred_element_type=F32)
+    result = jnp.where(is_own, result[:rows], result[rows:])
+    result = jnp.where(right, result[:, width:], result[:, :width])
+    return result.reshape(rows // 8, 8, width)
+
+
+def expert_kernel(
+    position_ref, left_ref, picked_ref, other_ref, gate_ref, up_ref, down_ref, *refs
+):
+    send_ref, hidden_ref, late, left, sems = refs[-5:]
+    operands = list(refs[:-5])
     copies = [
         pltpu.make_async_copy(operands[k], late.at[i], sems.at[i]) for i, k in enumerate(LATE)
     ]
     for copy in copies:
         copy.start()
-    pairs = {k: operands[k] for k in range(len(operands)) if k not in LATE}
-    pairs.update({k: late.at[i] for i, k in enumerate(LATE)})
-    size = late.shape[1] // 2
-    pieces = {
-        2 * k + i: ref.at[pl.ds(i * size, size)] for k, ref in pairs.items() for i in range(2)
-    }
-    rows, quarter = own_ref.shape
+    for i, k in enumerate(LATE):
+        operands[k] = late.at[i]
+    pieces = split_pairs(operands)
+    rows = other_ref.shape[0]
     width = late.shape[2]
-    kb = 4 * quarter // blocks
+    kb = 2 * width
     position = position_ref[0]
-    core = position & 1
-    row = lax.broadcasted_iota(jnp.int32, (rows, 1), 0)
-    for i, ref in enumerate((own_ref, other_ref)):
-        values = ref[...].astype(F32)
-        for q in range(4):
-            mine = jnp.where(((row >> 1) & 3) == q, values, 0.0)
-            left[i * rows : (i + 1) * rows, q * quarter : (q + 1) * quarter] = mine.astype(BF16)
-    both = jnp.dot(
-        left[...],
-        jnp.concatenate([gate_ref[...], up_ref[...]], axis=1),
-        preferred_element_type=F32,
-    )
-    both = whole_rows(both)
-    row2 = lax.broadcasted_iota(jnp.int32, (2 * rows, 1), 0)
-    is_dense = (row2 & 1) == 1
-    picked = jnp.where(is_dense, 0.0, silu(both[:, :width]) * both[:, width:]).astype(BF16)
-    both = None
+    spread(other_ref[...], left, 0)
+    picked = picked_hidden(left[...], gate_ref, up_ref)
+    sums = [None, None]
     for k, piece in pieces.items():
         if k == 2 * LATE[0]:
             for copy in copies:
                 copy.wait()
         inner = pl.ds(pl.multiple_of((position ^ k) * kb, kb), kb)
         weights = jnp.concatenate([piece[0:kb], piece[kb : 2 * kb]], axis=1)
-        part = jnp.dot(left[:, inner], weights, preferred_element_type=F32)
-        both = part if both is None else both + part
-    both = whole_rows(both)
-    hidden = jnp.where(is_dense, silu(both[:, :width]) * both[:, width:], 0.0).astype(BF16)
-    hidden = jnp.concatenate([picked, hidden], axis=1)
-    right = ((row >> 2) & 1) == 1
-    is_own = ((row >> 1) & 1) == core
+        for i, ref in enumerate((left_ref, left)):
+            part = jnp.dot(ref[:, inner], weights, preferred_element_type=F32)
+            sums[i] = part if sums[i] is None else sums[i] + part
+    row = lax.broadcasted_iota(jnp.int32, (rows, 1), 0)
+    for i, known in enumerate((picked_ref[...], picked)):
+        both = whole_rows(sums[i])
+        dense = silu(both[:, :width]) * both[:, width:]
+        dense = jnp.where((row & 1) == 1, dense, 0.0).astype(BF16)
+        hidden_ref[i * rows : (i + 1) * rows] = jnp.concatenate([known, dense], axis=1)
+    hidden = hidden_ref[...]
     for k, piece in pieces.items():
-        t = position ^ k
-        dense_down = jnp.concatenate(
-            [piece[2 * kb : 2 * kb + width], piece[2 * kb + width : 2 * kb + 2 * width]], axis=1
-        )
-        whole = pl.ds(pl.multiple_of(t * kb, kb), kb)
-        down = jnp.concatenate([down_ref[:, whole], dense_down], axis=0)
-        result = jnp.dot(hidden, down, preferred_element_type=F32)
-        result = jnp.where(is_own, result[:rows], result[rows:])
-        result = jnp.where(right, result[:, width:], result[:, :width])
-        result = result.reshape(rows // 8, 8, width)
+        if k % 2 == 1:
+            block = down_block(position, k, hidden, down_ref, piece, rows)
+            send_ref[:, (position ^ k) >> 1] = block.astype(BF16)
+
+
+def keep_kernel(position_ref, hidden_ref, down_ref, *refs):
+    keep_ref = refs[-1]
+    position = position_ref[0]
+    hidden = hidden_ref[...]
+    rows = hidden.shape[0] // 2
+    for k, piece in split_pairs(refs[:-1]).items():
         if k % 2 == 0:
-            keep_ref[:, t >> 1] = result
-        else:
-            send_ref[:, t >> 1] = result.astype(BF16)
+            block = down_block(position, k, hidden, down_ref, piece, rows)
+            keep_ref[:, (position ^ k) >> 1] = block
 
 
 def add_kernel(keep_ref, got_ref, out_ref):
     out_ref[...] = (keep_ref[...] + got_ref[...].astype(F32)).astype(BF16)
 
 
-def combine_kernel(rows_ref, table_ref, mix_ref, residual_ref, mark_ref, out_ref):
+def combine_kernel(rows_ref, table_ref, mix_ref, residual_ref, out_ref):
     seqs = mix_ref.shape[0]
     width = rows_ref.shape[1]
     sums = jnp.dot(table_ref[...], rows_ref[...], preferred_element_type=F32)
@@ -545,30 +577,53 @@
         mix_vector.reshape(1, -1),
     )
     arrived = exchange(outgoing.reshape(ep_count, 8, -1), EP).reshape(row_count, -1)
-    mark = pl.pallas_call(
-        mark_kernel,
-        name="mark",
-        out_shape=jax.ShapeDtypeStruct((8, 128), F32),
-        in_specs=[ANY],
-        out_specs=VMEM,
+    other = lax.ppermute(arrived, "core", sibling)
+    left, picked = pl.pallas_call(
+        own_kernel,
+        name="own",
+        out_shape=(
+            jax.ShapeDtypeStruct((row_count, model_width), BF16),
+            jax.ShapeDtypeStruct((row_count, head_width), BF16),
+        ),
+        in_specs=[VMEM] * 3,
+        out_specs=(VMEM, VMEM),
         compiler_params=limits(8),
-    )(arrived)
-    other = lax.ppermute(arrived, "core", sibling)
+    )(arrived, expert_gate[0], expert_up[0])
     blocks = (ep_count, tp_count // 2, 8, width_local // 2)
-    keep, send = pl.pallas_call(
+    send, hidden = pl.pallas_call(
         expert_kernel,
         name="experts",
-        out_shape=(jax.ShapeDtypeStruct(blocks, F32), jax.ShapeDtypeStruct(blocks, BF16)),
-        in_specs=[SMEM] + [VMEM] * 5 + [ANY if k in LATE else VMEM for k in range(chips)],
+        out_shape=(
+            jax.ShapeDtypeStruct(blocks, BF16),
+            jax.ShapeDtypeStruct((2 * row_count, 2 * head_width), BF16),
+        ),
+        in_specs=[SMEM] + [VMEM] * 6 + [ANY if k in LATE else VMEM for k in range(chips)],
         out_specs=(VMEM, VMEM),
         scratch_shapes=[
             pltpu.VMEM((len(LATE), *pair.shape), BF16),
-            pltpu.VMEM((2 * row_count, model_width), BF16),
+            pltpu.VMEM((row_count, model_width), BF16),
             pltpu.SemaphoreType.DMA((len(LATE),)),
         ],
         compiler_params=limits(16),
-    )(position, arrived, other, expert_gate[0], expert_up[0], expert_down[0], *dense_weights)
+    )(
+        position,
+        left,
+        picked,
+        other,
+        expert_gate[0],
+        expert_up[0],
+        expert_down[0],
+        *dense_weights,
+    )
     got = lax.ppermute(send, "core", sibling)
+    keep = pl.pallas_call(
+        keep_kernel,
+        name="keep",
+        out_shape=jax.ShapeDtypeStruct(blocks, F32),
+        in_specs=[SMEM] + [VMEM] * (2 + chips),
+        out_specs=VMEM,
+        compiler_params=limits(8),
+    )(position, hidden, expert_down[0], *dense_weights)
     results = pl.pallas_call(
         add_kernel,
         name="add",
@@ -584,10 +639,10 @@
         combine_kernel,
         name="combine",
         out_shape=jax.ShapeDtypeStruct((seqs, width_local), BF16),
-        in_specs=[VMEM] * 4 + [ANY],
+        in_specs=[VMEM] * 4,
         out_specs=VMEM,
         compiler_params=limits(8),
-    )(returned, table, mix_gate, residual, mark)
+    )(returned, table, mix_gate, residual)
 
 
 def solution(mesh):

time: 99 us -> 93.9 us (0.948)
  blocking collectives: 0 us -> 25.8 us
  waiting for transfers between devices: 45.3 us -> 27.9 us
  starting transfers between devices: 39.8 us -> 26.8 us
    all_to_all x0 -> x1, blocking collectives: none -> 25.8 us  [exchange(): return lax.all_to_all(array, axis, 0, 0, tiled=True)]
    all_to_all x3 -> x2, waiting for transfers between devices: 20.9 us -> 7.19 us  [exchange(): return lax.all_to_all(array, axis, 0, 0, tiled=True)]
    all_to_all x3 -> x2, starting transfers between devices: 30.3 us -> 17.2 us  [exchange(): return lax.all_to_all(array, axis, 0, 0, tiled=True)]
    ppermute x3, waiting for transfers between devices: 16.3 us -> 13 us  [body(): lax.ppermute(pair, 'y', [(i, i ^ k) for i in range(chips)])]
    pallas_call x1 -> x2, Pallas kernels: 0.01 us -> 1.93 us  [the longest x1 1.45 us: body(): pl.pallas_call(own_kernel, name='own', out_shape=(jax.ShapeDtypeStruct((r...]
  transfers between devices with their start and end apart: 10 -> 9, of which waited for: 7 -> 5; matrix products, arithmetic and copies ran while one was open for 0% -> 0% of each run, Pallas kernels for 1% -> 3%
where the time goes in v5:
time: 93.9 us; the launch traced here: 93.5 us
  waiting for transfers between devices  27.9 us (30%)
  starting transfers between devices  26.8 us (29%)
  blocking collectives  25.8 us (27%)
  Pallas kernels  12.9 us (14%)
    all_to_all x1, blocking collectives, exchange(): return lax.all_to_all(array, axis, 0, 0, tiled=True)  25.8 us
    all_to_all x2, starting transfers between devices, exchange(): return lax.all_to_all(array, axis, 0, 0, tiled=True)  17.2 us
    ppermute x3, waiting for transfers between devices, body(): lax.ppermute(pair, 'y', [(i, i ^ k) for i in range(chips)])  13 us
    all_to_all x2, waiting for transfers between devices, exchange(): return lax.all_to_all(array, axis, 0, 0, tiled=True)  7.19 us
    ppermute x2, waiting for transfers between devices, body(): first.append(lax.ppermute(own_dense, ('ep_1', 'core'), route))  6.59 us
    pallas_call x1, Pallas kernels, attention_call(): pl.pallas_call(attention_kernel, name='attention', out_shape=(jax.ShapeDt...  6.52 us
    ppermute x2, starting transfers between devices, body(): first.append(lax.ppermute(own_dense, ('ep_1', 'core'), route))  3.8 us
    ppermute x3, starting transfers between devices, body(): lax.ppermute(pair, 'y', [(i, i ^ k) for i in range(chips)])  3.34 us
  transfers between devices with their start and end apart: 9, of which 5 were waited for; matrix products, arithmetic and copies ran while one was open for 0% of the time, Pallas kernels for 3%

profile of v5, /device:TPU:1, one launch (start us, length us, event | category | flops | bytes accessed | tf_op | source)
XLA Modules:
  0.0 93.5 jit_solution(2044711398197398868)
XLA Ops:
  0.0 0.0 copy-start.3
  0.0 0.0 copy-start.5
  0.0 0.0 copy-start.6
  0.0 0.0 copy-start
  0.1 6.5 %attention.1 = (bf16[8,16,2176]{2,1,0:T(8,128)(2,1)}, bf16[96,1024]{1,0:T(8,128)(2,1)}) custom-call(bf16[16,2048]{1,0:T(8,128)(2,1)} %tokens_ref.1, f32[1,2048]{1,0:T(1,128)} %bitcast.27, bf16[2,2048]{1,0:T(2,128)(2,1)} %bitcast.28, f32[1,2]{1,0:T(1,128)} %bitcast.31, f32[16,2,1024]{2,1,0:T(2,128)} %gate_hbm.1, s32[1,16]{1,0:T(1,128)} %bitcast.32, ...), custom_call_target="tpu_custom_call" | custom-call | flops 1000000000 | bytes 12582912 | tf_op jit(solution)/shard_map/attention/pallas_call | solution.py:452
  6.6 0.0 copy-start.2
  6.6 6.7 %all-to-all-start = ((bf16[8,16,2176]{2,1,0:T(8,128)(2,1)}), bf16[8,16,2176]{2,1,0:T(8,128)(2,1)S(1)}, u32[]{:S(2)}, u32[]{:S(2)}) async-start(bf16[8,16,2176]{2,1,0:T(8,128)(2,1)} %get-tuple-element.14), calls=%async_computation | async-start | bytes 1114112 | tf_op jit(solution)/shard_map/all_to_all | solution.py:444
  13.4 2.5 %collective-permute-start.1 = (bf16[768,128]{1,0:T(8,128)(2,1)S(1)}, bf16[768,128]{1,0:T(8,128)(2,1)S(1)}, u32[]{:S(2)}, u32[]{:S(2)}) collective-permute-start(bf16[768,128]{1,0:T(8,128)(2,1)S(1)} %pad_maximum_fusion), channel_id=1, source_target_pairs={{0,0},{1,9},{8,8},{9,1},{16,16},{17,25},{24,24},{25,17},{2,2},{3,1... | collective-permute-start | bytes 589832 | tf_op jit(solution)/shard_map/ppermute | solution.py:530
  15.9 7.2 %all-to-all-done.parts_ref = bf16[8,16,2176]{2,1,0:T(8,128)(2,1)S(1)} async-done(((bf16[8,16,2176]{2,1,0:T(8,128)(2,1)}), bf16[8,16,2176]{2,1,0:T(8,128)(2,1)S(1)}, u32[]{:S(2)}, u32[]{:S(2)}) %all-to-all-start) | async-done | bytes 557088 | tf_op jit(solution)/shard_map/all_to_all | solution.py:444
  23.1 0.0 copy-done.5
  23.1 1.1 %dispatch.1 = (bf16[256,512]{1,0:T(8,128)(2,1)}, f32[16,256]{1,0:T(8,128)S(1)}, f32[16,1]{1,0:T(8,128)S(1)}) custom-call(s32[1]{0:T(128)} %bitcast.position_ref, bf16[8,16,2176]{2,1,0:T(8,128)(2,1)S(1)} %all-to-all-done.parts_ref, bf16[16,2048]{1,0:T(8,128)(2,1)S(1)} %copy-done.3, f32[1,2048]{1,0:T(1,128)S(1)} %bitcast.25, f32[1,2048]{1,0:T(1,128)S(1)} %bitcast.26), custom_call_target="tpu_custom_call" | custom-call | tf_op jit(solution)/shard_map/dispatch/pallas_call | solution.py:572
  24.2 10.5 %all-to-all-start.1 = ((bf16[32,8,512]{2,1,0:T(8,128)(2,1)}), bf16[32,8,512]{2,1,0:T(8,128)(2,1)}, u32[]{:S(2)}, u32[]{:S(2)}) async-start(bf16[32,8,512]{2,1,0:T(8,128)(2,1)} %bitcast.10), calls=%async_computation.1 | async-start | bytes 524288 | tf_op jit(solution)/shard_map/all_to_all | solution.py:444
  34.7 1.3 %collective-permute-start.2 = (bf16[768,128]{1,0:T(8,128)(2,1)S(1)}, bf16[768,128]{1,0:T(8,128)(2,1)S(1)}, u32[]{:S(2)}, u32[]{:S(2)}) collective-permute-start(bf16[768,128]{1,0:T(8,128)(2,1)S(1)} %pad_maximum_fusion), channel_id=1, source_target_pairs={{1,0},{0,9},{9,8},{8,1},{17,16},{16,25},{25,24},{24,17},{3,2},{2,1... | collective-permute-start | bytes 589832 | tf_op jit(solution)/shard_map/ppermute | solution.py:530
  36.0 0.0 collective-permute-done.1
  36.1 6.6 %collective-permute-done.2 = bf16[768,128]{1,0:T(8,128)(2,1)S(1)} collective-permute-done((bf16[768,128]{1,0:T(8,128)(2,1)S(1)}, bf16[768,128]{1,0:T(8,128)(2,1)S(1)}, u32[]{:S(2)}, u32[]{:S(2)}) %collective-permute-start.2) | collective-permute-done | bytes 196640 | tf_op jit(solution)/shard_map/ppermute | solution.py:530
  42.7 1.0 %collective-permute-start.5 = (bf16[1536,128]{1,0:T(8,128)(2,1)S(1)}, bf16[1536,128]{1,0:T(8,128)(2,1)S(1)}, u32[]{:S(2)}, u32[]{:S(2)}) collective-permute-start(bf16[1536,128]{1,0:T(8,128)(2,1)S(1)} %constant_dynamic-update-slice_fusion.refs_0_), channel_id=1, source_target_pairs={{0,6},{2,4},{4,2},{6,0},{1,7},{3,5},{5,3},{7,1},{8,14},{10,12},{12... | collective-permute-start | bytes 1179656 | tf_op jit(solution)/shard_map/ppermute | solution.py:535
  43.7 1.2 %collective-permute-start.4 = (bf16[1536,128]{1,0:T(8,128)(2,1)S(1)}, bf16[1536,128]{1,0:T(8,128)(2,1)S(1)}, u32[]{:S(2)}, u32[]{:S(2)}) collective-permute-start(bf16[1536,128]{1,0:T(8,128)(2,1)S(1)} %constant_dynamic-update-slice_fusion.refs_0_), channel_id=1, source_target_pairs={{0,4},{2,6},{4,0},{6,2},{1,5},{3,7},{5,1},{7,3},{8,12},{10,14},{12... | collective-permute-start | bytes 1179656 | tf_op jit(solution)/shard_map/ppermute | solution.py:535
  44.8 1.2 %collective-permute-start.3 = (bf16[1536,128]{1,0:T(8,128)(2,1)S(1)}, bf16[1536,128]{1,0:T(8,128)(2,1)S(1)}, u32[]{:S(2)}, u32[]{:S(2)}) collective-permute-start(bf16[1536,128]{1,0:T(8,128)(2,1)S(1)} %constant_dynamic-update-slice_fusion.refs_0_), channel_id=1, source_target_pairs={{0,2},{2,0},{4,6},{6,4},{1,3},{3,1},{5,7},{7,5},{8,10},{10,8},{12,... | collective-permute-start | bytes 1179656 | tf_op jit(solution)/shard_map/ppermute | solution.py:535
  46.0 0.0 all-to-all-done.1
  46.0 2.3 %collective-permute-start = (bf16[256,512]{1,0:T(8,128)(2,1)}, bf16[256,512]{1,0:T(8,128)(2,1)S(1)}, u32[]{:S(2)}, u32[]{:S(2)}) collective-permute-start(bf16[256,512]{1,0:T(8,128)(2,1)} %bitcast.11.own_ref), channel_id=1, source_target_pairs={{0,1},{1,0},{2,3},{3,2},{4,5},{5,4},{6,7},{7,6},{8,9},{9,8},{10,11... | collective-permute-start | bytes 786440 | tf_op jit(solution)/shard_map/ppermute | solution.py:580
  48.3 1.4 %own.1 = (bf16[256,2048]{1,0:T(8,128)(2,1)S(1)}, bf16[256,128]{1,0:T(8,128)(2,1)S(1)}) custom-call(bf16[256,512]{1,0:T(8,128)(2,1)} %bitcast.11.own_ref, bf16[2048,128]{1,0:T(8,128)(2,1)S(1)} %bitcast.17, bf16[2048,128]{1,0:T(8,128)(2,1)S(1)} %bitcast.19), custom_call_target="tpu_custom_call" | custom-call | tf_op jit(solution)/shard_map/own/pallas_call | solution.py:581
  49.8 12.1 %collective-permute-done.5.refs_3_ = bf16[1536,128]{1,0:T(8,128)(2,1)S(1)} collective-permute-done((bf16[1536,128]{1,0:T(8,128)(2,1)S(1)}, bf16[1536,128]{1,0:T(8,128)(2,1)S(1)}, u32[]{:S(2)}, u32[]{:S(2)}) %collective-permute-start.5) | collective-permute-done | bytes 393248 | tf_op jit(solution)/shard_map/ppermute | solution.py:535
  61.9 0.0 collective-permute-done.4.refs_2_
  61.9 0.9 collective-permute-done.3.refs_1_
  62.8 0.0 collective-permute-done.other_ref
  62.8 2.5 %experts.1 = (bf16[32,4,8,128]{3,2,1,0:T(8,128)(2,1)S(1)}, bf16[512,256]{1,0:T(8,128)(2,1)S(1)}) custom-call(s32[1]{0:T(128)} %bitcast.position_ref, bf16[256,2048]{1,0:T(8,128)(2,1)S(1)} %get-tuple-element.16.left_ref, bf16[256,128]{1,0:T(8,128)(2,1)S(1)} %get-tuple-element.17.picked_ref, bf16[256,512]{1,0:T(8,128)(2,1)S(1)} %collective-permute-done.other_ref, ...), custom_call_target="tpu_custom_call" | custom-call | tf_op jit(solution)/shard_map/experts/pallas_call | solution.py:593
  65.3 0.1 collective-permute-start.6
  65.4 0.5 keep.1.keep_ref
  65.9 1.0 %collective-permute-done.6.got_ref = bf16[32,4,8,128]{3,2,1,0:T(8,128)(2,1)S(1)} collective-permute-done((bf16[32,4,8,128]{3,2,1,0:T(8,128)(2,1)S(1)}, bf16[32,4,8,128]{3,2,1,0:T(8,128)(2,1)S(1)}, u32[]{:S(2)}, u32[]{:S(2)}) %collective-permute-start.6) | collective-permute-done | bytes 262176 | tf_op jit(solution)/shard_map/ppermute | solution.py:618
  67.0 25.8 %all_to_all.15 = bf16[128,8,128]{2,1,0:T(8,128)(2,1)S(1)} all-to-all(bf16[128,8,128]{2,1,0:T(8,128)(2,1)S(1)} %bitcast.24), channel_id=1, replica_groups=mesh['ep_0'=8,'ep_1'=4,'y'=4,'core'=2] {'ep_0','ep_1','y'}, dimensions={0} | all-to-all | bytes 524288 | tf_op jit(solution)/shard_map/all_to_all | solution.py:444
  92.7 0.0 copy-done.4
  92.7 0.8 combine.1
  (18 shorter events, 0.1 us)
Async XLA Ops:
  0.0 13.3 %copy-start.7 = (bf16[128,256]{1,0:T(8,128)(2,1)S(1)}, bf16[128,256]{1,0:T(8,128)(2,1)}, u32[]{:S(2)}) copy-start(bf16[128,256]{1,0:T(8,128)(2,1)} %param.44) | copy-start | bytes 196612
  0.0 13.4 %copy-start.8 = (bf16[256,128]{1,0:T(8,128)(2,1)S(1)}, bf16[256,128]{1,0:T(8,128)(2,1)}, u32[]{:S(2)}) copy-start(bf16[256,128]{1,0:T(8,128)(2,1)} %param.43) | copy-start | bytes 196612
  0.0 13.4 %copy-start.9 = (bf16[256,128]{1,0:T(8,128)(2,1)S(1)}, bf16[256,128]{1,0:T(8,128)(2,1)}, u32[]{:S(2)}) copy-start(bf16[256,128]{1,0:T(8,128)(2,1)} %param.42) | copy-start | bytes 196612
  0.0 23.1 %copy-start.3 = (bf16[16,2048]{1,0:T(8,128)(2,1)S(1)}, bf16[16,2048]{1,0:T(8,128)(2,1)}, u32[]{:S(2)}) copy-start(bf16[16,2048]{1,0:T(8,128)(2,1)} %tokens_ref.1) | copy-start | bytes 196612
  0.0 23.1 %copy-start.5 = (f32[2048]{0:T(1024)S(1)}, f32[2048]{0:T(1024)}, u32[]{:S(2)}) copy-start(f32[2048]{0:T(1024)} %param.35) | copy-start | bytes 24580
  0.0 23.1 %copy-start.6 = (f32[2048]{0:T(1024)S(1)}, f32[2048]{0:T(1024)}, u32[]{:S(2)}) copy-start(f32[2048]{0:T(1024)} %param.45) | copy-start | bytes 24580
  0.0 48.3 %copy-start = (bf16[1,2048,128]{2,1,0:T(8,128)(2,1)S(1)}, bf16[1,2048,128]{2,1,0:T(8,128)(2,1)}, u32[]{:S(2)}) copy-start(bf16[1,2048,128]{2,1,0:T(8,128)(2,1)} %param.39) | copy-start | bytes 1572868
  0.0 48.3 %copy-start.1 = (bf16[1,2048,128]{2,1,0:T(8,128)(2,1)S(1)}, bf16[1,2048,128]{2,1,0:T(8,128)(2,1)}, u32[]{:S(2)}) copy-start(bf16[1,2048,128]{2,1,0:T(8,128)(2,1)} %param.40) | copy-start | bytes 1572868
  6.6 56.3 %copy-start.2 = (bf16[1,128,2048]{2,1,0:T(8,128)(2,1)S(1)}, bf16[1,128,2048]{2,1,0:T(8,128)(2,1)}, u32[]{:S(2)}) copy-start(bf16[1,128,2048]{2,1,0:T(8,128)(2,1)} %param.41) | copy-start | bytes 1572868
  6.6 16.5 %all-to-all-start = ((bf16[8,16,2176]{2,1,0:T(8,128)(2,1)}), bf16[8,16,2176]{2,1,0:T(8,128)(2,1)S(1)}, u32[]{:S(2)}, u32[]{:S(2)}) async-start(bf16[8,16,2176]{2,1,0:T(8,128)(2,1)} %get-tuple-element.14), calls=%async_computation | async-start | bytes 1114112 | tf_op jit(solution)/shard_map/all_to_all | solution.py:444
  13.4 22.6 %collective-permute-start.1 = (bf16[768,128]{1,0:T(8,128)(2,1)S(1)}, bf16[768,128]{1,0:T(8,128)(2,1)S(1)}, u32[]{:S(2)}, u32[]{:S(2)}) collective-permute-start(bf16[768,128]{1,0:T(8,128)(2,1)S(1)} %pad_maximum_fusion), channel_id=1, source_target_pairs={{0,0},{1,9},{8,8},{9,1},{16,16},{17,25},{24,24},{25,17},{2,2},{3,1... | collective-permute-start | bytes 589832 | tf_op jit(solution)/shard_map/ppermute | solution.py:530
  24.2 21.8 %all-to-all-start.1 = ((bf16[32,8,512]{2,1,0:T(8,128)(2,1)}), bf16[32,8,512]{2,1,0:T(8,128)(2,1)}, u32[]{:S(2)}, u32[]{:S(2)}) async-start(bf16[32,8,512]{2,1,0:T(8,128)(2,1)} %bitcast.10), calls=%async_computation.1 | async-start | bytes 524288 | tf_op jit(solution)/shard_map/all_to_all | solution.py:444
  34.7 7.9 %collective-permute-start.2 = (bf16[768,128]{1,0:T(8,128)(2,1)S(1)}, bf16[768,128]{1,0:T(8,128)(2,1)S(1)}, u32[]{:S(2)}, u32[]{:S(2)}) collective-permute-start(bf16[768,128]{1,0:T(8,128)(2,1)S(1)} %pad_maximum_fusion), channel_id=1, source_target_pairs={{1,0},{0,9},{9,8},{8,1},{17,16},{16,25},{25,24},{24,17},{3,2},{2,1... | collective-permute-start | bytes 589832 | tf_op jit(solution)/shard_map/ppermute | solution.py:530
  42.7 19.3 %collective-permute-start.5 = (bf16[1536,128]{1,0:T(8,128)(2,1)S(1)}, bf16[1536,128]{1,0:T(8,128)(2,1)S(1)}, u32[]{:S(2)}, u32[]{:S(2)}) collective-permute-start(bf16[1536,128]{1,0:T(8,128)(2,1)S(1)} %constant_dynamic-update-slice_fusion.refs_0_), channel_id=1, source_target_pairs={{0,6},{2,4},{4,2},{6,0},{1,7},{3,5},{5,3},{7,1},{8,14},{10,12},{12... | collective-permute-start | bytes 1179656 | tf_op jit(solution)/shard_map/ppermute | solution.py:535
  43.7 18.3 %collective-permute-start.4 = (bf16[1536,128]{1,0:T(8,128)(2,1)S(1)}, bf16[1536,128]{1,0:T(8,128)(2,1)S(1)}, u32[]{:S(2)}, u32[]{:S(2)}) collective-permute-start(bf16[1536,128]{1,0:T(8,128)(2,1)S(1)} %constant_dynamic-update-slice_fusion.refs_0_), channel_id=1, source_target_pairs={{0,4},{2,6},{4,0},{6,2},{1,5},{3,7},{5,1},{7,3},{8,12},{10,14},{12... | collective-permute-start | bytes 1179656 | tf_op jit(solution)/shard_map/ppermute | solution.py:535
  44.8 18.0 %collective-permute-start.3 = (bf16[1536,128]{1,0:T(8,128)(2,1)S(1)}, bf16[1536,128]{1,0:T(8,128)(2,1)S(1)}, u32[]{:S(2)}, u32[]{:S(2)}) collective-permute-start(bf16[1536,128]{1,0:T(8,128)(2,1)S(1)} %constant_dynamic-update-slice_fusion.refs_0_), channel_id=1, source_target_pairs={{0,2},{2,0},{4,6},{6,4},{1,3},{3,1},{5,7},{7,5},{8,10},{10,8},{12,... | collective-permute-start | bytes 1179656 | tf_op jit(solution)/shard_map/ppermute | solution.py:535
  46.0 16.8 %collective-permute-start = (bf16[256,512]{1,0:T(8,128)(2,1)}, bf16[256,512]{1,0:T(8,128)(2,1)S(1)}, u32[]{:S(2)}, u32[]{:S(2)}) collective-permute-start(bf16[256,512]{1,0:T(8,128)(2,1)} %bitcast.11.own_ref), channel_id=1, source_target_pairs={{0,1},{1,0},{2,3},{3,2},{4,5},{5,4},{6,7},{7,6},{8,9},{9,8},{10,11... | collective-permute-start | bytes 786440 | tf_op jit(solution)/shard_map/ppermute | solution.py:580
  62.8 29.9 %copy-start.4 = (bf16[96,1024]{1,0:T(8,128)(2,1)S(1)}, bf16[96,1024]{1,0:T(8,128)(2,1)}, u32[]{:S(2)}) copy-start(bf16[96,1024]{1,0:T(8,128)(2,1)} %get-tuple-element.20.table_ref) | copy-start | bytes 589828
  65.3 1.6 %collective-permute-start.6 = (bf16[32,4,8,128]{3,2,1,0:T(8,128)(2,1)S(1)}, bf16[32,4,8,128]{3,2,1,0:T(8,128)(2,1)S(1)}, u32[]{:S(2)}, u32[]{:S(2)}) collective-permute-start(bf16[32,4,8,128]{3,2,1,0:T(8,128)(2,1)S(1)} %get-tuple-element.19), channel_id=1, source_target_pairs={{0,1},{1,0},{2,3},{3,2},{4,5},{5,4},{6,7},{7,6},{8,9},{9,8},{10,11... | collective-permute-start | bytes 786440 | tf_op jit(solution)/shard_map/ppermute | solution.py:618

commit v6 on v5

--- a/solution.py
+++ b/solution.py
@@ -338,7 +338,7 @@
     picked_ref[...] = picked_hidden(left_ref[...], gate_ref, up_ref)
 
 
-LATE = (1, 2)
+LATE = (1, 2, 3)
 
 
 def split_pairs(operands):
@@ -517,22 +517,6 @@
     width_local = model_width // tp_count
     head_width = key_cache.shape[2]
 
-    own_dense = jnp.concatenate(
-        [dense_gate, dense_up, dense_down[:, :head_width], dense_down[:, head_width:]], axis=0
-    )
-    ep_1 = lax.axis_size("ep_1")
-    same, cross = [], []
-    for e in range(ep_1):
-        same += [(2 * e, 2 * e), (2 * e + 1, 2 * (e ^ 1) + 1)]
-        cross += [(2 * e + 1, 2 * e), (2 * e, 2 * (e ^ 1) + 1)]
-    first = []
-    for route in (same, cross):
-        first.append(lax.ppermute(own_dense, ("ep_1", "core"), route))
-    pair = jnp.concatenate(first, axis=0)
-    dense_weights = [pair]
-    chips = lax.axis_size("y")
-    for k in range(1, chips):
-        dense_weights.append(lax.ppermute(pair, "y", [(i, i ^ k) for i in range(chips)]))
     sibling = [(0, 1), (1, 0)]
     parts, table = attention_call(
         tokens,
@@ -551,6 +535,25 @@
         key_cache,
         value_cache,
     )
+    parts, dense_gate, dense_up, dense_down = lax.optimization_barrier(
+        (parts, dense_gate, dense_up, dense_down)
+    )
+    own_dense = jnp.concatenate(
+        [dense_gate, dense_up, dense_down[:, :head_width], dense_down[:, head_width:]], axis=0
+    )
+    ep_1 = lax.axis_size("ep_1")
+    same, cross = [], []
+    for e in range(ep_1):
+        same += [(2 * e, 2 * e), (2 * e + 1, 2 * (e ^ 1) + 1)]
+        cross += [(2 * e + 1, 2 * e), (2 * e, 2 * (e ^ 1) + 1)]
+    first = []
+    for route in (same, cross):
+        first.append(lax.ppermute(own_dense, ("ep_1", "core"), route))
+    pair = jnp.concatenate(first, axis=0)
+    dense_weights = [pair]
+    chips = lax.axis_size("y")
+    for k in range(1, chips):
+        dense_weights.append(lax.ppermute(pair, "y", [(i, i ^ k) for i in range(chips)]))
     parts = exchange(parts, TP)
 
     position = tp_position.reshape(1)

time: 93.9 us -> 94.3 us (level)
  no operation moved by 1% of the time
where the time goes in v6:
time: 94.3 us; the launch traced here: 93.9 us
  waiting for transfers between devices  27.9 us (30%)
  starting transfers between devices  26.8 us (28%)
  blocking collectives  25.8 us (27%)
  Pallas kernels  13.3 us (14%)
    all_to_all x1, blocking collectives, exchange(): return lax.all_to_all(array, axis, 0, 0, tiled=True)  25.8 us
    all_to_all x2, starting transfers between devices, exchange(): return lax.all_to_all(array, axis, 0, 0, tiled=True)  17.2 us
    ppermute x3, waiting for transfers between devices, body(): lax.ppermute(pair, 'y', [(i, i ^ k) for i in range(chips)])  13 us
    all_to_all x2, waiting for transfers between devices, exchange(): return lax.all_to_all(array, axis, 0, 0, tiled=True)  7.19 us
    ppermute x2, waiting for transfers between devices, body(): first.append(lax.ppermute(own_dense, ('ep_1', 'core'), route))  6.59 us
    pallas_call x1, Pallas kernels, attention_call(): pl.pallas_call(attention_kernel, name='attention', out_shape=(jax.ShapeDt...  6.52 us
    ppermute x2, starting transfers between devices, body(): first.append(lax.ppermute(own_dense, ('ep_1', 'core'), route))  3.8 us
    ppermute x3, starting transfers between devices, body(): lax.ppermute(pair, 'y', [(i, i ^ k) for i in range(chips)])  3.34 us
  transfers between devices with their start and end apart: 9, of which 5 were waited for; matrix products, arithmetic and copies ran while one was open for 0% of the time, Pallas kernels for 3%

profile of v6, /device:TPU:1, one launch (start us, length us, event | category | flops | bytes accessed | tf_op | source)
XLA Modules:
  0.0 93.9 jit_solution(18218317792100452062)
XLA Ops:
  0.0 0.0 copy-start.3
  0.0 0.0 copy-start.5
  0.0 0.0 copy-start.6
  0.0 0.0 copy-start
  0.0 0.0 copy-start.1
  0.1 6.5 %attention.1 = (bf16[8,16,2176]{2,1,0:T(8,128)(2,1)}, bf16[96,1024]{1,0:T(8,128)(2,1)}) custom-call(bf16[16,2048]{1,0:T(8,128)(2,1)} %tokens_ref.1, f32[1,2048]{1,0:T(1,128)} %bitcast.27, bf16[2,2048]{1,0:T(2,128)(2,1)} %bitcast.28, f32[1,2]{1,0:T(1,128)} %bitcast.31, f32[16,2,1024]{2,1,0:T(2,128)} %gate_hbm.1, s32[1,16]{1,0:T(1,128)} %bitcast.32, ...), custom_call_target="tpu_custom_call" | custom-call | flops 1000000000 | bytes 12582912 | tf_op jit(solution)/shard_map/attention/pallas_call | solution.py:452
  6.6 0.0 copy-start.2
  6.6 6.7 %all-to-all-start = ((bf16[8,16,2176]{2,1,0:T(8,128)(2,1)}), bf16[8,16,2176]{2,1,0:T(8,128)(2,1)S(1)}, u32[]{:S(2)}, u32[]{:S(2)}) async-start(bf16[8,16,2176]{2,1,0:T(8,128)(2,1)} %get-tuple-element.19), calls=%async_computation | async-start | bytes 1114112 | tf_op jit(solution)/shard_map/all_to_all | solution.py:444
  13.4 2.5 %collective-permute-start.1 = (bf16[768,128]{1,0:T(8,128)(2,1)S(1)}, bf16[768,128]{1,0:T(8,128)(2,1)S(1)}, u32[]{:S(2)}, u32[]{:S(2)}) collective-permute-start(bf16[768,128]{1,0:T(8,128)(2,1)S(1)} %pad_maximum_fusion), channel_id=1, source_target_pairs={{0,0},{1,9},{8,8},{9,1},{16,16},{17,25},{24,24},{25,17},{2,2},{3,1... | collective-permute-start | bytes 589832 | tf_op jit(solution)/shard_map/ppermute | solution.py:551
  15.9 7.2 %all-to-all-done.parts_ref = bf16[8,16,2176]{2,1,0:T(8,128)(2,1)S(1)} async-done(((bf16[8,16,2176]{2,1,0:T(8,128)(2,1)}), bf16[8,16,2176]{2,1,0:T(8,128)(2,1)S(1)}, u32[]{:S(2)}, u32[]{:S(2)}) %all-to-all-start) | async-done | bytes 557088 | tf_op jit(solution)/shard_map/all_to_all | solution.py:444
  23.1 0.0 copy-done.5
  23.1 1.1 %dispatch.1 = (bf16[256,512]{1,0:T(8,128)(2,1)}, f32[16,256]{1,0:T(8,128)S(1)}, f32[16,1]{1,0:T(8,128)S(1)}) custom-call(s32[1]{0:T(128)} %bitcast.position_ref, bf16[8,16,2176]{2,1,0:T(8,128)(2,1)S(1)} %all-to-all-done.parts_ref, bf16[16,2048]{1,0:T(8,128)(2,1)S(1)} %copy-done.3, f32[1,2048]{1,0:T(1,128)S(1)} %bitcast.25, f32[1,2048]{1,0:T(1,128)S(1)} %bitcast.26), custom_call_target="tpu_custom_call" | custom-call | tf_op jit(solution)/shard_map/dispatch/pallas_call | solution.py:575
  24.2 10.5 %all-to-all-start.1 = ((bf16[32,8,512]{2,1,0:T(8,128)(2,1)}), bf16[32,8,512]{2,1,0:T(8,128)(2,1)}, u32[]{:S(2)}, u32[]{:S(2)}) async-start(bf16[32,8,512]{2,1,0:T(8,128)(2,1)} %bitcast.10), calls=%async_computation.1 | async-start | bytes 524288 | tf_op jit(solution)/shard_map/all_to_all | solution.py:444
  34.7 1.3 %collective-permute-start.2 = (bf16[768,128]{1,0:T(8,128)(2,1)S(1)}, bf16[768,128]{1,0:T(8,128)(2,1)S(1)}, u32[]{:S(2)}, u32[]{:S(2)}) collective-permute-start(bf16[768,128]{1,0:T(8,128)(2,1)S(1)} %pad_maximum_fusion), channel_id=1, source_target_pairs={{1,0},{0,9},{9,8},{8,1},{17,16},{16,25},{25,24},{24,17},{3,2},{2,1... | collective-permute-start | bytes 589832 | tf_op jit(solution)/shard_map/ppermute | solution.py:551
  36.0 0.0 collective-permute-done.1
  36.1 6.6 %collective-permute-done.2 = bf16[768,128]{1,0:T(8,128)(2,1)S(1)} collective-permute-done((bf16[768,128]{1,0:T(8,128)(2,1)S(1)}, bf16[768,128]{1,0:T(8,128)(2,1)S(1)}, u32[]{:S(2)}, u32[]{:S(2)}) %collective-permute-start.2) | collective-permute-done | bytes 196640 | tf_op jit(solution)/shard_map/ppermute | solution.py:551
  42.7 1.0 %collective-permute-start.5 = (bf16[1536,128]{1,0:T(8,128)(2,1)S(1)}, bf16[1536,128]{1,0:T(8,128)(2,1)S(1)}, u32[]{:S(2)}, u32[]{:S(2)}) collective-permute-start(bf16[1536,128]{1,0:T(8,128)(2,1)S(1)} %constant_dynamic-update-slice_fusion.refs_0_), channel_id=1, source_target_pairs={{0,6},{2,4},{4,2},{6,0},{1,7},{3,5},{5,3},{7,1},{8,14},{10,12},{12... | collective-permute-start | bytes 1179656 | tf_op jit(solution)/shard_map/ppermute | solution.py:556
  43.7 1.2 %collective-permute-start.4 = (bf16[1536,128]{1,0:T(8,128)(2,1)S(1)}, bf16[1536,128]{1,0:T(8,128)(2,1)S(1)}, u32[]{:S(2)}, u32[]{:S(2)}) collective-permute-start(bf16[1536,128]{1,0:T(8,128)(2,1)S(1)} %constant_dynamic-update-slice_fusion.refs_0_), channel_id=1, source_target_pairs={{0,4},{2,6},{4,0},{6,2},{1,5},{3,7},{5,1},{7,3},{8,12},{10,14},{12... | collective-permute-start | bytes 1179656 | tf_op jit(solution)/shard_map/ppermute | solution.py:556
  44.8 1.2 %collective-permute-start.3 = (bf16[1536,128]{1,0:T(8,128)(2,1)S(1)}, bf16[1536,128]{1,0:T(8,128)(2,1)S(1)}, u32[]{:S(2)}, u32[]{:S(2)}) collective-permute-start(bf16[1536,128]{1,0:T(8,128)(2,1)S(1)} %constant_dynamic-update-slice_fusion.refs_0_), channel_id=1, source_target_pairs={{0,2},{2,0},{4,6},{6,4},{1,3},{3,1},{5,7},{7,5},{8,10},{10,8},{12,... | collective-permute-start | bytes 1179656 | tf_op jit(solution)/shard_map/ppermute | solution.py:556
  46.0 0.0 all-to-all-done.1
  46.0 2.3 %collective-permute-start = (bf16[256,512]{1,0:T(8,128)(2,1)}, bf16[256,512]{1,0:T(8,128)(2,1)S(1)}, u32[]{:S(2)}, u32[]{:S(2)}) collective-permute-start(bf16[256,512]{1,0:T(8,128)(2,1)} %bitcast.11.own_ref), channel_id=1, source_target_pairs={{0,1},{1,0},{2,3},{3,2},{4,5},{5,4},{6,7},{7,6},{8,9},{9,8},{10,11... | collective-permute-start | bytes 786440 | tf_op jit(solution)/shard_map/ppermute | solution.py:583
  48.3 1.4 %own.1 = (bf16[256,2048]{1,0:T(8,128)(2,1)S(1)}, bf16[256,128]{1,0:T(8,128)(2,1)S(1)}) custom-call(bf16[256,512]{1,0:T(8,128)(2,1)} %bitcast.11.own_ref, bf16[2048,128]{1,0:T(8,128)(2,1)S(1)} %bitcast.17, bf16[2048,128]{1,0:T(8,128)(2,1)S(1)} %bitcast.19), custom_call_target="tpu_custom_call" | custom-call | tf_op jit(solution)/shard_map/own/pallas_call | solution.py:584
  49.8 12.1 %collective-permute-done.5.refs_3_ = bf16[1536,128]{1,0:T(8,128)(2,1)S(1)} collective-permute-done((bf16[1536,128]{1,0:T(8,128)(2,1)S(1)}, bf16[1536,128]{1,0:T(8,128)(2,1)S(1)}, u32[]{:S(2)}, u32[]{:S(2)}) %collective-permute-start.5) | collective-permute-done | bytes 393248 | tf_op jit(solution)/shard_map/ppermute | solution.py:556
  61.9 0.0 collective-permute-done.4.refs_2_
  61.9 0.9 collective-permute-done.3.refs_1_
  62.8 0.0 collective-permute-done.other_ref
  62.8 2.9 %experts.1 = (bf16[32,4,8,128]{3,2,1,0:T(8,128)(2,1)S(1)}, bf16[512,256]{1,0:T(8,128)(2,1)S(1)}) custom-call(s32[1]{0:T(128)} %bitcast.position_ref, bf16[256,2048]{1,0:T(8,128)(2,1)S(1)} %get-tuple-element.21.left_ref, bf16[256,128]{1,0:T(8,128)(2,1)S(1)} %get-tuple-element.22.picked_ref, bf16[256,512]{1,0:T(8,128)(2,1)S(1)} %collective-permute-done.other_ref, ...), custom_call_target="tpu_custom_call" | custom-call | tf_op jit(solution)/shard_map/experts/pallas_call | solution.py:596
  65.7 0.1 collective-permute-start.6
  65.8 0.5 keep.1.keep_ref
  66.3 1.0 %collective-permute-done.6.got_ref = bf16[32,4,8,128]{3,2,1,0:T(8,128)(2,1)S(1)} collective-permute-done((bf16[32,4,8,128]{3,2,1,0:T(8,128)(2,1)S(1)}, bf16[32,4,8,128]{3,2,1,0:T(8,128)(2,1)S(1)}, u32[]{:S(2)}, u32[]{:S(2)}) %collective-permute-start.6) | collective-permute-done | bytes 262176 | tf_op jit(solution)/shard_map/ppermute | solution.py:621
  67.4 25.8 %all_to_all.15 = bf16[128,8,128]{2,1,0:T(8,128)(2,1)S(1)} all-to-all(bf16[128,8,128]{2,1,0:T(8,128)(2,1)S(1)} %bitcast.24), channel_id=1, replica_groups=mesh['ep_0'=8,'ep_1'=4,'y'=4,'core'=2] {'ep_0','ep_1','y'}, dimensions={0} | all-to-all | bytes 524288 | tf_op jit(solution)/shard_map/all_to_all | solution.py:444
  93.1 0.8 combine.1
  (18 shorter events, 0.1 us)
Async XLA Ops:
  0.0 13.3 %copy-start.7 = (bf16[128,256]{1,0:T(8,128)(2,1)S(1)}, bf16[128,256]{1,0:T(8,128)(2,1)}, u32[]{:S(2)}) copy-start(bf16[128,256]{1,0:T(8,128)(2,1)} %param.44) | copy-start | bytes 196612
  0.0 13.4 %copy-start.8 = (bf16[256,128]{1,0:T(8,128)(2,1)S(1)}, bf16[256,128]{1,0:T(8,128)(2,1)}, u32[]{:S(2)}) copy-start(bf16[256,128]{1,0:T(8,128)(2,1)} %param.43) | copy-start | bytes 196612
  0.0 13.4 %copy-start.9 = (bf16[256,128]{1,0:T(8,128)(2,1)S(1)}, bf16[256,128]{1,0:T(8,128)(2,1)}, u32[]{:S(2)}) copy-start(bf16[256,128]{1,0:T(8,128)(2,1)} %param.42) | copy-start | bytes 196612
  0.0 23.1 %copy-start.3 = (bf16[16,2048]{1,0:T(8,128)(2,1)S(1)}, bf16[16,2048]{1,0:T(8,128)(2,1)}, u32[]{:S(2)}) copy-start(bf16[16,2048]{1,0:T(8,128)(2,1)} %tokens_ref.1) | copy-start | bytes 196612
  0.0 23.1 %copy-start.5 = (f32[2048]{0:T(1024)S(1)}, f32[2048]{0:T(1024)}, u32[]{:S(2)}) copy-start(f32[2048]{0:T(1024)} %param.35) | copy-start | bytes 24580
  0.0 23.1 %copy-start.6 = (f32[2048]{0:T(1024)S(1)}, f32[2048]{0:T(1024)}, u32[]{:S(2)}) copy-start(f32[2048]{0:T(1024)} %param.45) | copy-start | bytes 24580
  0.0 48.3 %copy-start = (bf16[1,2048,128]{2,1,0:T(8,128)(2,1)S(1)}, bf16[1,2048,128]{2,1,0:T(8,128)(2,1)}, u32[]{:S(2)}) copy-start(bf16[1,2048,128]{2,1,0:T(8,128)(2,1)} %param.39) | copy-start | bytes 1572868
  0.0 48.3 %copy-start.1 = (bf16[1,2048,128]{2,1,0:T(8,128)(2,1)S(1)}, bf16[1,2048,128]{2,1,0:T(8,128)(2,1)}, u32[]{:S(2)}) copy-start(bf16[1,2048,128]{2,1,0:T(8,128)(2,1)} %param.40) | copy-start | bytes 1572868
  6.6 56.3 %copy-start.2 = (bf16[1,128,2048]{2,1,0:T(8,128)(2,1)S(1)}, bf16[1,128,2048]{2,1,0:T(8,128)(2,1)}, u32[]{:S(2)}) copy-start(bf16[1,128,2048]{2,1,0:T(8,128)(2,1)} %param.41) | copy-start | bytes 1572868
  6.6 16.5 %all-to-all-start = ((bf16[8,16,2176]{2,1,0:T(8,128)(2,1)}), bf16[8,16,2176]{2,1,0:T(8,128)(2,1)S(1)}, u32[]{:S(2)}, u32[]{:S(2)}) async-start(bf16[8,16,2176]{2,1,0:T(8,128)(2,1)} %get-tuple-element.19), calls=%async_computation | async-start | bytes 1114112 | tf_op jit(solution)/shard_map/all_to_all | solution.py:444
  13.4 22.6 %collective-permute-start.1 = (bf16[768,128]{1,0:T(8,128)(2,1)S(1)}, bf16[768,128]{1,0:T(8,128)(2,1)S(1)}, u32[]{:S(2)}, u32[]{:S(2)}) collective-permute-start(bf16[768,128]{1,0:T(8,128)(2,1)S(1)} %pad_maximum_fusion), channel_id=1, source_target_pairs={{0,0},{1,9},{8,8},{9,1},{16,16},{17,25},{24,24},{25,17},{2,2},{3,1... | collective-permute-start | bytes 589832 | tf_op jit(solution)/shard_map/ppermute | solution.py:551
  24.2 21.8 %all-to-all-start.1 = ((bf16[32,8,512]{2,1,0:T(8,128)(2,1)}), bf16[32,8,512]{2,1,0:T(8,128)(2,1)}, u32[]{:S(2)}, u32[]{:S(2)}) async-start(bf16[32,8,512]{2,1,0:T(8,128)(2,1)} %bitcast.10), calls=%async_computation.1 | async-start | bytes 524288 | tf_op jit(solution)/shard_map/all_to_all | solution.py:444
  34.7 7.9 %collective-permute-start.2 = (bf16[768,128]{1,0:T(8,128)(2,1)S(1)}, bf16[768,128]{1,0:T(8,128)(2,1)S(1)}, u32[]{:S(2)}, u32[]{:S(2)}) collective-permute-start(bf16[768,128]{1,0:T(8,128)(2,1)S(1)} %pad_maximum_fusion), channel_id=1, source_target_pairs={{1,0},{0,9},{9,8},{8,1},{17,16},{16,25},{25,24},{24,17},{3,2},{2,1... | collective-permute-start | bytes 589832 | tf_op jit(solution)/shard_map/ppermute | solution.py:551
  42.7 19.3 %collective-permute-start.5 = (bf16[1536,128]{1,0:T(8,128)(2,1)S(1)}, bf16[1536,128]{1,0:T(8,128)(2,1)S(1)}, u32[]{:S(2)}, u32[]{:S(2)}) collective-permute-start(bf16[1536,128]{1,0:T(8,128)(2,1)S(1)} %constant_dynamic-update-slice_fusion.refs_0_), channel_id=1, source_target_pairs={{0,6},{2,4},{4,2},{6,0},{1,7},{3,5},{5,3},{7,1},{8,14},{10,12},{12... | collective-permute-start | bytes 1179656 | tf_op jit(solution)/shard_map/ppermute | solution.py:556
  43.7 18.3 %collective-permute-start.4 = (bf16[1536,128]{1,0:T(8,128)(2,1)S(1)}, bf16[1536,128]{1,0:T(8,128)(2,1)S(1)}, u32[]{:S(2)}, u32[]{:S(2)}) collective-permute-start(bf16[1536,128]{1,0:T(8,128)(2,1)S(1)} %constant_dynamic-update-slice_fusion.refs_0_), channel_id=1, source_target_pairs={{0,4},{2,6},{4,0},{6,2},{1,5},{3,7},{5,1},{7,3},{8,12},{10,14},{12... | collective-permute-start | bytes 1179656 | tf_op jit(solution)/shard_map/ppermute | solution.py:556
  44.8 18.0 %collective-permute-start.3 = (bf16[1536,128]{1,0:T(8,128)(2,1)S(1)}, bf16[1536,128]{1,0:T(8,128)(2,1)S(1)}, u32[]{:S(2)}, u32[]{:S(2)}) collective-permute-start(bf16[1536,128]{1,0:T(8,128)(2,1)S(1)} %constant_dynamic-update-slice_fusion.refs_0_), channel_id=1, source_target_pairs={{0,2},{2,0},{4,6},{6,4},{1,3},{3,1},{5,7},{7,5},{8,10},{10,8},{12,... | collective-permute-start | bytes 1179656 | tf_op jit(solution)/shard_map/ppermute | solution.py:556
  46.0 16.8 %collective-permute-start = (bf16[256,512]{1,0:T(8,128)(2,1)}, bf16[256,512]{1,0:T(8,128)(2,1)S(1)}, u32[]{:S(2)}, u32[]{:S(2)}) collective-permute-start(bf16[256,512]{1,0:T(8,128)(2,1)} %bitcast.11.own_ref), channel_id=1, source_target_pairs={{0,1},{1,0},{2,3},{3,2},{4,5},{5,4},{6,7},{7,6},{8,9},{9,8},{10,11... | collective-permute-start | bytes 786440 | tf_op jit(solution)/shard_map/ppermute | solution.py:583
  62.8 30.3 %copy-start.4 = (bf16[96,1024]{1,0:T(8,128)(2,1)S(1)}, bf16[96,1024]{1,0:T(8,128)(2,1)}, u32[]{:S(2)}) copy-start(bf16[96,1024]{1,0:T(8,128)(2,1)} %get-tuple-element.28.table_ref) | copy-start | bytes 589828
  65.7 1.6 %collective-permute-start.6 = (bf16[32,4,8,128]{3,2,1,0:T(8,128)(2,1)S(1)}, bf16[32,4,8,128]{3,2,1,0:T(8,128)(2,1)S(1)}, u32[]{:S(2)}, u32[]{:S(2)}) collective-permute-start(bf16[32,4,8,128]{3,2,1,0:T(8,128)(2,1)S(1)} %get-tuple-element.27), channel_id=1, source_target_pairs={{0,1},{1,0},{2,3},{3,2},{4,5},{5,4},{6,7},{7,6},{8,9},{9,8},{10,11... | collective-permute-start | bytes 786440 | tf_op jit(solution)/shard_map/ppermute | solution.py:621
